TPU v7x, 128 devices: a whole 4x4x4 slice. The times are simulated.
128 devices in a mesh: sp: 32 (over z, y, core), tp: 4 (over x).
Axes of the slice: x: 4, y: 4, z: 4, core: 2. Of those that a mesh axis runs over, the one named last changes fastest.
Arguments:
- residual_input_stream: bfloat16 [24576, 2048], P('sp'), may hold values from -6 to 6
- projected_queries: bfloat16 [24576, 512], P('sp', 'tp'), may hold values from -6 to 6
- projected_keys: bfloat16 [24576, 512], P('sp', 'tp'), may hold values from -6 to 6
- projected_values: bfloat16 [24576, 1024], P('sp', 'tp'), may hold values from -6 to 6
- emitted_switch_entries: bfloat16 [24576, 1024], P('sp', 'tp'), may hold values from -6 to 6
- retention_preactivations: bfloat16 [24576, 512], P('sp', 'tp'), may hold values from -6 to 15
- additional_fading_amount: float32 [24576], P('sp'), may hold values from -2 to 0
- head_norm_gain: float32 [128], replicated, may hold values from 0.1 to 1.9
- attention_output_weight: bfloat16 [1024, 2048], P('tp'), may hold values from -0.1875 to 0.1875
- feedforward_norm_gain: float32 [2048], replicated, may hold values from 0.1 to 1.9
- gate_up_matrix: bfloat16 [2048, 5632], P('sp', 'tp'), may hold values from -0.125 to 0.125
- value_up_matrix: bfloat16 [2048, 5632], P('sp', 'tp'), may hold values from -0.125 to 0.125
- gate_filter_taps: bfloat16 [3, 5632], P(None, 'tp'), may hold values from -3.5 to 3.5
- value_filter_taps: bfloat16 [3, 5632], P(None, 'tp'), may hold values from -3.5 to 3.5
- down_projection_weight: bfloat16 [5632, 2048], P('tp', 'sp'), may hold values from -0.078125 to 0.078125
Outputs:
- layer_out: bfloat16 [24576, 2048], P(('sp', 'tp'))
All inputs are finite; a program needn't handle non-finite values.
Results may differ from a plain program's by a relative error of at most 0.011.
Values may be sent and summed in bfloat16 or wider, within the bound.
No kernel may reach another device: no remote copies, remote signals or barrier semaphores. Data moves between devices by JAX's collectives and lax.ppermute only.
A program may use at most 128 MiB of HBM per device.

v0:
```python
import jax
import jax.numpy as jnp
from jax import lax
from jax.sharding import Mesh
from jax.sharding import PartitionSpec as P

DK = 64
DV = 128
CONV = 3
BLOCK = 64
SP = ("sp_0", "sp_1", "sp_2")
SP_TP = ("sp_0", "sp_1", "sp_2", "tp")


eps = 1e-06
retention_sharpness = 16.0


def laid_out(pieces, dim):
    pieces = jnp.moveaxis(pieces, 0, dim)
    dims = pieces.shape
    return pieces.reshape(*dims[:dim], dims[dim] * dims[dim + 1], *dims[dim + 2 :])


def copy_for_each(array, axis):
    size = lax.axis_size(axis)
    return lax.all_to_all(
        jnp.broadcast_to(array[None], (size, *array.shape)), axis, 0, 0, tiled=True
    )


def gather_directly(array, axis, dim):
    return laid_out(copy_for_each(array, axis), dim)


def filled_with(array, identity):
    return jax.tree.map(
        lambda part, zero: jnp.zeros_like(part) + jnp.asarray(zero, part.dtype), array, identity
    )


def all_in_one(array, axis):
    leaves = jax.tree.leaves(array)
    order = sorted(range(len(leaves)), key=lambda k: -leaves[k].size)
    width = (1, *leaves[order[0]].shape)[-1]
    lines = [
        jnp.pad(leaves[k].reshape(-1), (0, -leaves[k].size % width)).reshape(-1, width)
        for k in order
    ]
    both, at, found = (lax.all_gather(jnp.concatenate(lines), axis), 0, {})
    for k, line in zip(order, lines):
        share = both[:, at : at + len(line)].reshape(len(both), -1)
        found[k] = share[:, : leaves[k].size].reshape(-1, *leaves[k].shape)
        at += len(line)
    numbers = iter(range(len(leaves)))
    return jax.tree.map(lambda _: found[next(numbers)], array)


def entering(array, axes, combine, identity):
    before = start = filled_with(array, identity)
    subtotal = array
    for axis in reversed(axes):
        size, mine = (lax.axis_size(axis), lax.axis_index(axis))
        pieces = all_in_one(subtotal, axis)
        inside, subtotal = (start, start)
        for k in range(size):
            passed = k < mine
            subtotal = combine(subtotal, jax.tree.map(lambda part: part[k], pieces))
            inside = jax.tree.map(lambda new, old: jnp.where(passed, new, old), subtotal, inside)
        before = combine(inside, before)
    return before


def in_one_piece(arrays, axis, dim, along):
    both = jnp.concatenate(arrays, axis=along)
    out, at, outs = (lax.all_gather(both, axis, axis=dim, tiled=True), 0, [])
    for a in arrays:
        outs.append(lax.slice_in_dim(out, at, at + a.shape[along], axis=along))
        at += a.shape[along]
    return tuple(outs)


def from_behind(block, axis, distance):
    devices = range(lax.axis_size(axis))
    route = [(i - distance, i) for i in devices if i - distance in devices]
    return lax.ppermute(block, axis, route)


def all_blocks(array, axes, order):
    pieces = array[None]
    for k in order:
        pieces = lax.all_gather(pieces, axes[k], axis=0, tiled=True)
    held = [lax.axis_size(axes[k]) for k in reversed(order)]
    pieces = pieces.reshape(*held, *array.shape)
    turned = sorted(range(len(order)), key=lambda place: order[len(order) - 1 - place])
    return pieces.transpose(*turned, *range(len(order), pieces.ndim)).reshape(-1, *array.shape)


def whole_of(array, axes, order, dim):
    return laid_out(all_blocks(array, axes, order), dim)


def split_up(array, dim, size):
    before, after = (array.shape[:dim], array.shape[dim + 1 :])
    return jnp.moveaxis(array.reshape(*before, size, -1, *after), dim, 0)


def summed_on_arrival(array, axis, dim):
    size = lax.axis_size(axis)
    pieces = lax.all_to_all(split_up(array, dim, size), axis, 0, 0, tiled=True)
    return jnp.sum(pieces.astype(jnp.float32), axis=0)


def to_blocks(tensor, local_heads, width):
    count = tensor.shape[0] // BLOCK
    return tensor.astype(jnp.float32).reshape(count, BLOCK, local_heads, width)


def row_norm(stream, gain):
    scaled = stream * lax.rsqrt(jnp.mean(stream * stream, axis=-1, keepdims=True) + eps)
    return (scaled * gain).astype(jnp.bfloat16)


def depthwise(upward, before, taps):
    length = upward.shape[0]
    padded = jnp.concatenate([before, upward], axis=0)
    result = jnp.zeros(upward.shape, jnp.float32)
    for offset in range(CONV):
        result = result + taps[offset].astype(jnp.float32)[None] * padded[
            offset : offset + length
        ].astype(jnp.float32)
    return result


def per_device(
    residual_input_stream,
    projected_queries,
    projected_keys,
    projected_values,
    emitted_switch_entries,
    retention_preactivations,
    additional_fading_amount,
    head_norm_gain,
    attention_output_weight,
    feedforward_norm_gain,
    gate_up_matrix,
    value_up_matrix,
    gate_filter_taps,
    value_filter_taps,
    down_projection_weight,
):
    largest_exponent = lax.Precision.HIGHEST
    tok_rows = residual_input_stream.shape[0]
    local_heads = projected_queries.shape[1] // DK
    out_full = gather_directly(attention_output_weight, "tp", 0)
    retention_logarithm = (
        jax.nn.log_sigmoid(retention_preactivations.astype(jnp.float32)) / retention_sharpness
        + additional_fading_amount[:, None]
    )
    scaled_q = to_blocks(projected_queries, local_heads, DK) * DK ** (-0.5)
    key_heads = to_blocks(projected_keys, local_heads, DK)
    value_heads = to_blocks(projected_values, local_heads, DV)
    rate_cum = jnp.cumsum(to_blocks(retention_logarithm, local_heads, DK), axis=1)
    block_total = rate_cum[:, -1]
    before_block = jnp.cumsum(block_total, axis=0) - block_total
    q_decayed = scaled_q * jnp.exp(rate_cum)
    k_growth = key_heads * jnp.exp(-rate_cum)
    fading_through_finish = key_heads * jnp.exp(block_total[:, None] - rate_cum)
    lower = jnp.tril(jnp.ones((BLOCK, BLOCK), bool))
    scores = jnp.einsum("nihk,njhk->nhij", q_decayed, k_growth, precision=largest_exponent)
    scores = jnp.where(lower[None, None], scores, 0.0)
    within = jnp.einsum("nhij,njhv->nihv", scores, value_heads, precision=largest_exponent)
    increments = jnp.einsum(
        "nchk,nchv->nhkv", fading_through_finish, value_heads, precision=largest_exponent
    )

    def advance_recurrence(state, inputs):
        factor, increment = inputs
        return (factor[..., None] * state + increment, state)

    start_state = jnp.zeros((local_heads, DK, DV), jnp.float32)
    dev_state, state_before = lax.scan(
        advance_recurrence, start_state, (jnp.exp(block_total), increments)
    )
    earlier = jnp.einsum("nchk,nhkv->nchv", q_decayed, state_before, precision=largest_exponent)
    query_shard = scaled_q * jnp.exp(rate_cum + before_block[:, None])
    dev_log = jnp.sum(block_total, axis=0)

    def compose(earlier_pair, later_pair):
        return (
            earlier_pair[0] * later_pair[0],
            later_pair[0][..., None] * earlier_pair[1] + later_pair[1],
        )

    unit = (jnp.ones((local_heads, DK), jnp.float32), start_state)
    carried = entering((jnp.exp(dev_log), dev_state), SP, compose, unit)
    arriving_state = carried[1]
    earlier_memory_share = jnp.einsum(
        "osyq,yqi->osyi", query_shard, arriving_state, precision=largest_exponent
    )
    mech_out = (within + earlier + earlier_memory_share).reshape(tok_rows, local_heads, DV)
    mech_out = (
        mech_out
        * lax.rsqrt(jnp.mean(mech_out * mech_out, axis=-1, keepdims=True) + eps)
        * head_norm_gain
    )
    mixed = (
        mech_out.reshape(tok_rows, local_heads * DV)
        * jax.nn.silu(emitted_switch_entries.astype(jnp.float32))
    ).astype(jnp.bfloat16)
    tp_count = lax.axis_size("tp")
    share = tok_rows // tp_count
    tp_index = lax.axis_index("tp")
    own_input = lax.dynamic_slice_in_dim(residual_input_stream, tp_index * share, share, 0)
    mixed_own = lax.all_to_all(mixed, "tp", split_axis=0, concat_axis=1, tiled=True)
    attended = jnp.dot(mixed_own, out_full, preferred_element_type=jnp.float32)
    resid_own = own_input.astype(jnp.float32) + attended
    normed = gather_directly(row_norm(resid_own, feedforward_norm_gain), "tp", 0)
    pieces = in_one_piece((gate_up_matrix, value_up_matrix), SP, 0, 1)
    gate_sum = jnp.dot(normed, pieces[0], preferred_element_type=jnp.float32)
    value_sum = jnp.dot(normed, pieces[1], preferred_element_type=jnp.float32)
    gate_up = gate_sum.astype(jnp.bfloat16)
    value_up = value_sum.astype(jnp.bfloat16)
    gate_prev, value_prev = from_behind(
        (gate_up[tok_rows - (CONV - 1) :], value_up[tok_rows - (CONV - 1) :]), SP, 1
    )
    gate_mix = depthwise(gate_up, gate_prev, gate_filter_taps)
    value_mix = depthwise(value_up, value_prev, value_filter_taps)
    hidden = (jax.nn.silu(gate_mix) * value_mix).astype(jnp.bfloat16)
    down_full = whole_of(down_projection_weight, (("sp_0", "sp_1"), "sp_2"), (0, 1), 1)
    feed = summed_on_arrival(
        jnp.dot(hidden, down_full, preferred_element_type=jnp.float32).astype(jnp.bfloat16), "tp", 0
    )
    return (resid_own + feed).astype(jnp.bfloat16)


def solution(mesh):
    torus = Mesh(mesh.devices.reshape(4, 4, 2, mesh.shape["tp"]), ("sp_0", "sp_1", "sp_2", "tp"))
    return jax.shard_map(
        per_device,
        mesh=torus,
        in_specs=(
            P(SP, None),
            P(SP, "tp"),
            P(SP, "tp"),
            P(SP, "tp"),
            P(SP, "tp"),
            P(SP, "tp"),
            P(SP),
            P(),
            P("tp", None),
            P(),
            P(SP, "tp"),
            P(SP, "tp"),
            P(None, "tp"),
            P(None, "tp"),
            P("tp", SP),
        ),
        out_specs=P(SP_TP, None),
        check_vma=False,
    )
```

profile of v0, /device:TPU:24, one launch (start us, length us, event | category | flops | bytes accessed | tf_op | source)
XLA Modules:
  0.0 252.4 jit_solution(11430812572905853029)
XLA Ops:
  6.5 0.7 all-gather.15.cloned.1.call-update
  7.3 1.8 pad_maximum_fusion.2
  9.1 1.2 fusion.31
  10.3 0.5 reshape.301
  10.8 0.7 fusion.15
  11.6 0.5 mul.410
  12.0 1.4 reshape.313
  13.7 3.9 %copy_multiply_fusion.2 = (f32[12,64,2,64]{3,0,1,2:T(8,128)}, f32[12,64,2,64]{3,0,1,2:T(8,128)S(1)}, f32[12,64,2,64]{3,0,1,2:T(8,128)S(1)}, f32[12,64,2,64]{3,0,1,2:T(8,128)}) fusion(f32[12,64,2,64]{3,2,1,0:T(2,128)S(1)} %mul.410, f32[12,64,2,64]{3,0,1,2:T(8,128)S(1)} %fusion.15, f32[12,2,64]{2,0,1:T(8,128)S(1)} %get-tuple-element.117, ...), kind=kLoop, calls=%fused_computation.34 | loop fusion | flops 688128 | bytes 2764800 | tf_op jit(solution)/shard_map/mul | solution.py:186
  17.6 1.0 fusion.23
  18.6 9.2 %while.13 = (s32[]{:T(128)}, f32[2,64,128]{2,1,0:T(8,128)S(1)}, f32[12,2,64,128]{3,2,1,0:T(8,128)}, f32[12,2,64]{2,0,1:T(8,128)S(1)}, f32[12,2,64,128]{3,2,1,0:T(8,128)S(1)}, /*index=5*/s32[]{:T(128)}, s32[]{:T(128)}) while((s32[]{:T(128)}, f32[2,64,128]{2,1,0:T(8,128)S(1)}, f32[12,2,64,128]{3,2,1,0:T(8,128)}, ...), condition=%wide.region_2.3_spmd.clone, body=%wide.region_1.2_spmd.clone.sunk | while | flops 65539 | bytes 329824 | solution.py:182
  18.6 0.6 bitcast_dynamic-update-slice_fusion.2
  19.4 0.6 bitcast_dynamic-update-slice_fusion.2
  20.1 0.6 bitcast_dynamic-update-slice_fusion.2
  20.9 0.6 bitcast_dynamic-update-slice_fusion.2
  21.7 0.6 bitcast_dynamic-update-slice_fusion.2
  22.4 0.6 bitcast_dynamic-update-slice_fusion.2
  23.2 0.6 bitcast_dynamic-update-slice_fusion.2
  23.9 0.6 bitcast_dynamic-update-slice_fusion.2
  24.7 0.6 bitcast_dynamic-update-slice_fusion.2
  25.5 0.6 bitcast_dynamic-update-slice_fusion.2
  26.2 0.6 bitcast_dynamic-update-slice_fusion.2
  27.0 0.6 bitcast_dynamic-update-slice_fusion.2
  27.8 1.9 all-gather.4
  29.8 12.5 %all-gather.5 = f32[4,129,128]{2,1,0:T(8,128)S(1)} all-gather(f32[1,129,128]{2,1,0:T(8,128)S(1)} %maximum_bitcast_fusion.1), channel_id=3, replica_groups=mesh['sp_0'=4,'sp_1'=4,'sp_2'=2,'tp'=4] {'sp_1'}, dimensions={0}, use_global_device_ids=true | all-gather | bytes 330240 | tf_op jit(solution)/shard_map/all_gather | solution.py:50
  43.0 15.7 %all-gather.6 = f32[4,129,128]{2,1,0:T(8,128)S(1)} all-gather(f32[1,129,128]{2,1,0:T(8,128)S(1)} %maximum_bitcast_fusion.2), channel_id=4, replica_groups=mesh['sp_0'=4,'sp_1'=4,'sp_2'=2,'tp'=4] {'sp_0'}, dimensions={0}, use_global_device_ids=true | all-gather | bytes 330240 | tf_op jit(solution)/shard_map/all_gather | solution.py:50
  59.1 2.3 convolution_bitcast_fusion.1
  61.5 1.9 convolution_select_fusion
  63.4 0.5 fusion.14
  64.0 1.5 multiply_reduce_fusion.1
  65.7 0.6 copy.97
  66.4 1.0 mul.473
  67.6 11.5 %all_to_all.31 = bf16[4,192,256]{2,1,0:T(8,128)(2,1)S(1)} all-to-all(bf16[4,192,256]{2,1,0:T(8,128)(2,1)S(1)} %bitcast.153), channel_id=1, replica_groups=mesh['sp_0'=4,'sp_1'=4,'sp_2'=2,'tp'=4] {'tp'}, dimensions={0} | all-to-all | bytes 786432 | tf_op jit(solution)/shard_map/all_to_all | solution.py:215
  79.1 2.5 %broadcast_in_dim.70 = bf16[4,256,2048]{2,1,0:T(8,128)(2,1)} broadcast(bf16[256,2048]{1,0:T(8,128)(2,1)S(1)} %copy-done.5), dimensions={1,2} | broadcast | bytes 5242880 | tf_op jit(solution)/shard_map/broadcast_in_dim | solution.py:28
  81.7 4.8 %all-to-all-start.1 = ((bf16[4,256,2048]{2,1,0:T(8,128)(2,1)}), bf16[4,256,2048]{2,1,0:T(8,128)(2,1)}, u32[]{:S(2)}, u32[]{:S(2)}) async-start(bf16[4,256,2048]{2,1,0:T(8,128)(2,1)} %broadcast_in_dim.70), calls=%async_computation.1 | async-start | bytes 8388608 | tf_op jit(solution)/shard_map/all_to_all | solution.py:27
  86.6 3.8 %copy.108 = bf16[8,8,16,1408]{3,2,1,0:T(8,128)(2,1)} copy(bf16[8,8,16,1408]{3,1,2,0:T(8,128)(2,1)} %bitcast.151) | data formatting | bytes 5767168
  90.5 38.2 %all-to-all-done.1 = bf16[4,256,2048]{2,1,0:T(8,128)(2,1)} async-done(((bf16[4,256,2048]{2,1,0:T(8,128)(2,1)}), bf16[4,256,2048]{2,1,0:T(8,128)(2,1)}, u32[]{:S(2)}, u32[]{:S(2)}) %all-to-all-start.1) | async-done | bytes 4194336 | tf_op jit(solution)/shard_map/all_to_all | solution.py:27
  128.7 3.5 %multiply_reduce_fusion = (f32[192]{0:T(256)S(1)}, f32[192,2048]{1,0:T(8,128)S(1)}) fusion(bf16[4,256,2048]{2,1,0:T(8,128)(2,1)} %all-to-all-done.1, bf16[4,192,256]{2,1,0:T(8,128)(2,1)S(1)} %all_to_all.31, bf16[768,2048]{1,0:T(8,128)(2,1)} %param.17, s32[]{:T(128)S(6)} %select_n.144), kind=kOutput, calls=%fused_computation.24 | convolution fusion | flops 806879040 | bytes 6947588 | tf_op jit(solution)/shard_map/dot_general | solution.py:216
  132.9 33.4 %all_to_all.32 = bf16[4,192,2048]{2,1,0:T(8,128)(2,1)} all-to-all(bf16[4,192,2048]{2,1,0:T(8,128)(2,1)S(1)} %broadcast_in_dim.71), channel_id=1, replica_groups=mesh['sp_0'=4,'sp_1'=4,'sp_2'=2,'tp'=4] {'tp'}, dimensions={0} | all-to-all | bytes 6291456 | tf_op jit(solution)/shard_map/all_to_all | solution.py:27
  166.3 8.5 %fusion.4 = bf16[768,1408]{1,0:T(8,128)(2,1)S(1)} fusion(bf16[768,2048]{1,0:T(8,128)(2,1)} %bitcast.146, bf16[2048,2816]{1,0:T(8,128)(2,1)} %all-gather.11.cloned.1.call-done), kind=kOutput, calls=%fused_computation.9 | convolution fusion | flops 4430266368 | bytes 11075584 | tf_op jit(solution)/shard_map/dot_general | solution.py:220
  174.8 1.4 copy-done.13
  176.2 1.9 collective-permute-start
  178.1 5.3 %fusion.7 = bf16[768,1408]{1,0:T(8,128)(2,1)S(1)} fusion(bf16[768,2048]{1,0:T(8,128)(2,1)S(1)} %bitcast.147, bf16[2048,2816]{1,0:T(8,128)(2,1)S(1)} %copy-done.17), kind=kOutput, calls=%fused_computation.10 | convolution fusion | flops 4430266368 | bytes 11075584 | tf_op jit(solution)/shard_map/dot_general | solution.py:221
  183.4 6.7 %collective-permute-start.1 = (bf16[2,1408]{1,0:T(2,128)(2,1)S(1)}, bf16[2,1408]{1,0:T(2,128)(2,1)S(1)}, u32[]{:S(2)}, u32[]{:S(2)}) collective-permute-start(bf16[2,1408]{1,0:T(2,128)(2,1)S(1)} %slice.212), channel_id=1, source_target_pairs={{0,4},{4,8},{8,12},{12,16},{16,20},{20,24},{24,28},{28,32},{32,36}... | collective-permute-start | bytes 16904 | tf_op jit(solution)/shard_map/ppermute | solution.py:86
  190.4 4.7 %copy.101 = bf16[16,2,1408,64]{2,3,1,0:T(8,128)(2,1)S(1)} copy(bf16[16,2,1408,64]{2,0,1,3:T(8,128)(2,1)} %bitcast.144) | data formatting | bytes 11534336 | tf_op jit(solution)/shard_map/transpose | solution.py:96
  195.1 8.4 %convolution_convert_fusion = bf16[768,2048]{1,0:T(8,128)(2,1)S(1)} fusion(bf16[1408,2048]{0,1:T(8,128)(2,1)S(1)} %bitcast.145, bf16[768,1408]{1,0:T(8,128)(2,1)S(1)} %copy-done.16, bf16[768,1408]{1,0:T(8,128)(2,1)S(1)} %copy-done.14, bf16[2,1408]{1,0:T(2,128)(2,1)S(1)} %collective-permute-done.1, bf16[2,1408]{1,0:T(2,128)(2,1)S(1)} %collective-permute-done, ...), kind=kOutput, calls=%fused_computation.11 | convolution fusion | flops 4467523584 | bytes 13283328 | tf_op jit(solution)/shard_map/dot_general | solution.py:232
  203.6 40.5 %all_to_all.33 = bf16[4,192,2048]{2,1,0:T(8,128)(2,1)S(1)} all-to-all(bf16[4,192,2048]{2,1,0:T(8,128)(2,1)S(1)} %bitcast.148), channel_id=1, replica_groups=mesh['sp_0'=4,'sp_1'=4,'sp_2'=2,'tp'=4] {'tp'}, dimensions={0} | all-to-all | bytes 6291456 | tf_op jit(solution)/shard_map/all_to_all | solution.py:110
  244.1 0.6 convert_reduce_fusion
  244.7 1.1 add_convert_fusion
  (112 shorter events, 4.1 us)
Async XLA Ops:
  6.5 59.8 %copy-start = (f32[128]{0:T(128)S(1)}, f32[128]{0:T(128)}, u32[]{:S(2)}) copy-start(f32[128]{0:T(128)} %param.24) | copy-start | bytes 1540
  6.5 5.0 %copy-start.8 = (bf16[768,128]{1,0:T(8,128)(2,1)S(1)}, bf16[768,128]{1,0:T(8,128)(2,1)}, u32[]{:S(2)}) copy-start(bf16[768,128]{1,0:T(8,128)(2,1)} %param.18) | copy-start | bytes 589828
  6.5 5.5 %copy-start.9 = (bf16[768,128]{1,0:T(8,128)(2,1)S(1)}, bf16[768,128]{1,0:T(8,128)(2,1)}, u32[]{:S(2)}) copy-start(bf16[768,128]{1,0:T(8,128)(2,1)} %param.19) | copy-start | bytes 589828
  6.5 80.1 %all-gather.15.cloned.1.call-start = ((), (), s32[]{:S(2)}) async-start(), calls=%async_computation.6 | async-start | bytes 3063808 | tf_op jit(solution)/shard_map/all_gather | solution.py:92
  7.3 159.0 %all-gather.11.cloned.1.call-start = ((), (), s32[]{:S(2)}) async-start(), calls=%async_computation.4 | async-start | bytes 11894784 | tf_op jit(solution)/shard_map/all_gather | solution.py:76
  10.8 2.6 %copy-start.6 = (bf16[768,256]{1,0:T(8,128)(2,1)S(1)}, bf16[768,256]{1,0:T(8,128)(2,1)}, u32[]{:S(2)}) copy-start(bf16[768,256]{1,0:T(8,128)(2,1)} %param.20) | copy-start | bytes 1179652
  17.6 43.9 %copy-start.3 = (f32[12,64,2,64]{3,0,1,2:T(8,128)S(1)}, f32[12,64,2,64]{3,0,1,2:T(8,128)}, u32[]{:S(2)}) copy-start(f32[12,64,2,64]{3,0,1,2:T(8,128)} %get-tuple-element.119) | copy-start | bytes 1179652
  59.1 4.9 %copy-start.2 = (f32[12,64,2,64]{3,0,1,2:T(8,128)S(1)}, f32[12,64,2,64]{3,0,1,2:T(8,128)}, u32[]{:S(2)}) copy-start(f32[12,64,2,64]{3,0,1,2:T(8,128)} %get-tuple-element.111) | copy-start | bytes 1179652
  63.4 4.0 %copy-start.7 = (bf16[768,256]{1,0:T(8,128)(2,1)S(1)}, bf16[768,256]{1,0:T(8,128)(2,1)}, u32[]{:S(2)}) copy-start(bf16[768,256]{1,0:T(8,128)(2,1)} %param.21) | copy-start | bytes 1179652
  64.0 15.2 %copy-start.5 = (bf16[256,2048]{1,0:T(8,128)(2,1)S(1)}, bf16[256,2048]{1,0:T(8,128)(2,1)}, u32[]{:S(2)}) copy-start(bf16[256,2048]{1,0:T(8,128)(2,1)} %param.25) | copy-start | bytes 3145732
  81.7 47.0 %all-to-all-start.1 = ((bf16[4,256,2048]{2,1,0:T(8,128)(2,1)}), bf16[4,256,2048]{2,1,0:T(8,128)(2,1)}, u32[]{:S(2)}, u32[]{:S(2)}) async-start(bf16[4,256,2048]{2,1,0:T(8,128)(2,1)} %broadcast_in_dim.70), calls=%async_computation.1 | async-start | bytes 8388608 | tf_op jit(solution)/shard_map/all_to_all | solution.py:27
  86.5 103.8 %all-gather.13.cloned.1.call-start = ((), (), s32[]{:S(2)}) async-start(), calls=%async_computation.5 | async-start | bytes 8650752 | tf_op jit(solution)/shard_map/all_gather | solution.py:92
  90.4 41.8 %copy-start.12 = (f32[2048]{0:T(1024)S(1)}, f32[2048]{0:T(1024)}, u32[]{:S(2)}) copy-start(f32[2048]{0:T(1024)} %param.26) | copy-start | bytes 24580
  166.2 11.8 %copy-start.4 = (bf16[4,192,2048]{2,1,0:T(8,128)(2,1)S(1)}, bf16[4,192,2048]{2,1,0:T(8,128)(2,1)}, u32[]{:S(2)}) copy-start(bf16[4,192,2048]{2,1,0:T(8,128)(2,1)} %all_to_all.32) | copy-start | bytes 9437188
  166.3 11.8 %copy-start.17 = (bf16[2048,2816]{1,0:T(8,128)(2,1)S(1)}, bf16[2048,2816]{1,0:T(8,128)(2,1)}, u32[]{:S(2)}) copy-start(bf16[2048,2816]{1,0:T(8,128)(2,1)} %all-gather.11.cloned.1.call-done) | copy-start | bytes 34603012
  174.7 1.4 copy-start.13
  176.1 14.1 %copy-start.10 = (bf16[3,1408]{1,0:T(4,128)(2,1)S(1)}, bf16[3,1408]{1,0:T(4,128)(2,1)}, u32[]{:S(2)}) copy-start(bf16[3,1408]{1,0:T(4,128)(2,1)} %param.30) | copy-start | bytes 25348
  176.1 14.1 %copy-start.11 = (bf16[3,1408]{1,0:T(4,128)(2,1)S(1)}, bf16[3,1408]{1,0:T(4,128)(2,1)}, u32[]{:S(2)}) copy-start(bf16[3,1408]{1,0:T(4,128)(2,1)} %param.29) | copy-start | bytes 25348
  176.2 18.9 %collective-permute-start = (bf16[2,1408]{1,0:T(2,128)(2,1)S(1)}, bf16[2,1408]{1,0:T(2,128)(2,1)S(1)}, u32[]{:S(2)}, u32[]{:S(2)}) collective-permute-start(bf16[2,1408]{1,0:T(2,128)(2,1)S(1)} %slice.208), channel_id=1, source_target_pairs={{0,4},{4,8},{8,12},{12,16},{16,20},{20,24},{24,28},{28,32},{32,36}... | collective-permute-start | bytes 16904 | tf_op jit(solution)/shard_map/ppermute | solution.py:86
  183.4 6.8 %copy-start.15 = (bf16[768,1408]{1,0:T(8,128)(2,1)}, bf16[768,1408]{1,0:T(8,128)(2,1)S(1)}, u32[]{:S(2)}) copy-start(bf16[768,1408]{1,0:T(8,128)(2,1)S(1)} %fusion.7) | copy-start | bytes 6488068
  183.4 11.6 %collective-permute-start.1 = (bf16[2,1408]{1,0:T(2,128)(2,1)S(1)}, bf16[2,1408]{1,0:T(2,128)(2,1)S(1)}, u32[]{:S(2)}, u32[]{:S(2)}) collective-permute-start(bf16[2,1408]{1,0:T(2,128)(2,1)S(1)} %slice.212), channel_id=1, source_target_pairs={{0,4},{4,8},{8,12},{12,16},{16,20},{20,24},{24,28},{28,32},{32,36}... | collective-permute-start | bytes 16904 | tf_op jit(solution)/shard_map/ppermute | solution.py:86
  190.4 4.7 %copy-start.14 = (bf16[768,1408]{1,0:T(8,128)(2,1)S(1)}, bf16[768,1408]{1,0:T(8,128)(2,1)}, u32[]{:S(2)}) copy-start(bf16[768,1408]{1,0:T(8,128)(2,1)} %copy-done.13) | copy-start | bytes 6488068
  190.4 4.7 %copy-start.16 = (bf16[768,1408]{1,0:T(8,128)(2,1)S(1)}, bf16[768,1408]{1,0:T(8,128)(2,1)}, u32[]{:S(2)}) copy-start(bf16[768,1408]{1,0:T(8,128)(2,1)} %copy-done.15) | copy-start | bytes 6488068
  203.5 42.3 %copy-start.1 = (f32[128]{0:T(128)S(1)}, f32[128]{0:T(128)}, u32[]{:S(2)}) copy-start(f32[128]{0:T(128)} %param.24) | copy-start | bytes 1540
Sparse Core Ops, SparseCore 0:
  9.5 49.9 all-gather.14
  61.8 59.6 all-gather.10
  123.2 18.2 all-gather.12
where the time goes:
time: 253 us; the launch traced here: 252 us
  blocking collectives  115 us (45%)
  waiting for transfers between devices  39 us (15%)
  matrix products  33 us (13%)
  other arithmetic  19.1 us (8%)
  local copies, waits for them, and re-layouts  18.1 us (7%)
  between operations  13.7 us (5%)
  starting transfers between devices  13.6 us (5%)
    all_to_all x1, blocking collectives, summed_on_arrival(): pieces = lax.all_to_all(split_up(array, dim, size), axis, 0, 0, tiled=True)  40.5 us
    all_to_all x1, waiting for transfers between devices, copy_for_each(): lax.all_to_all(jnp.broadcast_to(array[None], (size, *array.shape)), axis,...  38.2 us
    all_to_all x1, blocking collectives, copy_for_each(): lax.all_to_all(jnp.broadcast_to(array[None], (size, *array.shape)), axis,...  33.4 us
    all_gather x3, blocking collectives, all_in_one(): both, at, found = (lax.all_gather(jnp.concatenate(lines), axis), 0, {})  30.1 us
    all_to_all x1, blocking collectives, per_device(): lax.all_to_all(mixed, 'tp', split_axis=0, concat_axis=1, tiled=True)  11.5 us
    ppermute x2, starting transfers between devices, from_behind(): return lax.ppermute(block, axis, route)  8.66 us
    dot_general x1, matrix products, per_device(): gate_sum = jnp.dot(normed, pieces[0], preferred_element_type=jnp.float32)  8.48 us
    dot_general x1, matrix products, per_device(): jnp.dot(hidden, down_full, preferred_element_type=jnp.float32)  8.43 us
  transfers between devices with their start and end apart: 6, of which 1 were waited for; matrix products, arithmetic and copies ran while one was open for 23% of the time, Pallas kernels for 0%

commit v1 on v0

v1 whole, which is shorter than its diff:
```python
import functools
import jax
import jax.numpy as jnp
from jax import lax
from jax.experimental import pallas as pl
from jax.experimental.pallas import tpu as pltpu
from jax.sharding import Mesh
from jax.sharding import PartitionSpec as P

DK = 64
DV = 128
BLOCK = 64
TOK = 768
D = 2048
HID = 1408
HALO = 16
Z, Y, C, X = "z", "y", "c", "x"
SP = (Z, Y, C)
EPS = 1e-06
f32 = jnp.float32
bf16 = jnp.bfloat16
NT = (((1,), (1,)), ((), ()))
TN = (((0,), (0,)), ((), ()))
PACK = 136
VMEM = pl.BlockSpec(memory_space=pltpu.VMEM)


def _params(mib=40, sem=None):
    return pltpu.CompilerParams(vmem_limit_bytes=mib * 1024 * 1024, dimension_semantics=sem)


def _cost(flops, nbytes, trans=0):
    return pl.CostEstimate(flops=int(flops), bytes_accessed=int(nbytes), transcendentals=int(trans))


def _dot(a, b, dims=None):
    if dims is None:
        dims = (((1,), (0,)), ((), ()))
    return lax.dot_general(a, b, dims, preferred_element_type=f32)


def _log_sigmoid(x):
    return jnp.minimum(x, 0.0) - jnp.log1p(jnp.exp(-jnp.abs(x)))


def _silu(x):
    return x / (1.0 + jnp.exp(-x))


def _first_head():
    return lax.broadcasted_iota(jnp.int32, (1, 2 * DK), 1) < DK


def state_kernel(pre_ref, fade_ref, k_ref, v_ref, cum_ref, pack_ref, kf_ref):
    row = lax.broadcasted_iota(jnp.int32, (128, 128), 0)
    col = lax.broadcasted_iota(jnp.int32, (128, 128), 1)
    lower = ((row >= col) & ((row < BLOCK) == (col < BLOCK))).astype(f32)
    ones = jnp.ones((128, 128), f32)
    high = lax.Precision.HIGHEST
    cums = []
    for n in range(TOK // 128):
        rows = slice(n * 128, (n + 1) * 128)
        rate = _log_sigmoid(pre_ref[rows, :].astype(f32)) * (1.0 / 16.0)
        cum = jnp.dot(lower, rate, precision=high, preferred_element_type=f32)
        cum = cum + jnp.dot(
            lower * fade_ref[n : n + 1, :], ones, precision=high, preferred_element_type=f32
        )
        cum_ref[rows, :] = cum
        cums.append(cum)
    suffix = jnp.zeros((1, 2 * DK), f32)
    for b in reversed(range(TOK // BLOCK)):
        n, half = divmod(b, 2)
        cum = cums[n][half * BLOCK : (half + 1) * BLOCK]
        total = cum[BLOCK - 1 : BLOCK]
        rows = slice(b * BLOCK, (b + 1) * BLOCK)
        kf_ref[rows, :] = (k_ref[rows, :].astype(f32) * jnp.exp(suffix + total - cum)).astype(bf16)
        suffix = suffix + total
    kf = kf_ref[...]
    first = _dot(v_ref[:, :DV], kf, TN)
    second = _dot(v_ref[:, DV:], kf, TN)
    pack_ref[0:128, :] = jnp.where(_first_head(), first, second)
    pack_ref[128:PACK, :] = jnp.broadcast_to(jnp.exp(suffix), (8, 128))


def local_kernel(q_ref, k_ref, v_ref, cum_ref, mech_ref, qs_ref):
    head = _first_head()
    row = lax.broadcasted_iota(jnp.int32, (128, BLOCK), 0)
    col = lax.broadcasted_iota(jnp.int32, (128, BLOCK), 1)
    lower = jnp.where(row < BLOCK, row, row - BLOCK) >= col
    state = jnp.zeros((DV, 2 * DK), f32)
    before = jnp.zeros((1, 2 * DK), f32)
    for b in range(TOK // BLOCK):
        rows = slice(b * BLOCK, (b + 1) * BLOCK)
        cum = cum_ref[rows, :]
        total = cum[BLOCK - 1 : BLOCK]
        q = q_ref[rows, :].astype(f32) * DK**-0.5
        k = k_ref[rows, :].astype(f32)
        qd = q * jnp.exp(cum)
        qs_ref[rows, :] = (q * jnp.exp(cum + before)).astype(bf16)
        both = jnp.concatenate([jnp.where(head, qd, 0.0), jnp.where(head, 0.0, qd)], 0).astype(bf16)
        grown = (k * jnp.exp(-cum)).astype(bf16)
        faded = (k * jnp.exp(total - cum)).astype(bf16)
        scores = _dot(both, grown, NT)
        scores = jnp.where(lower, scores, 0.0).astype(bf16)
        inter = _dot(both, state.astype(bf16), NT)
        v0, v1 = v_ref[rows, :DV], v_ref[rows, DV:]
        mech_ref[rows, :DV] = _dot(scores[:BLOCK], v0) + inter[:BLOCK]
        mech_ref[rows, DV:] = _dot(scores[BLOCK:], v1) + inter[BLOCK:]
        update = jnp.where(head, _dot(v0, faded, TN), _dot(v1, faded, TN))
        state = state * jnp.exp(total) + update
        before = before + total


def chip_kernel(own_ref, other_ref, chip_ref):
    second = lax.axis_index(C) == 1
    own_s, own_d = own_ref[0:128, :], own_ref[128:PACK, :]
    oth_s, oth_d = other_ref[0:128, :], other_ref[128:PACK, :]
    s = jnp.where(second, own_d[0:1] * oth_s + own_s, oth_d[0:1] * own_s + oth_s)
    chip_ref[0:128, :] = s
    chip_ref[128:PACK, :] = own_d * oth_d


def plane_kernel(own_ref, up_ref, opp_ref, down_ref, total_ref, before_ref, held):
    y = lax.axis_index(Y)
    held[0] = own_ref[...]
    held[1] = up_ref[...]
    held[2] = opp_ref[...]
    held[3] = down_ref[...]
    s = jnp.zeros((128, 128), f32)
    d = jnp.ones((8, 128), f32)
    before_ref[0:128, :] = s
    before_ref[128:PACK, :] = d
    for k in range(4):
        if k > 0:

            @pl.when(y == k)
            def _(s=s, d=d):
                before_ref[0:128, :] = s
                before_ref[128:PACK, :] = d

        piece = held[lax.rem(k - y + 4, 4)]
        s = piece[128:129] * s + piece[0:128]
        d = piece[128:PACK] * d
    total_ref[0:128, :] = s
    total_ref[128:PACK, :] = d


def finish_kernel(
    mech_ref, qs_ref, z1_ref, z2_ref, z3_ref, yb_ref, other_ref, gate_ref, gain_ref, out_ref
):
    s = z3_ref[0:128, :]
    s = z2_ref[128:129, :] * s + z2_ref[0:128, :]
    s = z1_ref[128:129, :] * s + z1_ref[0:128, :]
    s = yb_ref[128:129, :] * s + yb_ref[0:128, :]
    s = jnp.where(lax.axis_index(C) == 1, other_ref[128:129, :] * s + other_ref[0:128, :], s)
    head = _first_head()
    s0 = jnp.where(head, s, 0.0).astype(bf16)
    s1 = jnp.where(head, 0.0, s).astype(bf16)
    gain = gain_ref[...]
    for n in range(TOK // 128):
        rows = slice(n * 128, (n + 1) * 128)
        for h, sh in enumerate((s0, s1)):
            cols = slice(h * DV, (h + 1) * DV)
            o = mech_ref[rows, cols] + _dot(qs_ref[rows, :], sh, NT)
            o = o * lax.rsqrt(jnp.mean(o * o, axis=-1, keepdims=True) + EPS) * gain
            out_ref[rows, cols] = (o * _silu(gate_ref[rows, cols].astype(f32))).astype(bf16)


ROWS = TOK // 4


def attend_kernel(
    m0, m1, m2, m3, own_w, got1, got2, got3, sib1, sib2, sib3, x_ref, gain_ref,
    normed_ref, resid_ref, w_ref,
):
    c = lax.axis_index(C)
    mine = pl.multiple_of(c * 128, 128)
    theirs = pl.multiple_of((1 - c) * 128, 128)
    w_ref[0] = own_w[...]
    for j, (got, sib) in enumerate(((got1, sib1), (got2, sib2), (got3, sib3))):
        w_ref[j + 1, pl.ds(mine, 128), :] = got[...]
        w_ref[j + 1, pl.ds(theirs, 128), :] = sib[...]
    gain = gain_ref[...]
    xi = lax.axis_index(X)
    for n in range(4):
        rows = slice(n * ROWS, (n + 1) * ROWS)
        acc = x_ref[rows, :].astype(f32)
        for j, m in enumerate((m0, m1, m2, m3)):
            acc = acc + _dot(m[rows, :], w_ref[j])

        @pl.when(xi == n)
        def _(acc=acc):
            resid_ref[...] = acc

        scaled = acc * lax.rsqrt(jnp.mean(acc * acc, axis=-1, keepdims=True) + EPS)
        normed_ref[rows, :] = (scaled * gain).astype(bf16)


def up_kernel(x_ref, halo_ref, wg_ref, wv_ref, tg_ref, tv_ref, out_ref, g_ref):
    w = jnp.concatenate([wg_ref[...].reshape(D, 128), wv_ref[...].reshape(D, 128)], axis=1)
    g_ref[0:HALO, :] = _dot(halo_ref[...], w).astype(bf16).astype(f32)
    for n in range(3):
        at = n * 256
        g_ref[HALO + at : HALO + at + 256, :] = _dot(x_ref[at : at + 256, :], w).astype(bf16).astype(f32)
    taps = jnp.concatenate([tg_ref[...], tv_ref[...]], axis=1).astype(f32)
    for n in range(12):
        at = n * 64
        mix = taps[0:1] * g_ref[HALO - 2 + at : HALO - 2 + at + 64, :]
        mix = mix + taps[1:2] * g_ref[HALO - 1 + at : HALO - 1 + at + 64, :]
        mix = mix + taps[2:3] * g_ref[HALO + at : HALO + at + 64, :]
        out_ref[at : at + 64, :] = (_silu(mix[:, :128]) * mix[:, 128:]).astype(bf16)


def down_kernel(rels, h_ref, w_ref, *out_refs):
    xi = lax.axis_index(X)
    w = w_ref[...].reshape(512, HID)
    for rel, out_ref in zip(rels, out_refs):
        at = pl.multiple_of(lax.rem(xi + rel, 4) * ROWS, ROWS)
        out_ref[...] = _dot(h_ref[pl.ds(at, ROWS), :], w, NT).astype(out_ref.dtype)


def add_kernel(p_ref, ap_ref, m_ref, am_ref, out_p, out_m):
    out_p[...] = (p_ref[...] + ap_ref[...].astype(f32)).astype(bf16)
    out_m[...] = (m_ref[...] + am_ref[...].astype(f32)).astype(bf16)


def last_kernel(resid_ref, own_ref, l_a, l_b, r_a, r_b, out_ref):
    out = resid_ref[:, :1024] + (own_ref[:, :1024] + l_a[...].astype(f32) + r_a[...].astype(f32))
    out_ref[:, :1024] = out.astype(bf16)
    out = resid_ref[:, 1024:] + (own_ref[:, 1024:] + l_b[...].astype(f32) + r_b[...].astype(f32))
    out_ref[:, 1024:] = out.astype(bf16)


def ring(step):
    return [(i, (i + step) % 4) for i in range(4)]


def shape(*dims, dtype=bf16):
    return jax.ShapeDtypeStruct(dims, dtype)


def call(kernel, out_shape, n_in, name, cost, scratch=(), mib=40):
    out_specs = jax.tree.map(lambda _: VMEM, out_shape)
    return pl.pallas_call(
        kernel,
        out_shape=out_shape,
        in_specs=[VMEM] * n_in,
        out_specs=out_specs,
        scratch_shapes=list(scratch),
        compiler_params=_params(mib),
        cost_estimate=cost,
        name=name,
    )


def down(hidden, weights, rels, half, dtype, columns):
    first = half * 2
    blocks = columns // 512
    return pl.pallas_call(
        functools.partial(down_kernel, rels),
        grid=(blocks,),
        out_shape=[shape(ROWS, columns, dtype=dtype) for _ in rels],
        in_specs=[
            pl.BlockSpec((TOK, HID), lambda n: (0, 0)),
            pl.BlockSpec((8, 64, HID), lambda n: (n + first, 2, 0)),
        ],
        out_specs=[pl.BlockSpec((ROWS, 512), lambda n: (0, n)) for _ in rels],
        compiler_params=_params(24, ("arbitrary",)),
        cost_estimate=_cost(2 * ROWS * HID * columns * len(rels), columns * HID * 2 + TOK * HID * 2),
        name="down",
    )(hidden, weights)


def per_device(
    x, q, k, v, switch, pre, fade, head_gain, w_out, ff_gain, w_gate, w_value, t_gate, t_value, w_down
):
    c = lax.axis_index(C)
    packed = jnp.concatenate([w_gate, w_value, w_down.T], axis=0)
    weights = lax.all_gather(packed, SP, axis=0)

    cum, pack = call(
        state_kernel,
        (shape(TOK, 128, dtype=f32), shape(PACK, 128, dtype=f32)),
        4, "state", _cost(2 * TOK * 128 * 256, 1e6), [pltpu.VMEM((TOK, 128), bf16)],
    )(pre, fade.reshape(6, 128), k, v)
    other = lax.ppermute(pack, C, [(0, 1), (1, 0)])

    w_half = lax.dynamic_slice_in_dim(w_out, c * 128, 128, 0)
    w_got = [lax.ppermute(w_half, X, ring(s)) for s in (1, 3, 2)]
    w_sib = [lax.ppermute(w, C, [(0, 1), (1, 0)]) for w in w_got]

    chip = call(chip_kernel, shape(PACK, 128, dtype=f32), 2, "chip", _cost(1e5, 2e5))(pack, other)
    along_y = [lax.ppermute(chip, Y, ring(s)) for s in (3, 2, 1)]
    mech, q_shard = call(
        local_kernel, (shape(TOK, 256, dtype=f32), shape(TOK, 128)), 4, "local",
        _cost(12 * 2 * 128 * 128 * 64 * 8, 3e6),
    )(q, k, v, cum)
    plane, before = call(
        plane_kernel, (shape(PACK, 128, dtype=f32), shape(PACK, 128, dtype=f32)), 4, "plane",
        _cost(1e5, 4e5), [pltpu.VMEM((4, PACK, 128), f32)],
    )(chip, *along_y)
    along_z = [
        lax.ppermute(plane, Z, [(i, i + s) for i in range(4 - s)]) for s in (1, 2, 3)
    ]
    mixed = call(
        finish_kernel, shape(TOK, 256), 9, "finish", _cost(2 * TOK * 128 * 256, 3e6)
    )(mech, q_shard, *along_z, before, other, switch, head_gain.reshape(1, DV))

    mixed_got = [lax.ppermute(mixed, X, ring(s)) for s in (1, 3, 2)]
    normed, resid = call(
        attend_kernel, (shape(TOK, D), shape(ROWS, D, dtype=f32)), 13, "attend",
        _cost(2 * TOK * 1024 * D, 1.2e7), [pltpu.VMEM((4, 256, D), bf16)],
    )(mixed, *mixed_got, w_out, *w_got, *w_sib, x, ff_gain.reshape(1, D))
    halo = lax.ppermute(normed[TOK - HALO :], SP, [(i, i + 1) for i in range(31)])

    hidden = pl.pallas_call(
        up_kernel,
        grid=(HID // 128,),
        out_shape=shape(TOK, HID),
        in_specs=[
            pl.BlockSpec((TOK, D), lambda n: (0, 0)),
            pl.BlockSpec((HALO, D), lambda n: (0, 0)),
            pl.BlockSpec((32, 64, 128), lambda n: (0, 0, n)),
            pl.BlockSpec((32, 64, 128), lambda n: (0, 1, n)),
            pl.BlockSpec((3, 128), lambda n: (0, n)),
            pl.BlockSpec((3, 128), lambda n: (0, n)),
        ],
        out_specs=pl.BlockSpec((TOK, 128), lambda n: (0, n)),
        scratch_shapes=[pltpu.VMEM((HALO + TOK, 256), f32)],
        compiler_params=_params(40, ("arbitrary",)),
        cost_estimate=_cost(2 * TOK * D * 2 * HID, 2 * D * HID * 2 + TOK * D * 2),
        name="up",
    )(normed, halo, weights, weights, t_gate, t_value)

    part = functools.partial(down, hidden, weights)
    (opp_a,) = part((2,), 0, bf16, 1024)
    far_r = lax.ppermute(opp_a, X, ring(1))
    (opp_b,) = part((2,), 1, bf16, 1024)
    far_l = lax.ppermute(opp_b, X, ring(3))
    (next_b,) = part((1,), 1, bf16, 1024)
    near_l_b = lax.ppermute(next_b, X, ring(1))
    (prev_a,) = part((3,), 0, bf16, 1024)
    near_r_a = lax.ppermute(prev_a, X, ring(3))
    (next_a,) = part((1,), 0, f32, 1024)
    (prev_b,) = part((3,), 1, f32, 1024)
    (own,) = part((0,), 0, f32, 2048)
    send_r, send_l = call(
        add_kernel, (shape(ROWS, 1024), shape(ROWS, 1024)), 4, "add", _cost(4e5, 4e6)
    )(next_a, far_r, prev_b, far_l)
    near_l_a = lax.ppermute(send_r, X, ring(1))
    near_r_b = lax.ppermute(send_l, X, ring(3))
    return call(last_kernel, shape(ROWS, D), 6, "last", _cost(1e6, 5e6))(
        resid, own, near_l_a, near_l_b, near_r_a, near_r_b
    )


def solution(mesh):
    torus = Mesh(mesh.devices.reshape(4, 4, 2, 4), (Z, Y, C, X))
    return jax.shard_map(
        per_device,
        mesh=torus,
        in_specs=(
            P(SP, None), P(SP, X), P(SP, X), P(SP, X), P(SP, X), P(SP, X), P(SP), P(),
            P(X, None), P(), P(SP, X), P(SP, X), P(None, X), P(None, X), P(X, SP),
        ),
        out_specs=P((Z, Y, C, X), None),
        check_vma=False,
    )
```

time: 253 us -> 150 us (0.59)
  blocking collectives: 115 us -> 0 us
  Pallas kernels: 0 us -> 42 us
  matrix products: 33 us -> 0 us
  starting transfers between devices: 13.6 us -> 39.6 us
  other arithmetic: 19.1 us -> 2.06 us
  local copies, waits for them, and re-layouts: 18.1 us -> 6.57 us
  waiting for transfers between devices: 39 us -> 45.5 us
    all_to_all x3 -> x0, blocking collectives: 85.4 us -> none  [the longest x1 40.5 us: summed_on_arrival(): pieces = lax.all_to_all(split_up(array, dim, size), axis, 0, 0, tiled=True)]
    pallas_call x0 -> x16, Pallas kernels: none -> 42 us  [the longest x1 18.6 us: per_device(): pl.pallas_call(up_kernel, grid=(HID // 128,), out_shape=shape(TOK, HID),...]
    all_to_all x1 -> x0, waiting for transfers between devices: 38.2 us -> none  [copy_for_each(): lax.all_to_all(jnp.broadcast_to(array[None], (size, *array.shape)), axis,...]
    ppermute x2 -> x23, waiting for transfers between devices: 0.01 us -> 37.9 us  [the longest x3 18.6 us: per_device(): mixed_got = [lax.ppermute(mixed, X, ring(s)) for s in (1, 3, 2)]]
    dot_general x9 -> x0, matrix products: 33 us -> none  [the longest x1 8.48 us: per_device(): gate_sum = jnp.dot(normed, pieces[0], preferred_element_type=jnp.float32)]
    ppermute x2 -> x23, starting transfers between devices: 8.66 us -> 39.5 us  [the longest x3 14.7 us: per_device(): lax.ppermute(plane, Z, [(i, i + s) for i in range(4 - s)])]
    all_gather x3 -> x0, blocking collectives: 30.1 us -> none  [all_in_one(): both, at, found = (lax.all_gather(jnp.concatenate(lines), axis), 0, {})]
    dynamic_update_slice x12 -> x0, other arithmetic: 7.69 us -> none  [per_device(): lax.scan(advance_recurrence, start_state, (jnp.exp(block_total), incremen...]
  transfers between devices with their start and end apart: 6 -> 24, of which waited for: 1 -> 14; matrix products, arithmetic and copies ran while one was open for 23% -> 0% of each run, Pallas kernels for 0% -> 13%
where the time goes in v1:
time: 150 us; the launch traced here: 149 us
  waiting for transfers between devices  45.5 us (30%)
  Pallas kernels  42 us (28%)
  starting transfers between devices  39.6 us (26%)
  between operations  13.8 us (9%)
  local copies, waits for them, and re-layouts  6.57 us (4%)
  other arithmetic  2.06 us (1%)
    ppermute x3, waiting for transfers between devices, per_device(): mixed_got = [lax.ppermute(mixed, X, ring(s)) for s in (1, 3, 2)]  18.6 us
    pallas_call x1, Pallas kernels, per_device(): pl.pallas_call(up_kernel, grid=(HID // 128,), out_shape=shape(TOK, HID),...  18.6 us
    ppermute x3, starting transfers between devices, per_device(): lax.ppermute(plane, Z, [(i, i + s) for i in range(4 - s)])  14.7 us
    pallas_call x7, Pallas kernels, down(): pl.pallas_call(functools.partial(down_kernel, rels), grid=(blocks,), out_...  12.5 us
    all_gather x1, waiting for transfers between devices, per_device(): weights = lax.all_gather(packed, SP, axis=0)  7.59 us
    ppermute x1, waiting for transfers between devices, per_device(): near_l_a = lax.ppermute(send_r, X, ring(1))  7.43 us
    unnamed x38, local copies, waits for them, and re-layouts  6.53 us
    pallas_call x1, Pallas kernels, per_device(): call(attend_kernel, (shape(TOK, D), shape(ROWS, D, dtype=f32)), 13, 'atte...  5.48 us
  transfers between devices with their start and end apart: 24, of which 14 were waited for; matrix products, arithmetic and copies ran while one was open for 0% of the time, Pallas kernels for 13%

profile of v1, /device:TPU:24, one launch (start us, length us, event | category | flops | bytes accessed | tf_op | source)
XLA Modules:
  0.0 149.4 jit_solution(13145374072904252282)
XLA Ops:
  6.6 2.1 %pad_maximum_fusion = bf16[192,1408]{1,0:T(8,128)(2,1)} fusion(bf16[64,1408]{1,0:T(8,128)(2,1)} %bitcast.17, bf16[64,1408]{1,0:T(8,128)(2,1)} %param.26, bf16[64,1408]{1,0:T(8,128)(2,1)} %param.25), kind=kLoop, calls=%fused_computation | loop fusion | flops 1622016 | bytes 1081344 | tf_op jit(solution)/shard_map/concatenate | solution.py:278
  8.7 1.1 state.1
  10.0 1.2 collective-permute-done.other_ref
  11.3 0.8 collective-permute-start.1
  12.1 1.6 %collective-permute-start.10 = (bf16[128,2048]{1,0:T(8,128)(2,1)S(1)}, bf16[128,2048]{1,0:T(8,128)(2,1)S(1)}, u32[]{:S(2)}, u32[]{:S(2)}) collective-permute-start(bf16[128,2048]{1,0:T(8,128)(2,1)S(1)} %constant_dynamic-slice_fusion), channel_id=1, source_target_pairs={{0,1},{1,2},{2,3},{3,0},{4,5},{5,6},{6,7},{7,4},{8,9},{9,10},{10,1... | collective-permute-start | bytes 1572872 | tf_op jit(solution)/shard_map/ppermute | solution.py:289
  13.7 1.7 %collective-permute-start.11 = (bf16[128,2048]{1,0:T(8,128)(2,1)S(1)}, bf16[128,2048]{1,0:T(8,128)(2,1)S(1)}, u32[]{:S(2)}, u32[]{:S(2)}) collective-permute-start(bf16[128,2048]{1,0:T(8,128)(2,1)S(1)} %constant_dynamic-slice_fusion), channel_id=1, source_target_pairs={{0,3},{1,0},{2,1},{3,2},{4,7},{5,4},{6,5},{7,6},{8,11},{9,8},{10,9... | collective-permute-start | bytes 1572872 | tf_op jit(solution)/shard_map/ppermute | solution.py:289
  15.4 1.8 %collective-permute-start.12 = (bf16[128,2048]{1,0:T(8,128)(2,1)S(1)}, bf16[128,2048]{1,0:T(8,128)(2,1)S(1)}, u32[]{:S(2)}, u32[]{:S(2)}) collective-permute-start(bf16[128,2048]{1,0:T(8,128)(2,1)S(1)} %constant_dynamic-slice_fusion), channel_id=1, source_target_pairs={{0,2},{1,3},{2,0},{3,1},{4,6},{5,7},{6,4},{7,5},{8,10},{9,11},{10,... | collective-permute-start | bytes 1572872 | tf_op jit(solution)/shard_map/ppermute | solution.py:289
  17.2 0.9 collective-permute-start.2
  18.2 2.2 %collective-permute-start.3 = (f32[136,128]{1,0:T(8,128)S(1)}, f32[136,128]{1,0:T(8,128)S(1)}, u32[]{:S(2)}, u32[]{:S(2)}) collective-permute-start(f32[136,128]{1,0:T(8,128)S(1)} %chip.1.own_ref), channel_id=1, source_target_pairs={{0,8},{8,16},{16,24},{24,0},{1,9},{9,17},{17,25},{25,1},{2,10},{10... | collective-permute-start | bytes 208904 | tf_op jit(solution)/shard_map/ppermute | solution.py:293
  20.4 2.7 %collective-permute-done.2.opp_ref = f32[136,128]{1,0:T(8,128)S(1)} collective-permute-done((f32[136,128]{1,0:T(8,128)S(1)}, f32[136,128]{1,0:T(8,128)S(1)}, u32[]{:S(2)}, u32[]{:S(2)}) %collective-permute-start.2) | collective-permute-done | bytes 69664 | tf_op jit(solution)/shard_map/ppermute | solution.py:293
  23.0 0.6 collective-permute-done.3.down_ref
  23.7 4.0 %collective-permute-start.4 = (f32[136,128]{1,0:T(8,128)S(1)}, f32[136,128]{1,0:T(8,128)S(1)}, u32[]{:S(2)}, u32[]{:S(2)}) collective-permute-start(f32[136,128]{1,0:T(8,128)S(1)} %get-tuple-element.19), channel_id=1, source_target_pairs={{0,32},{32,64},{64,96},{1,33},{33,65},{65,97},{2,34},{34,66},{66,9... | collective-permute-start | bytes 208904 | tf_op jit(solution)/shard_map/ppermute | solution.py:303
  27.7 7.0 %collective-permute-start.5 = (f32[136,128]{1,0:T(8,128)S(1)}, f32[136,128]{1,0:T(8,128)S(1)}, u32[]{:S(2)}, u32[]{:S(2)}) collective-permute-start(f32[136,128]{1,0:T(8,128)S(1)} %get-tuple-element.19), channel_id=1, source_target_pairs={{0,64},{32,96},{1,65},{33,97},{2,66},{34,98},{3,67},{35,99},{4,68}... | collective-permute-start | bytes 208904 | tf_op jit(solution)/shard_map/ppermute | solution.py:303
  34.7 3.7 %collective-permute-start.6 = (f32[136,128]{1,0:T(8,128)S(1)}, f32[136,128]{1,0:T(8,128)S(1)}, u32[]{:S(2)}, u32[]{:S(2)}) collective-permute-start(f32[136,128]{1,0:T(8,128)S(1)} %get-tuple-element.19), channel_id=1, source_target_pairs={{0,96},{1,97},{2,98},{3,99},{4,100},{5,101},{6,102},{7,103},{8,104... | collective-permute-start | bytes 208904 | tf_op jit(solution)/shard_map/ppermute | solution.py:303
  38.4 1.5 local.1
  39.9 0.4 collective-permute-done.6.z3_ref
  40.3 0.7 finish.1.m0
  41.2 0.5 collective-permute-start.14
  41.8 3.1 %collective-permute-start.8 = (bf16[768,256]{1,0:T(8,128)(2,1)S(1)}, bf16[768,256]{1,0:T(8,128)(2,1)S(1)}, u32[]{:S(2)}, u32[]{:S(2)}) collective-permute-start(bf16[768,256]{1,0:T(8,128)(2,1)S(1)} %finish.1.m0), channel_id=1, source_target_pairs={{0,3},{1,0},{2,1},{3,2},{4,7},{5,4},{6,5},{7,6},{8,11},{9,8},{10,9... | collective-permute-start | bytes 1179656 | tf_op jit(solution)/shard_map/ppermute | solution.py:309
  44.9 9.4 %collective-permute-done.7.m1 = bf16[768,256]{1,0:T(8,128)(2,1)S(1)} collective-permute-done((bf16[768,256]{1,0:T(8,128)(2,1)S(1)}, bf16[768,256]{1,0:T(8,128)(2,1)S(1)}, u32[]{:S(2)}, u32[]{:S(2)}) %collective-permute-start.7) | collective-permute-done | bytes 393248 | tf_op jit(solution)/shard_map/ppermute | solution.py:309
  54.3 8.0 %collective-permute-done.8.m2 = bf16[768,256]{1,0:T(8,128)(2,1)S(1)} collective-permute-done((bf16[768,256]{1,0:T(8,128)(2,1)S(1)}, bf16[768,256]{1,0:T(8,128)(2,1)S(1)}, u32[]{:S(2)}, u32[]{:S(2)}) %collective-permute-start.8) | collective-permute-done | bytes 393248 | tf_op jit(solution)/shard_map/ppermute | solution.py:309
  62.3 1.2 collective-permute-done.9.m3
  63.6 5.5 %attend.1 = (bf16[768,2048]{1,0:T(8,128)(2,1)S(1)}, f32[192,2048]{1,0:T(8,128)S(1)}) custom-call(bf16[768,256]{1,0:T(8,128)(2,1)S(1)} %finish.1.m0, bf16[768,256]{1,0:T(8,128)(2,1)S(1)} %collective-permute-done.7.m1, bf16[768,256]{1,0:T(8,128)(2,1)S(1)} %collective-permute-done.8.m2, bf16[768,256]{1,0:T(8,128)(2,1)S(1)} %collective-permute-done.9.m3, ...), custom_call_target="tpu_custom_call" | custom-call | flops 3221225472 | bytes 12000000 | tf_op jit(solution)/shard_map/attend/pallas_call | solution.py:310
  69.1 1.2 copy-done.4
  70.3 1.6 %copy-done.1 = bf16[768,2048]{1,0:T(8,128)(2,1)} copy-done((bf16[768,2048]{1,0:T(8,128)(2,1)}, bf16[768,2048]{1,0:T(8,128)(2,1)S(1)}, u32[]{:S(2)}) %copy-start.1) | copy-done | bytes 3145752
  71.9 1.9 %collective-permute-start.16 = (bf16[16,2048]{1,0:T(8,128)(2,1)S(1)}, bf16[16,2048]{1,0:T(8,128)(2,1)S(1)}, u32[]{:S(2)}, u32[]{:S(2)}) collective-permute-start(bf16[16,2048]{1,0:T(8,128)(2,1)S(1)} %slice.3), channel_id=1, source_target_pairs={{0,4},{4,8},{8,12},{12,16},{16,20},{20,24},{24,28},{28,32},{32,36}... | collective-permute-start | bytes 196616 | tf_op jit(solution)/shard_map/ppermute | solution.py:314
  73.9 5.2 %collective-permute-done.16.halo_ref = bf16[16,2048]{1,0:T(8,128)(2,1)S(1)} collective-permute-done((bf16[16,2048]{1,0:T(8,128)(2,1)S(1)}, bf16[16,2048]{1,0:T(8,128)(2,1)S(1)}, u32[]{:S(2)}, u32[]{:S(2)}) %collective-permute-start.16) | collective-permute-done | bytes 65568 | tf_op jit(solution)/shard_map/ppermute | solution.py:314
  79.0 7.6 %all-gather.3.cloned.1.call-done = bf16[6144,1408]{1,0:T(8,128)(2,1)} async-done(((bf16[192,1408]{1,0:T(8,128)(2,1)}), bf16[6144,1408]{1,0:T(8,128)(2,1)}) %all-gather.3.cloned.1.call-update) | async-done | bytes 17301520 | tf_op jit(solution)/shard_map/all_gather | solution.py:279
  86.6 1.9 %copy-done.2 = bf16[768,2048]{1,0:T(8,128)(2,1)S(1)} copy-done((bf16[768,2048]{1,0:T(8,128)(2,1)S(1)}, bf16[768,2048]{1,0:T(8,128)(2,1)}, u32[]{:S(2)}) %copy-start.2) | copy-done | bytes 3145752
  88.5 18.6 %up.1.h_ref = bf16[768,1408]{1,0:T(8,128)(2,1)S(1)} custom-call(bf16[768,2048]{1,0:T(8,128)(2,1)S(1)} %copy-done.2, bf16[16,2048]{1,0:T(8,128)(2,1)S(1)} %collective-permute-done.16.halo_ref, bf16[32,192,1408]{2,1,0:T(8,128)(2,1)} %bitcast.5, bf16[32,192,1408]{2,1,0:T(8,128)(2,1)} %bitcast.6, bf16[3,1408]{1,0:T(4,128)(2,1)S(1)} %copy-done.13, ...), custom_call_target="tpu_custom_call" | custom-call | flops 8858370048 | bytes 14680064 | tf_op jit(solution)/shard_map/up/pallas_call | solution.py:316
  107.1 1.6 %down.9 = bf16[192,1024]{1,0:T(8,128)(2,1)S(1)} custom-call(bf16[768,1408]{1,0:T(8,128)(2,1)S(1)} %up.1.h_ref, bf16[32,192,1408]{2,1,0:T(8,128)(2,1)S(1)} %bitcast.7), custom_call_target="tpu_custom_call" | custom-call | flops 553648128 | bytes 5046272 | tf_op jit(solution)/shard_map/down/pallas_call | solution.py:259
  108.7 1.6 %down.11 = bf16[192,1024]{1,0:T(8,128)(2,1)S(1)} custom-call(bf16[768,1408]{1,0:T(8,128)(2,1)S(1)} %up.1.h_ref, bf16[32,192,1408]{2,1,0:T(8,128)(2,1)S(1)} %bitcast.8), custom_call_target="tpu_custom_call" | custom-call | flops 553648128 | bytes 5046272 | tf_op jit(solution)/shard_map/down/pallas_call | solution.py:259
  110.2 1.5 %collective-permute-start.17 = (bf16[192,1024]{1,0:T(8,128)(2,1)S(1)}, bf16[192,1024]{1,0:T(8,128)(2,1)S(1)}, u32[]{:S(2)}, u32[]{:S(2)}) collective-permute-start(bf16[192,1024]{1,0:T(8,128)(2,1)S(1)} %down.9), channel_id=1, source_target_pairs={{0,1},{1,2},{2,3},{3,0},{4,5},{5,6},{6,7},{7,4},{8,9},{9,10},{10,1... | collective-permute-start | bytes 1179656 | tf_op jit(solution)/shard_map/ppermute | solution.py:337
  111.8 1.8 %collective-permute-start.18 = (bf16[192,1024]{1,0:T(8,128)(2,1)S(1)}, bf16[192,1024]{1,0:T(8,128)(2,1)S(1)}, u32[]{:S(2)}, u32[]{:S(2)}) collective-permute-start(bf16[192,1024]{1,0:T(8,128)(2,1)S(1)} %down.11), channel_id=1, source_target_pairs={{0,3},{1,0},{2,1},{3,2},{4,7},{5,4},{6,5},{7,6},{8,11},{9,8},{10,9... | collective-permute-start | bytes 1179656 | tf_op jit(solution)/shard_map/ppermute | solution.py:339
  113.6 1.6 %down.12 = bf16[192,1024]{1,0:T(8,128)(2,1)S(1)} custom-call(bf16[768,1408]{1,0:T(8,128)(2,1)S(1)} %up.1.h_ref, bf16[32,192,1408]{2,1,0:T(8,128)(2,1)S(1)} %bitcast.9), custom_call_target="tpu_custom_call" | custom-call | flops 553648128 | bytes 5046272 | tf_op jit(solution)/shard_map/down/pallas_call | solution.py:259
  115.5 1.5 %down.13 = bf16[192,1024]{1,0:T(8,128)(2,1)S(1)} custom-call(bf16[768,1408]{1,0:T(8,128)(2,1)S(1)} %up.1.h_ref, bf16[32,192,1408]{2,1,0:T(8,128)(2,1)S(1)} %bitcast.10), custom_call_target="tpu_custom_call" | custom-call | flops 553648128 | bytes 5046272 | tf_op jit(solution)/shard_map/down/pallas_call | solution.py:259
  117.0 3.0 %collective-permute-start.21 = (bf16[192,1024]{1,0:T(8,128)(2,1)S(1)}, bf16[192,1024]{1,0:T(8,128)(2,1)S(1)}, u32[]{:S(2)}, u32[]{:S(2)}) collective-permute-start(bf16[192,1024]{1,0:T(8,128)(2,1)S(1)} %down.13), channel_id=1, source_target_pairs={{0,3},{1,0},{2,1},{3,2},{4,7},{5,4},{6,5},{7,6},{8,11},{9,8},{10,9... | collective-permute-start | bytes 1179656 | tf_op jit(solution)/shard_map/ppermute | solution.py:343
  120.0 1.6 %down.8.p_ref = f32[192,1024]{1,0:T(8,128)S(1)} custom-call(bf16[768,1408]{1,0:T(8,128)(2,1)S(1)} %up.1.h_ref, bf16[32,192,1408]{2,1,0:T(8,128)(2,1)S(1)} %bitcast.11), custom_call_target="tpu_custom_call" | custom-call | flops 553648128 | bytes 5046272 | tf_op jit(solution)/shard_map/down/pallas_call | solution.py:259
  121.6 1.6 %down.10.m_ref = f32[192,1024]{1,0:T(8,128)S(1)} custom-call(bf16[768,1408]{1,0:T(8,128)(2,1)S(1)} %up.1.h_ref, bf16[32,192,1408]{2,1,0:T(8,128)(2,1)S(1)} %bitcast.12), custom_call_target="tpu_custom_call" | custom-call | flops 553648128 | bytes 5046272 | tf_op jit(solution)/shard_map/down/pallas_call | solution.py:259
  123.8 1.0 add.5
  124.8 1.5 collective-permute-start.19
  126.2 1.8 %collective-permute-start.22 = (bf16[192,1024]{1,0:T(8,128)(2,1)}, bf16[192,1024]{1,0:T(8,128)(2,1)S(1)}, u32[]{:S(2)}, u32[]{:S(2)}) collective-permute-start(bf16[192,1024]{1,0:T(8,128)(2,1)} %get-tuple-element.24), channel_id=1, source_target_pairs={{0,3},{1,0},{2,1},{3,2},{4,7},{5,4},{6,5},{7,6},{8,11},{9,8},{10,9... | collective-permute-start | bytes 1179656 | tf_op jit(solution)/shard_map/ppermute | solution.py:351
  128.0 3.1 %down.7.own_ref = f32[192,2048]{1,0:T(8,128)S(1)} custom-call(bf16[768,1408]{1,0:T(8,128)(2,1)S(1)} %up.1.h_ref, bf16[32,192,1408]{2,1,0:T(8,128)(2,1)S(1)} %bitcast.13), custom_call_target="tpu_custom_call" | custom-call | flops 1107296256 | bytes 7929856 | tf_op jit(solution)/shard_map/down/pallas_call | solution.py:259
  131.1 0.8 collective-permute-done.20.l_b
  132.2 7.4 %collective-permute-done.19.l_a = bf16[192,1024]{1,0:T(8,128)(2,1)S(1)} collective-permute-done((bf16[192,1024]{1,0:T(8,128)(2,1)}, bf16[192,1024]{1,0:T(8,128)(2,1)S(1)}, u32[]{:S(2)}, u32[]{:S(2)}) %collective-permute-start.19) | collective-permute-done | bytes 393248 | tf_op jit(solution)/shard_map/ppermute | solution.py:350
  139.7 0.7 copy-done.8
  140.4 1.0 copy-done.9
  141.4 1.2 last.1
  (58 shorter events, 1.8 us)
Async XLA Ops:
  6.5 2.2 %copy-start.15 = (f32[768]{0:T(1024)S(1)}, f32[768]{0:T(1024)}, u32[]{:S(2)}) copy-start(f32[768]{0:T(1024)} %param.21) | copy-start | bytes 9220
  6.5 2.2 %copy-start.6 = (bf16[768,128]{1,0:T(8,128)(2,1)S(1)}, bf16[768,128]{1,0:T(8,128)(2,1)}, u32[]{:S(2)}) copy-start(bf16[768,128]{1,0:T(8,128)(2,1)} %k_ref.3) | copy-start | bytes 589828
  6.5 2.2 %copy-start.3 = (bf16[768,256]{1,0:T(8,128)(2,1)S(1)}, bf16[768,256]{1,0:T(8,128)(2,1)}, u32[]{:S(2)}) copy-start(bf16[768,256]{1,0:T(8,128)(2,1)} %v_ref.3) | copy-start | bytes 1179652
  6.5 2.2 %copy-start.12 = (bf16[768,128]{1,0:T(8,128)(2,1)S(1)}, bf16[768,128]{1,0:T(8,128)(2,1)}, u32[]{:S(2)}) copy-start(bf16[768,128]{1,0:T(8,128)(2,1)} %pre_ref.1) | copy-start | bytes 589828
  6.5 5.5 %copy-start.10 = (bf16[256,2048]{1,0:T(8,128)(2,1)S(1)}, bf16[256,2048]{1,0:T(8,128)(2,1)}, u32[]{:S(2)}) copy-start(bf16[256,2048]{1,0:T(8,128)(2,1)} %own_w.1) | copy-start | bytes 3145732
  6.5 80.1 %all-gather.3.cloned.1.call-start = ((), (), s32[]{:S(2)}) async-start(), calls=%async_computation | async-start | bytes 17842176 | tf_op jit(solution)/shard_map/all_gather | solution.py:279
  8.7 29.7 %copy-start.11 = (bf16[768,128]{1,0:T(8,128)(2,1)S(1)}, bf16[768,128]{1,0:T(8,128)(2,1)}, u32[]{:S(2)}) copy-start(bf16[768,128]{1,0:T(8,128)(2,1)} %q_ref.1) | copy-start | bytes 589828
  8.7 31.6 %copy-start.7 = (bf16[768,256]{1,0:T(8,128)(2,1)S(1)}, bf16[768,256]{1,0:T(8,128)(2,1)}, u32[]{:S(2)}) copy-start(bf16[768,256]{1,0:T(8,128)(2,1)} %gate_ref.1) | copy-start | bytes 1179652
  8.7 31.6 %copy-start.16 = (f32[128]{0:T(128)S(1)}, f32[128]{0:T(128)}, u32[]{:S(2)}) copy-start(f32[128]{0:T(128)} %param.22) | copy-start | bytes 1540
  9.9 1.3 collective-permute-start
  11.3 6.9 %collective-permute-start.1 = (f32[136,128]{1,0:T(8,128)S(1)}, f32[136,128]{1,0:T(8,128)S(1)}, u32[]{:S(2)}, u32[]{:S(2)}) collective-permute-start(f32[136,128]{1,0:T(8,128)S(1)} %chip.1.own_ref), channel_id=1, source_target_pairs={{0,24},{8,0},{16,8},{24,16},{1,25},{9,1},{17,9},{25,17},{2,26},{10... | collective-permute-start | bytes 208904 | tf_op jit(solution)/shard_map/ppermute | solution.py:293
  12.1 29.0 %collective-permute-start.10 = (bf16[128,2048]{1,0:T(8,128)(2,1)S(1)}, bf16[128,2048]{1,0:T(8,128)(2,1)S(1)}, u32[]{:S(2)}, u32[]{:S(2)}) collective-permute-start(bf16[128,2048]{1,0:T(8,128)(2,1)S(1)} %constant_dynamic-slice_fusion), channel_id=1, source_target_pairs={{0,1},{1,2},{2,3},{3,0},{4,5},{5,6},{6,7},{7,4},{8,9},{9,10},{10,1... | collective-permute-start | bytes 1572872 | tf_op jit(solution)/shard_map/ppermute | solution.py:289
  13.7 27.5 %collective-permute-start.11 = (bf16[128,2048]{1,0:T(8,128)(2,1)S(1)}, bf16[128,2048]{1,0:T(8,128)(2,1)S(1)}, u32[]{:S(2)}, u32[]{:S(2)}) collective-permute-start(bf16[128,2048]{1,0:T(8,128)(2,1)S(1)} %constant_dynamic-slice_fusion), channel_id=1, source_target_pairs={{0,3},{1,0},{2,1},{3,2},{4,7},{5,4},{6,5},{7,6},{8,11},{9,8},{10,9... | collective-permute-start | bytes 1572872 | tf_op jit(solution)/shard_map/ppermute | solution.py:289
  15.4 26.3 %collective-permute-start.12 = (bf16[128,2048]{1,0:T(8,128)(2,1)S(1)}, bf16[128,2048]{1,0:T(8,128)(2,1)S(1)}, u32[]{:S(2)}, u32[]{:S(2)}) collective-permute-start(bf16[128,2048]{1,0:T(8,128)(2,1)S(1)} %constant_dynamic-slice_fusion), channel_id=1, source_target_pairs={{0,2},{1,3},{2,0},{3,1},{4,6},{5,7},{6,4},{7,5},{8,10},{9,11},{10,... | collective-permute-start | bytes 1572872 | tf_op jit(solution)/shard_map/ppermute | solution.py:289
  17.2 5.8 %collective-permute-start.2 = (f32[136,128]{1,0:T(8,128)S(1)}, f32[136,128]{1,0:T(8,128)S(1)}, u32[]{:S(2)}, u32[]{:S(2)}) collective-permute-start(f32[136,128]{1,0:T(8,128)S(1)} %chip.1.own_ref), channel_id=1, source_target_pairs={{0,16},{8,24},{16,0},{24,8},{1,17},{9,25},{17,1},{25,9},{2,18},{10... | collective-permute-start | bytes 208904 | tf_op jit(solution)/shard_map/ppermute | solution.py:293
  18.2 5.4 %collective-permute-start.3 = (f32[136,128]{1,0:T(8,128)S(1)}, f32[136,128]{1,0:T(8,128)S(1)}, u32[]{:S(2)}, u32[]{:S(2)}) collective-permute-start(f32[136,128]{1,0:T(8,128)S(1)} %chip.1.own_ref), channel_id=1, source_target_pairs={{0,8},{8,16},{16,24},{24,0},{1,9},{9,17},{17,25},{25,1},{2,10},{10... | collective-permute-start | bytes 208904 | tf_op jit(solution)/shard_map/ppermute | solution.py:293
  23.7 11.0 %collective-permute-start.4 = (f32[136,128]{1,0:T(8,128)S(1)}, f32[136,128]{1,0:T(8,128)S(1)}, u32[]{:S(2)}, u32[]{:S(2)}) collective-permute-start(f32[136,128]{1,0:T(8,128)S(1)} %get-tuple-element.19), channel_id=1, source_target_pairs={{0,32},{32,64},{64,96},{1,33},{33,65},{65,97},{2,34},{34,66},{66,9... | collective-permute-start | bytes 208904 | tf_op jit(solution)/shard_map/ppermute | solution.py:303
  27.7 12.2 %collective-permute-start.5 = (f32[136,128]{1,0:T(8,128)S(1)}, f32[136,128]{1,0:T(8,128)S(1)}, u32[]{:S(2)}, u32[]{:S(2)}) collective-permute-start(f32[136,128]{1,0:T(8,128)S(1)} %get-tuple-element.19), channel_id=1, source_target_pairs={{0,64},{32,96},{1,65},{33,97},{2,66},{34,98},{3,67},{35,99},{4,68}... | collective-permute-start | bytes 208904 | tf_op jit(solution)/shard_map/ppermute | solution.py:303
  34.7 5.6 %collective-permute-start.6 = (f32[136,128]{1,0:T(8,128)S(1)}, f32[136,128]{1,0:T(8,128)S(1)}, u32[]{:S(2)}, u32[]{:S(2)}) collective-permute-start(f32[136,128]{1,0:T(8,128)S(1)} %get-tuple-element.19), channel_id=1, source_target_pairs={{0,96},{1,97},{2,98},{3,99},{4,100},{5,101},{6,102},{7,103},{8,104... | collective-permute-start | bytes 208904 | tf_op jit(solution)/shard_map/ppermute | solution.py:303
  38.4 25.2 %copy-start.17 = (bf16[768,2048]{1,0:T(8,128)(2,1)S(1)}, bf16[768,2048]{1,0:T(8,128)(2,1)}, u32[]{:S(2)}) copy-start(bf16[768,2048]{1,0:T(8,128)(2,1)} %x_ref.1) | copy-start | bytes 9437188
  38.4 25.2 %copy-start.18 = (f32[2048]{0:T(1024)S(1)}, f32[2048]{0:T(1024)}, u32[]{:S(2)}) copy-start(f32[2048]{0:T(1024)} %param.24) | copy-start | bytes 24580
  41.0 13.3 %collective-permute-start.7 = (bf16[768,256]{1,0:T(8,128)(2,1)S(1)}, bf16[768,256]{1,0:T(8,128)(2,1)S(1)}, u32[]{:S(2)}, u32[]{:S(2)}) collective-permute-start(bf16[768,256]{1,0:T(8,128)(2,1)S(1)} %finish.1.m0), channel_id=1, source_target_pairs={{0,1},{1,2},{2,3},{3,0},{4,5},{5,6},{6,7},{7,4},{8,9},{9,10},{10,1... | collective-permute-start | bytes 1179656 | tf_op jit(solution)/shard_map/ppermute | solution.py:309
  41.1 22.5 %collective-permute-start.13 = (bf16[128,2048]{1,0:T(8,128)(2,1)S(1)}, bf16[128,2048]{1,0:T(8,128)(2,1)S(1)}, u32[]{:S(2)}, u32[]{:S(2)}) collective-permute-start(bf16[128,2048]{1,0:T(8,128)(2,1)S(1)} %collective-permute-done.10.got1), channel_id=1, source_target_pairs={{0,4},{4,0},{1,5},{5,1},{2,6},{6,2},{3,7},{7,3},{8,12},{12,8},{9,1... | collective-permute-start | bytes 1572872 | tf_op jit(solution)/shard_map/ppermute | solution.py:290
  41.2 22.4 %collective-permute-start.14 = (bf16[128,2048]{1,0:T(8,128)(2,1)S(1)}, bf16[128,2048]{1,0:T(8,128)(2,1)S(1)}, u32[]{:S(2)}, u32[]{:S(2)}) collective-permute-start(bf16[128,2048]{1,0:T(8,128)(2,1)S(1)} %collective-permute-done.11.got2), channel_id=1, source_target_pairs={{0,4},{4,0},{1,5},{5,1},{2,6},{6,2},{3,7},{7,3},{8,12},{12,8},{9,1... | collective-permute-start | bytes 1572872 | tf_op jit(solution)/shard_map/ppermute | solution.py:290
  41.7 21.9 %collective-permute-start.15 = (bf16[128,2048]{1,0:T(8,128)(2,1)S(1)}, bf16[128,2048]{1,0:T(8,128)(2,1)S(1)}, u32[]{:S(2)}, u32[]{:S(2)}) collective-permute-start(bf16[128,2048]{1,0:T(8,128)(2,1)S(1)} %collective-permute-done.12.got3), channel_id=1, source_target_pairs={{0,4},{4,0},{1,5},{5,1},{2,6},{6,2},{3,7},{7,3},{8,12},{12,8},{9,1... | collective-permute-start | bytes 1572872 | tf_op jit(solution)/shard_map/ppermute | solution.py:290
  41.8 20.5 %collective-permute-start.8 = (bf16[768,256]{1,0:T(8,128)(2,1)S(1)}, bf16[768,256]{1,0:T(8,128)(2,1)S(1)}, u32[]{:S(2)}, u32[]{:S(2)}) collective-permute-start(bf16[768,256]{1,0:T(8,128)(2,1)S(1)} %finish.1.m0), channel_id=1, source_target_pairs={{0,3},{1,0},{2,1},{3,2},{4,7},{5,4},{6,5},{7,6},{8,11},{9,8},{10,9... | collective-permute-start | bytes 1179656 | tf_op jit(solution)/shard_map/ppermute | solution.py:309
  54.3 9.3 %collective-permute-start.9 = (bf16[768,256]{1,0:T(8,128)(2,1)S(1)}, bf16[768,256]{1,0:T(8,128)(2,1)S(1)}, u32[]{:S(2)}, u32[]{:S(2)}) collective-permute-start(bf16[768,256]{1,0:T(8,128)(2,1)S(1)} %finish.1.m0), channel_id=1, source_target_pairs={{0,2},{1,3},{2,0},{3,1},{4,6},{5,7},{6,4},{7,5},{8,10},{9,11},{10,... | collective-permute-start | bytes 1179656 | tf_op jit(solution)/shard_map/ppermute | solution.py:309
  63.6 23.1 %copy-start.13 = (bf16[3,1408]{1,0:T(4,128)(2,1)S(1)}, bf16[3,1408]{1,0:T(4,128)(2,1)}, u32[]{:S(2)}) copy-start(bf16[3,1408]{1,0:T(4,128)(2,1)} %tg_ref.1) | copy-start | bytes 25348
  63.6 23.1 %copy-start.14 = (bf16[3,1408]{1,0:T(4,128)(2,1)S(1)}, bf16[3,1408]{1,0:T(4,128)(2,1)}, u32[]{:S(2)}) copy-start(bf16[3,1408]{1,0:T(4,128)(2,1)} %tv_ref.1) | copy-start | bytes 25348
  69.1 1.2 copy-start.4
  70.3 1.6 %copy-start.1 = (bf16[768,2048]{1,0:T(8,128)(2,1)}, bf16[768,2048]{1,0:T(8,128)(2,1)S(1)}, u32[]{:S(2)}) copy-start(bf16[768,2048]{1,0:T(8,128)(2,1)S(1)} %get-tuple-element.22.x_ref) | copy-start | bytes 9437188
  71.9 7.1 %collective-permute-start.16 = (bf16[16,2048]{1,0:T(8,128)(2,1)S(1)}, bf16[16,2048]{1,0:T(8,128)(2,1)S(1)}, u32[]{:S(2)}, u32[]{:S(2)}) collective-permute-start(bf16[16,2048]{1,0:T(8,128)(2,1)S(1)} %slice.3), channel_id=1, source_target_pairs={{0,4},{4,8},{8,12},{12,16},{16,20},{20,24},{24,28},{28,32},{32,36}... | collective-permute-start | bytes 196616 | tf_op jit(solution)/shard_map/ppermute | solution.py:314
  86.6 1.9 %copy-start.2 = (bf16[768,2048]{1,0:T(8,128)(2,1)S(1)}, bf16[768,2048]{1,0:T(8,128)(2,1)}, u32[]{:S(2)}) copy-start(bf16[768,2048]{1,0:T(8,128)(2,1)} %copy-done.1) | copy-start | bytes 9437188
  88.5 18.6 %copy-start = (bf16[6144,1408]{1,0:T(8,128)(2,1)S(1)}, bf16[6144,1408]{1,0:T(8,128)(2,1)}, u32[]{:S(2)}) copy-start(bf16[6144,1408]{1,0:T(8,128)(2,1)} %all-gather.3.cloned.1.call-done) | copy-start | bytes 51904516
  110.2 13.3 %collective-permute-start.17 = (bf16[192,1024]{1,0:T(8,128)(2,1)S(1)}, bf16[192,1024]{1,0:T(8,128)(2,1)S(1)}, u32[]{:S(2)}, u32[]{:S(2)}) collective-permute-start(bf16[192,1024]{1,0:T(8,128)(2,1)S(1)} %down.9), channel_id=1, source_target_pairs={{0,1},{1,2},{2,3},{3,0},{4,5},{5,6},{6,7},{7,4},{8,9},{9,10},{10,1... | collective-permute-start | bytes 1179656 | tf_op jit(solution)/shard_map/ppermute | solution.py:337
  111.8 12.0 %collective-permute-start.18 = (bf16[192,1024]{1,0:T(8,128)(2,1)S(1)}, bf16[192,1024]{1,0:T(8,128)(2,1)S(1)}, u32[]{:S(2)}, u32[]{:S(2)}) collective-permute-start(bf16[192,1024]{1,0:T(8,128)(2,1)S(1)} %down.11), channel_id=1, source_target_pairs={{0,3},{1,0},{2,1},{3,2},{4,7},{5,4},{6,5},{7,6},{8,11},{9,8},{10,9... | collective-permute-start | bytes 1179656 | tf_op jit(solution)/shard_map/ppermute | solution.py:339
  115.1 16.8 %collective-permute-start.20 = (bf16[192,1024]{1,0:T(8,128)(2,1)S(1)}, bf16[192,1024]{1,0:T(8,128)(2,1)S(1)}, u32[]{:S(2)}, u32[]{:S(2)}) collective-permute-start(bf16[192,1024]{1,0:T(8,128)(2,1)S(1)} %down.12), channel_id=1, source_target_pairs={{0,1},{1,2},{2,3},{3,0},{4,5},{5,6},{6,7},{7,4},{8,9},{9,10},{10,1... | collective-permute-start | bytes 1179656 | tf_op jit(solution)/shard_map/ppermute | solution.py:341
  117.0 15.2 %collective-permute-start.21 = (bf16[192,1024]{1,0:T(8,128)(2,1)S(1)}, bf16[192,1024]{1,0:T(8,128)(2,1)S(1)}, u32[]{:S(2)}, u32[]{:S(2)}) collective-permute-start(bf16[192,1024]{1,0:T(8,128)(2,1)S(1)} %down.13), channel_id=1, source_target_pairs={{0,3},{1,0},{2,1},{3,2},{4,7},{5,4},{6,5},{7,6},{8,11},{9,8},{10,9... | collective-permute-start | bytes 1179656 | tf_op jit(solution)/shard_map/ppermute | solution.py:343
  124.8 14.9 %collective-permute-start.19 = (bf16[192,1024]{1,0:T(8,128)(2,1)}, bf16[192,1024]{1,0:T(8,128)(2,1)S(1)}, u32[]{:S(2)}, u32[]{:S(2)}) collective-permute-start(bf16[192,1024]{1,0:T(8,128)(2,1)} %get-tuple-element.23), channel_id=1, source_target_pairs={{0,1},{1,2},{2,3},{3,0},{4,5},{5,6},{6,7},{7,4},{8,9},{9,10},{10,1... | collective-permute-start | bytes 1179656 | tf_op jit(solution)/shard_map/ppermute | solution.py:350
  126.2 14.2 %copy-start.5 = (f32[192,2048]{1,0:T(8,128)S(1)}, f32[192,2048]{1,0:T(8,128)}, u32[]{:S(2)}) copy-start(f32[192,2048]{1,0:T(8,128)} %copy-done.4) | copy-start | bytes 4718596
  126.2 13.4 %collective-permute-start.22 = (bf16[192,1024]{1,0:T(8,128)(2,1)}, bf16[192,1024]{1,0:T(8,128)(2,1)S(1)}, u32[]{:S(2)}, u32[]{:S(2)}) collective-permute-start(bf16[192,1024]{1,0:T(8,128)(2,1)} %get-tuple-element.24), channel_id=1, source_target_pairs={{0,3},{1,0},{2,1},{3,2},{4,7},{5,4},{6,5},{7,6},{8,11},{9,8},{10,9... | collective-permute-start | bytes 1179656 | tf_op jit(solution)/shard_map/ppermute | solution.py:351
  139.7 0.7 copy-start.8
  140.4 1.0 copy-start.9
Sparse Core Ops, SparseCore 0:
  9.6 76.9 all-gather.2

commit v2 on v1

v2 whole, which is shorter than its diff:
```python
import functools
import jax
import jax.numpy as jnp
from jax import lax
from jax.experimental import pallas as pl
from jax.experimental.pallas import tpu as pltpu
from jax.sharding import Mesh
from jax.sharding import PartitionSpec as P


DK = 64
DV = 128
BLOCK = 64
TOK = 768
D = 2048
HID = 1408
HALO = 16
Z, Y, C, X = "z", "y", "c", "x"
SP = (Z, Y, C)
EPS = 1e-06
f32 = jnp.float32
bf16 = jnp.bfloat16
NT = (((1,), (1,)), ((), ()))
TN = (((0,), (0,)), ((), ()))
PACK = 136
VMEM = pl.BlockSpec(memory_space=pltpu.VMEM)


def _params(mib=40, sem=None):
    return pltpu.CompilerParams(vmem_limit_bytes=mib * 1024 * 1024, dimension_semantics=sem)


def _cost(flops, nbytes, trans=0):
    return pl.CostEstimate(flops=int(flops), bytes_accessed=int(nbytes), transcendentals=int(trans))


def _dot(a, b, dims=None):
    if dims is None:
        dims = (((1,), (0,)), ((), ()))
    return lax.dot_general(a, b, dims, preferred_element_type=f32)


def _log_sigmoid(x):
    return jnp.minimum(x, 0.0) - jnp.log1p(jnp.exp(-jnp.abs(x)))


def _silu(x):
    return x / (1.0 + jnp.exp(-x))


def _first_head():
    return lax.broadcasted_iota(jnp.int32, (1, 2 * DK), 1) < DK


def state_kernel(
    pre_hbm, fade_hbm, k_hbm, v_hbm, cum_ref, pack_ref, kf_ref, pre_ref, fade_ref, k_ref, v_ref, sems
):
    pairs = ((pre_hbm, pre_ref), (fade_hbm, fade_ref), (k_hbm, k_ref), (v_hbm, v_ref))
    copies = [pltpu.make_async_copy(*pair, sems.at[n]) for n, pair in enumerate(pairs)]
    for copy in copies:
        copy.start()
    for copy in copies:
        copy.wait()
    row = lax.broadcasted_iota(jnp.int32, (128, 128), 0)
    col = lax.broadcasted_iota(jnp.int32, (128, 128), 1)
    lower = ((row >= col) & ((row < BLOCK) == (col < BLOCK))).astype(f32)
    ones = jnp.ones((128, 128), f32)
    high = lax.Precision.HIGHEST
    cums = []
    for n in range(TOK // 128):
        rows = slice(n * 128, (n + 1) * 128)
        rate = _log_sigmoid(pre_ref[rows, :].astype(f32)) * (1.0 / 16.0)
        cum = jnp.dot(lower, rate, precision=high, preferred_element_type=f32)
        cum = cum + jnp.dot(
            lower * fade_ref[n : n + 1, :], ones, precision=high, preferred_element_type=f32
        )
        cum_ref[rows, :] = cum
        cums.append(cum)
    suffix = jnp.zeros((1, 2 * DK), f32)
    for b in reversed(range(TOK // BLOCK)):
        n, half = divmod(b, 2)
        cum = cums[n][half * BLOCK : (half + 1) * BLOCK]
        total = cum[BLOCK - 1 : BLOCK]
        rows = slice(b * BLOCK, (b + 1) * BLOCK)
        kf_ref[rows, :] = (k_ref[rows, :].astype(f32) * jnp.exp(suffix + total - cum)).astype(bf16)
        suffix = suffix + total
    kf = kf_ref[...]
    first = _dot(v_ref[:, :DV], kf, TN)
    second = _dot(v_ref[:, DV:], kf, TN)
    pack_ref[0:128, :] = jnp.where(_first_head(), first, second)
    pack_ref[128:PACK, :] = jnp.broadcast_to(jnp.exp(suffix), (8, 128))


def local_kernel(q_ref, k_ref, v_ref, cum_ref, mech_ref, qs_ref):
    head = _first_head()
    row = lax.broadcasted_iota(jnp.int32, (128, BLOCK), 0)
    col = lax.broadcasted_iota(jnp.int32, (128, BLOCK), 1)
    lower = jnp.where(row < BLOCK, row, row - BLOCK) >= col
    state = jnp.zeros((DV, 2 * DK), f32)
    before = jnp.zeros((1, 2 * DK), f32)
    for b in range(TOK // BLOCK):
        rows = slice(b * BLOCK, (b + 1) * BLOCK)
        cum = cum_ref[rows, :]
        total = cum[BLOCK - 1 : BLOCK]
        q = q_ref[rows, :].astype(f32) * DK**-0.5
        k = k_ref[rows, :].astype(f32)
        qd = q * jnp.exp(cum)
        qs_ref[rows, :] = (q * jnp.exp(cum + before)).astype(bf16)
        both = jnp.concatenate([jnp.where(head, qd, 0.0), jnp.where(head, 0.0, qd)], 0).astype(bf16)
        grown = (k * jnp.exp(-cum)).astype(bf16)
        faded = (k * jnp.exp(total - cum)).astype(bf16)
        scores = _dot(both, grown, NT)
        scores = jnp.where(lower, scores, 0.0).astype(bf16)
        inter = _dot(both, state.astype(bf16), NT)
        v0, v1 = v_ref[rows, :DV], v_ref[rows, DV:]
        mech_ref[rows, :DV] = _dot(scores[:BLOCK], v0) + inter[:BLOCK]
        mech_ref[rows, DV:] = _dot(scores[BLOCK:], v1) + inter[BLOCK:]
        update = jnp.where(head, _dot(v0, faded, TN), _dot(v1, faded, TN))
        state = state * jnp.exp(total) + update
        before = before + total


def chip_kernel(own_ref, other_ref, chip_ref):
    second = lax.axis_index(C) == 1
    own_s, own_d = own_ref[0:128, :], own_ref[128:PACK, :]
    oth_s, oth_d = other_ref[0:128, :], other_ref[128:PACK, :]
    s = jnp.where(second, own_d[0:1] * oth_s + own_s, oth_d[0:1] * own_s + oth_s)
    chip_ref[0:128, :] = s
    chip_ref[128:PACK, :] = own_d * oth_d


def plane_kernel(own_ref, up_ref, opp_ref, down_ref, total_ref, before_ref, held):
    y = lax.axis_index(Y)
    held[0] = own_ref[...]
    held[1] = up_ref[...]
    held[2] = opp_ref[...]
    held[3] = down_ref[...]
    s = jnp.zeros((128, 128), f32)
    d = jnp.ones((8, 128), f32)
    before_ref[0:128, :] = s
    before_ref[128:PACK, :] = d
    for k in range(4):
        if k > 0:

            @pl.when(y == k)
            def _(s=s, d=d):
                before_ref[0:128, :] = s
                before_ref[128:PACK, :] = d

        piece = held[lax.rem(k - y + 4, 4)]
        s = piece[128:129] * s + piece[0:128]
        d = piece[128:PACK] * d
    total_ref[0:128, :] = s
    total_ref[128:PACK, :] = d


def enter_kernel(z1_ref, z2_ref, z3_ref, yb_ref, out_ref):
    s = z3_ref[0:128, :]
    s = z2_ref[128:129, :] * s + z2_ref[0:128, :]
    s = z1_ref[128:129, :] * s + z1_ref[0:128, :]
    out_ref[...] = yb_ref[128:129, :] * s + yb_ref[0:128, :]


def finish_kernel(mech_ref, qs_ref, mine_ref, given_ref, other_ref, gate_ref, gain_ref, out_ref):
    given = given_ref[...]
    s = jnp.where(
        lax.axis_index(C) == 1, other_ref[128:129, :] * given + other_ref[0:128, :], mine_ref[...]
    )
    head = _first_head()
    s0 = jnp.where(head, s, 0.0).astype(bf16)
    s1 = jnp.where(head, 0.0, s).astype(bf16)
    gain = gain_ref[...]
    for n in range(TOK // 128):
        rows = slice(n * 128, (n + 1) * 128)
        for h, sh in enumerate((s0, s1)):
            cols = slice(h * DV, (h + 1) * DV)
            o = mech_ref[rows, cols] + _dot(qs_ref[rows, :], sh, NT)
            o = o * lax.rsqrt(jnp.mean(o * o, axis=-1, keepdims=True) + EPS) * gain
            out_ref[rows, cols] = (o * _silu(gate_ref[rows, cols].astype(f32))).astype(bf16)


OFFSETS = (0, 3, 1, 2)
SLOTS = tuple((j, i) for j in range(4) for i in range(4))


def chip_of(core, j, i):
    dz, dy = (i, j) if core == 0 else (j, i)
    z = lax.rem(lax.axis_index(Z) + OFFSETS[dz], 4)
    y = lax.rem(lax.axis_index(Y) + OFFSETS[dy], 4)
    return z * 4 + y


def chip_columns(chip):
    return pl.ds(pl.multiple_of(chip * 128, 128), 128)


def left_half():
    return lax.broadcasted_iota(jnp.int32, (1, 128), 1) < 64


def reorder(src_ref, dst_ref, rows):
    c = lax.axis_index(C)
    left = left_half()
    for core in range(2):
        base = jnp.where(c == core, 0, 1024)
        for t in range(8):
            one = src_ref[:, chip_columns(chip_of(core, *SLOTS[2 * t]))]
            two = src_ref[:, chip_columns(chip_of(core, *SLOTS[2 * t + 1]))]
            if core == 0:
                both = jnp.where(left, one, pltpu.roll(two, 64, 1))
            else:
                both = jnp.where(left, pltpu.roll(one, 64, 1), two)
            at = pl.ds(pl.multiple_of(base + t * 128, 128), 128)
            dst_ref[rows, at] = both.astype(bf16)


ROWS = TOK // 4


def attend_kernel(
    m0, m1, m2, m3, own_w, got1, got2, got3, sib1, sib2, sib3, x_ref, gain_ref,
    *refs,
):
    normed_ref, tail_ref, resid_ref, w_ref, n_ref = refs
    c = lax.axis_index(C)
    mine = pl.multiple_of(c * 128, 128)
    theirs = pl.multiple_of((1 - c) * 128, 128)
    w_ref[0] = own_w[...]
    for j, (got, sib) in enumerate(((got1, sib1), (got2, sib2), (got3, sib3))):
        w_ref[j + 1, pl.ds(mine, 128), :] = got[...]
        w_ref[j + 1, pl.ds(theirs, 128), :] = sib[...]
    gain = gain_ref[...]
    xi = lax.axis_index(X)
    w = w_ref[...].reshape(1024, D)

    def block(n, _):
        rows = pl.ds(pl.multiple_of(n * ROWS, ROWS), ROWS)
        mixed = jnp.concatenate([m[rows, :] for m in (m0, m1, m2, m3)], axis=1)
        acc = x_ref[rows, :].astype(f32) + _dot(mixed, w)

        @pl.when(xi == n)
        def _():
            resid_ref[...] = acc

        scaled = acc * lax.rsqrt(jnp.mean(acc * acc, axis=-1, keepdims=True) + EPS)
        n_ref[...] = scaled * gain

        @pl.when(n == 3)
        def _():
            tail_ref[...] = n_ref[ROWS - HALO :, :].astype(bf16)

        reorder(n_ref, normed_ref, rows)
        return 0

    lax.fori_loop(0, 4, block, 0)


SEG = HALO + ROWS
CHUNKS = tuple((a, min(256, HID - a)) for a in range(0, HID, 256))


def feed_kernel(rels, plan, x_ref, halo_ref, tg_ref, tv_ref, *refs):
    own, sib, refs = refs[:5], refs[5:10], refs[10:]
    out_refs, refs = refs[: len(plan)], refs[len(plan) :]
    xs_ref, hf_ref, hs_ref, g_ref, h_ref = refs
    hf_ref[...] = halo_ref[...].astype(f32)
    reorder(hf_ref, hs_ref, slice(None))
    xi = lax.axis_index(X)
    for s, rel in enumerate(rels):
        block = lax.rem(xi + rel, 4)
        at = pl.multiple_of(block * ROWS, ROWS)
        ahead = pl.multiple_of(jnp.maximum(at - HALO, 0), HALO)
        xs_ref[s * SEG : s * SEG + HALO, :] = jnp.where(
            block == 0, hs_ref[...], x_ref[pl.ds(ahead, HALO), :]
        )
        xs_ref[s * SEG + HALO : (s + 1) * SEG, :] = x_ref[pl.ds(at, ROWS), :]

    def blocks(arrays, part, cols):
        return [w[:, part, :, cols].reshape(w.shape[0] * 64, cols.stop - cols.start) for w in arrays]

    def project(n):
        a, wide = CHUNKS[n]
        for part in range(2):
            cols = slice(a, a + wide)
            w = jnp.concatenate(blocks(own, part, cols) + blocks(sib, part, cols), axis=0)
            new = _dot(xs_ref[...], w).astype(bf16).astype(f32)
            g_ref[n % 2, :, part * 256 : part * 256 + wide] = new

    def mix_columns(n):
        a, wide = CHUNKS[n]
        cols = slice(a, a + wide)
        for s in range(len(rels)):
            r = s * SEG + HALO
            mixes = []
            for part, t_ref in enumerate((tg_ref, tv_ref)):
                taps = t_ref[:, cols].astype(f32)
                at = slice(part * 256, part * 256 + wide)
                mix = taps[0:1] * g_ref[n % 2, r - 2 : r - 2 + ROWS, at]
                mix = mix + taps[1:2] * g_ref[n % 2, r - 1 : r - 1 + ROWS, at]
                mixes.append(mix + taps[2:3] * g_ref[n % 2, r : r + ROWS, at])
            h_ref[s * ROWS : (s + 1) * ROWS, cols] = (_silu(mixes[0]) * mixes[1]).astype(bf16)

    for n in range(len(CHUNKS)):
        project(n)
        if n > 0:
            mix_columns(n - 1)
    mix_columns(len(CHUNKS) - 1)
    for half, arrays in enumerate((own, sib)):
        rows = blocks(arrays, 2, slice(0, HID))
        for n, w in enumerate((rows[:2], rows[2:])):
            new = _dot(h_ref[...], jnp.concatenate(w, axis=0), NT)
            cols = slice(n * 512, n * 512 + 512)
            for (block, want), out_ref in zip(plan, out_refs):
                if want == half:
                    out_ref[:, cols] = new[block * ROWS : (block + 1) * ROWS].astype(out_ref.dtype)


def add_kernel(p_ref, ap_ref, m_ref, am_ref, out_p, out_m):
    out_p[...] = (p_ref[...] + ap_ref[...].astype(f32)).astype(bf16)
    out_m[...] = (m_ref[...] + am_ref[...].astype(f32)).astype(bf16)


def last_kernel(resid_ref, own_a, own_b, l_a, l_b, r_a, r_b, out_ref):
    first = lax.axis_index(C) == 0
    left = left_half()

    def total(g):
        cols = slice(g * 128, (g + 1) * 128)
        a = own_a[:, cols] + l_a[:, cols].astype(f32) + r_a[:, cols].astype(f32)
        b = own_b[:, cols] + l_b[:, cols].astype(f32) + r_b[:, cols].astype(f32)
        return jnp.where(first, a, b), jnp.where(first, b, a)

    totals = [total(g) for g in range(8)]
    for j, i in SLOTS:
        low, high = j * 4 + i, i * 4 + j
        one, two = totals[low // 2][0], totals[high // 2][1]
        one = one if low % 2 == 0 else pltpu.roll(one, 64, 1)
        two = two if high % 2 == 1 else pltpu.roll(two, 64, 1)
        cols = chip_columns(chip_of(0, j, i))
        out_ref[:, cols] = (resid_ref[:, cols] + jnp.where(left, one, two)).astype(bf16)


def by_first_core(along_y, along_z):
    pairs = []
    for z in range(4 - along_z):
        for y in range(4):
            to = (z + along_z) * 4 + (y + along_y) % 4
            pairs.append(((z * 4 + y) * 2, to * 2))
    return pairs


def ring(step):
    return [(i, (i + step) % 4) for i in range(4)]


def shape(*dims, dtype=bf16):
    return jax.ShapeDtypeStruct(dims, dtype)


def call(kernel, out_shape, n_in, cost, scratch=(), mib=8, n_hbm=0):
    out_specs = jax.tree.map(lambda _: VMEM, out_shape)
    return pl.pallas_call(
        kernel,
        out_shape=out_shape,
        in_specs=[VMEM] * n_in + [HBM] * n_hbm,
        out_specs=out_specs,
        scratch_shapes=list(scratch),
        compiler_params=_params(mib),
        cost_estimate=cost,
    )


HBM = pl.BlockSpec(memory_space=pltpu.HBM)
FEED_MIB = 20
ATTEND_MIB = 20


def feed(normed, halo, t_gate, t_value, pieces, rels, plan, dtypes):
    rows = SEG * len(rels)
    return pl.pallas_call(
        functools.partial(feed_kernel, rels, plan),
        out_shape=[shape(ROWS, 1024, dtype=d) for d in dtypes],
        in_specs=[VMEM] * 14,
        out_specs=[VMEM for _ in plan],
        scratch_shapes=[
            pltpu.VMEM((rows, D), bf16),
            pltpu.VMEM((HALO, D), f32),
            pltpu.VMEM((HALO, D), bf16),
            pltpu.VMEM((2, rows, 512), f32),
            pltpu.VMEM((ROWS * len(rels), HID), bf16),
        ],
        compiler_params=_params(FEED_MIB),
        cost_estimate=_cost(2 * rows * D * 3 * HID, 3 * D * HID * 2),
        name="feed",
    )(normed, halo, t_gate, t_value, *pieces)


def around(step, second):
    pairs = []
    for z in range(4):
        for y in range(4):
            for c in range(2):
                along_z = (c == 0) != second
                to = ((z + step) % 4, y, c) if along_z else (z, (y + step) % 4, c)
                pairs.append(((z * 4 + y) * 2 + c, (to[0] * 4 + to[1]) * 2 + c))
    return pairs


def per_device(
    x, q, k, v, switch, pre, fade, head_gain, w_out, ff_gain, w_gate, w_value, t_gate, t_value, w_down
):
    c = lax.axis_index(C)
    swap = [(0, 1), (1, 0)]

    steps = (1, 3, 2)
    shard = jnp.stack([w_gate, w_value, w_down.T], axis=0)
    first = [lax.ppermute(shard, SP, around(s, False)) for s in steps]

    cum, pack = call(
        state_kernel,
        (shape(TOK, 128, dtype=f32), shape(PACK, 128, dtype=f32)),
        0, _cost(2 * TOK * 128 * 256, 1e6),
        [
            pltpu.VMEM((TOK, 128), bf16), pltpu.VMEM((TOK, 128), bf16), pltpu.VMEM((6, 128), f32),
            pltpu.VMEM((TOK, 128), bf16), pltpu.VMEM((TOK, 256), bf16), pltpu.SemaphoreType.DMA((4,)),
        ], 8, 4,
    )(pre, fade.reshape(6, 128), k, v)
    other = lax.ppermute(pack, C, swap)

    w_half = lax.dynamic_slice_in_dim(w_out, c * 128, 128, 0)
    w_got = [lax.ppermute(w_half, X, ring(s)) for s in steps]

    chip = call(chip_kernel, shape(PACK, 128, dtype=f32), 2, _cost(1e5, 2e5))(pack, other)
    along_y = [lax.ppermute(chip, SP, by_first_core(s, 0)) for s in (3, 2, 1)]
    mech, q_shard = call(
        local_kernel, (shape(TOK, 256, dtype=f32), shape(TOK, 128)), 4,
        _cost(12 * 2 * 128 * 128 * 64 * 8, 3e6),
    )(q, k, v, cum)
    plane, before = call(
        plane_kernel, (shape(PACK, 128, dtype=f32), shape(PACK, 128, dtype=f32)), 4,
        _cost(1e5, 4e5), [pltpu.VMEM((4, PACK, 128), f32)],
    )(chip, *along_y)
    along_z = [lax.ppermute(plane, SP, by_first_core(0, s)) for s in (1, 2, 3)]
    entering = call(enter_kernel, shape(128, 128, dtype=f32), 4, _cost(1e5, 3e5))(*along_z, before)
    given = lax.ppermute(entering, C, [(0, 1)])
    stack = jnp.stack([shard, *first], axis=0)
    sides = [lax.ppermute(stack, SP, around(s, True)) for s in (1, 3)]
    mixed = call(
        finish_kernel, shape(TOK, 256), 7, _cost(2 * TOK * 128 * 256, 3e6)
    )(mech, q_shard, entering, given, other, switch, head_gain.reshape(1, DV))

    mixed_got = [lax.ppermute(mixed, X, ring(s)) for s in steps]
    sib_stack = lax.ppermute(stack, C, swap)
    w_sib = [lax.ppermute(w, C, swap) for w in w_got]
    far = [
        lax.ppermute(sides[0][:2], SP, around(1, True)),
        lax.ppermute(sides[1][2:], SP, around(3, True)),
    ]
    sib_sides = [lax.ppermute(w, C, swap) for w in sides]
    normed, tail, resid = call(
        attend_kernel,
        (shape(TOK, D), shape(HALO, D), shape(ROWS, D, dtype=f32)), 13,
        _cost(2 * TOK * 1024 * D, 1.2e7),
        [pltpu.VMEM((4, 256, D), bf16), pltpu.VMEM((ROWS, D), f32)], ATTEND_MIB,
    )(mixed, *mixed_got, w_out, *w_got, *w_sib, x, ff_gain.reshape(1, D))
    halo = lax.ppermute(tail, SP, [(i, i + 1) for i in range(31)])
    sib_far = [lax.ppermute(w, C, swap) for w in far]
    pieces = [stack, *sides, *far, sib_stack, *sib_sides, *sib_far]

    feeds = functools.partial(feed, normed, halo, t_gate, t_value, pieces)
    opp_a, opp_b = feeds((2,), ((0, 0), (0, 1)), (bf16, bf16))
    far_r = lax.ppermute(opp_a, X, ring(1))
    far_l = lax.ppermute(opp_b, X, ring(3))
    next_a, next_b, prev_a, prev_b = feeds(
        (1, 3), ((0, 0), (0, 1), (1, 0), (1, 1)), (f32, bf16, bf16, f32)
    )
    near_l_b = lax.ppermute(next_b, X, ring(1))
    near_r_a = lax.ppermute(prev_a, X, ring(3))
    send_r, send_l = call(
        add_kernel, (shape(ROWS, 1024), shape(ROWS, 1024)), 4, _cost(4e5, 4e6)
    )(next_a, far_r, prev_b, far_l)
    near_l_a = lax.ppermute(send_r, X, ring(1))
    near_r_b = lax.ppermute(send_l, X, ring(3))
    own_a, own_b = feeds((0,), ((0, 0), (0, 1)), (f32, f32))
    return call(last_kernel, shape(ROWS, D), 7, _cost(1e6, 5e6))(
        resid, own_a, own_b, near_l_a, near_l_b, near_r_a, near_r_b
    )


def solution(mesh):
    torus = Mesh(mesh.devices.reshape(4, 4, 2, 4), (Z, Y, C, X))
    return jax.shard_map(
        per_device,
        mesh=torus,
        in_specs=(
            P(SP, None), P(SP, X), P(SP, X), P(SP, X), P(SP, X), P(SP, X), P(SP), P(),
            P(X, None), P(), P(SP, X), P(SP, X), P(None, X), P(None, X), P(X, SP),
        ),
        out_specs=P((Z, Y, C, X), None),
        check_vma=False,
    )
```

time: 150 us -> 167 us (1.11)
  starting transfers between devices: 39.6 us -> 58.5 us
  between operations: 13.8 us -> 0.35 us
  waiting for transfers between devices: 45.5 us -> 56 us
  local copies, waits for them, and re-layouts: 6.57 us -> 9.76 us
  Pallas kernels: 42 us -> 39.5 us
    ppermute x17 -> x30, waiting for transfers between devices: 28.8 us -> 49.6 us  [the longest x3 20.6 us: per_device(): w_got = [lax.ppermute(w_half, X, ring(s)) for s in steps]]
    ppermute x17 -> x30, starting transfers between devices: 29.6 us -> 48.4 us  [the longest x3 9.59 us: per_device(): along_y = [lax.ppermute(chip, SP, by_first_core(s, 0)) for s in (3, 2, 1)]]
    all_gather x1 -> x0, waiting for transfers between devices: 7.59 us -> none  [per_device(): weights = lax.all_gather(packed, SP, axis=0)]
    pallas_call x14 -> x10, Pallas kernels: 40.8 us -> 37 us  [the longest x3 24.8 us: feed(): pl.pallas_call(functools.partial(feed_kernel, rels, plan), out_shape=[sha...]
    slice x1 -> x2, local copies, waits for them, and re-layouts: 0.01 us -> 2.64 us  [the longest x1 1.32 us: per_device(): sides[0][:2]]
    concatenate x1 -> x0, other arithmetic: 2.06 us -> none  [per_device(): packed = jnp.concatenate([w_gate, w_value, w_down.T], axis=0)]
    unnamed x38 -> x36, local copies, waits for them, and re-layouts: 6.53 us -> 6.03 us
  transfers between devices with their start and end apart: 24 -> 36, of which waited for: 14 -> 12; matrix products, arithmetic and copies ran while one was open for 0% -> 2% of each run, Pallas kernels for 13% -> 19%
where the time goes in v2:
time: 167 us; the launch traced here: 166 us
  starting transfers between devices  58.5 us (35%)
  waiting for transfers between devices  56 us (34%)
  Pallas kernels  39.5 us (24%)
  local copies, waits for them, and re-layouts  9.76 us (6%)
    pallas_call x3, Pallas kernels, feed(): pl.pallas_call(functools.partial(feed_kernel, rels, plan), out_shape=[sha...  24.8 us
    ppermute x3, waiting for transfers between devices, per_device(): w_got = [lax.ppermute(w_half, X, ring(s)) for s in steps]  20.6 us
    ppermute x1, waiting for transfers between devices, per_device(): lax.ppermute(sides[0][:2], SP, around(1, True))  9.8 us
    ppermute x3, starting transfers between devices, per_device(): along_y = [lax.ppermute(chip, SP, by_first_core(s, 0)) for s in (3, 2, 1)]  9.59 us
    ppermute x3, starting transfers between devices, per_device(): along_z = [lax.ppermute(plane, SP, by_first_core(0, s)) for s in (1, 2, 3)]  9.4 us
    ppermute x3, waiting for transfers between devices, per_device(): mixed_got = [lax.ppermute(mixed, X, ring(s)) for s in steps]  8.63 us
    pallas_call x1, Pallas kernels, per_device(): call(attend_kernel, (shape(TOK, D), shape(HALO, D), shape(ROWS, D, dtype=...  7.33 us
    ppermute x3, starting transfers between devices, per_device(): first = [lax.ppermute(shard, SP, around(s, False)) for s in steps]  7.19 us
  transfers between devices with their start and end apart: 36, of which 12 were waited for; matrix products, arithmetic and copies ran while one was open for 2% of the time, Pallas kernels for 19%

profile of v2, /device:TPU:24, one launch (start us, length us, event | category | flops | bytes accessed | tf_op | source)
XLA Modules:
  0.0 165.7 jit_solution(17314338996029748746)
XLA Ops:
  0.0 1.2 fusion
  1.2 4.0 %collective-permute-start.20 = (bf16[3,64,1408]{2,1,0:T(8,128)(2,1)S(1)}, bf16[3,64,1408]{2,1,0:T(8,128)(2,1)S(1)}, u32[]{:S(2)}, u32[]{:S(2)}) collective-permute-start(bf16[3,64,1408]{2,1,0:T(8,128)(2,1)S(1)} %get-tuple-element.44), channel_id=1, source_target_pairs={{0,64},{4,20},{8,72},{12,28},{16,80},{20,4},{24,88},{28,12},{32,96... | collective-permute-start | bytes 1622024 | tf_op jit(solution)/shard_map/ppermute | solution.py:417
  5.1 1.0 collective-permute-start.18
  6.2 2.2 %collective-permute-start.19 = (bf16[3,64,1408]{2,1,0:T(8,128)(2,1)S(1)}, bf16[3,64,1408]{2,1,0:T(8,128)(2,1)S(1)}, u32[]{:S(2)}, u32[]{:S(2)}) collective-permute-start(bf16[3,64,1408]{2,1,0:T(8,128)(2,1)S(1)} %get-tuple-element.44), channel_id=1, source_target_pairs={{0,96},{4,28},{8,104},{12,4},{16,112},{20,12},{24,120},{28,20},{32... | collective-permute-start | bytes 1622024 | tf_op jit(solution)/shard_map/ppermute | solution.py:417
  8.4 1.0 copy-done
  11.9 1.8 %shard_map.145 = (f32[768,128]{1,0:T(8,128)S(1)}, f32[136,128]{1,0:T(8,128)S(1)}) custom-call(bf16[768,128]{1,0:T(8,128)(2,1)S(1)} %copy-done.9, f32[6,128]{1,0:T(8,128)S(1)} %bitcast.13, bf16[768,128]{1,0:T(8,128)(2,1)S(1)} %copy-done.2, bf16[768,256]{1,0:T(8,128)(2,1)S(1)} %copy-done), custom_call_target="tpu_custom_call" | custom-call | flops 50331648 | bytes 1000000 | tf_op jit(solution)/shard_map/pallas_call | solution.py:419
  13.8 1.2 collective-permute-done.other_ref
  15.1 2.7 %collective-permute-start.1 = (f32[136,128]{1,0:T(8,128)S(1)}, f32[136,128]{1,0:T(8,128)S(1)}, u32[]{:S(2)}, u32[]{:S(2)}) collective-permute-start(f32[136,128]{1,0:T(8,128)S(1)} %shard_map.147.own_ref), channel_id=1, source_target_pairs={{0,24},{8,0},{16,8},{24,16},{32,56},{40,32},{48,40},{56,48},{64,88... | collective-permute-start | bytes 208904 | tf_op jit(solution)/shard_map/ppermute | solution.py:434
  17.8 2.8 %collective-permute-start.2 = (f32[136,128]{1,0:T(8,128)S(1)}, f32[136,128]{1,0:T(8,128)S(1)}, u32[]{:S(2)}, u32[]{:S(2)}) collective-permute-start(f32[136,128]{1,0:T(8,128)S(1)} %shard_map.147.own_ref), channel_id=1, source_target_pairs={{0,16},{8,24},{16,0},{24,8},{32,48},{40,56},{48,32},{56,40},{64,80... | collective-permute-start | bytes 208904 | tf_op jit(solution)/shard_map/ppermute | solution.py:434
  20.6 4.1 %collective-permute-start.3 = (f32[136,128]{1,0:T(8,128)S(1)}, f32[136,128]{1,0:T(8,128)S(1)}, u32[]{:S(2)}, u32[]{:S(2)}) collective-permute-start(f32[136,128]{1,0:T(8,128)S(1)} %shard_map.147.own_ref), channel_id=1, source_target_pairs={{0,8},{8,16},{16,24},{24,0},{32,40},{40,48},{48,56},{56,32},{64,72... | collective-permute-start | bytes 208904 | tf_op jit(solution)/shard_map/ppermute | solution.py:434
  25.2 1.0 collective-permute-start.21
  26.2 1.1 collective-permute-start.22
  28.6 2.3 %collective-permute-start.4 = (f32[136,128]{1,0:T(8,128)}, f32[136,128]{1,0:T(8,128)}, u32[]{:S(2)}, u32[]{:S(2)}) collective-permute-start(f32[136,128]{1,0:T(8,128)} %get-tuple-element.28), channel_id=1, source_target_pairs={{0,32},{8,40},{16,48},{24,56},{32,64},{40,72},{48,80},{56,88},{64,... | collective-permute-start | bytes 208904 | tf_op jit(solution)/shard_map/ppermute | solution.py:443
  30.9 5.2 %collective-permute-start.5 = (f32[136,128]{1,0:T(8,128)}, f32[136,128]{1,0:T(8,128)}, u32[]{:S(2)}, u32[]{:S(2)}) collective-permute-start(f32[136,128]{1,0:T(8,128)} %get-tuple-element.28), channel_id=1, source_target_pairs={{0,64},{8,72},{16,80},{24,88},{32,96},{40,104},{48,112},{56,120},{... | collective-permute-start | bytes 208904 | tf_op jit(solution)/shard_map/ppermute | solution.py:443
  36.1 1.9 %collective-permute-start.6 = (f32[136,128]{1,0:T(8,128)}, f32[136,128]{1,0:T(8,128)}, u32[]{:S(2)}, u32[]{:S(2)}) collective-permute-start(f32[136,128]{1,0:T(8,128)} %get-tuple-element.28), channel_id=1, source_target_pairs={{0,96},{8,104},{16,112},{24,120},{1,97},{9,105},{17,113},{25,121},... | collective-permute-start | bytes 208904 | tf_op jit(solution)/shard_map/ppermute | solution.py:443
  38.3 1.9 %collective-permute-done.6.z3_ref = f32[136,128]{1,0:T(8,128)} collective-permute-done((f32[136,128]{1,0:T(8,128)}, f32[136,128]{1,0:T(8,128)}, u32[]{:S(2)}, u32[]{:S(2)}) %collective-permute-start.6) | collective-permute-done | bytes 69664 | tf_op jit(solution)/shard_map/ppermute | solution.py:443
  41.1 1.0 shard_map.149.mine_ref
  42.1 1.4 collective-permute-start.7
  43.5 1.1 constant_dynamic-slice_fusion
  44.6 1.6 collective-permute-start.11
  46.2 1.7 %collective-permute-start.12 = (bf16[128,2048]{1,0:T(8,128)(2,1)S(1)}, bf16[128,2048]{1,0:T(8,128)(2,1)S(1)}, u32[]{:S(2)}, u32[]{:S(2)}) collective-permute-start(bf16[128,2048]{1,0:T(8,128)(2,1)S(1)} %constant_dynamic-slice_fusion), channel_id=1, source_target_pairs={{0,3},{1,0},{2,1},{3,2},{4,7},{5,4},{6,5},{7,6},{8,11},{9,8},{10,9... | collective-permute-start | bytes 1572872 | tf_op jit(solution)/shard_map/ppermute | solution.py:431
  48.0 1.8 %collective-permute-start.13 = (bf16[128,2048]{1,0:T(8,128)(2,1)S(1)}, bf16[128,2048]{1,0:T(8,128)(2,1)S(1)}, u32[]{:S(2)}, u32[]{:S(2)}) collective-permute-start(bf16[128,2048]{1,0:T(8,128)(2,1)S(1)} %constant_dynamic-slice_fusion), channel_id=1, source_target_pairs={{0,2},{1,3},{2,0},{3,1},{4,6},{5,7},{6,4},{7,5},{8,10},{9,11},{10,... | collective-permute-start | bytes 1572872 | tf_op jit(solution)/shard_map/ppermute | solution.py:431
  49.8 0.9 copy-done.8
  50.7 1.4 shard_map.146
  52.9 20.6 %collective-permute-done.11.got1 = bf16[128,2048]{1,0:T(8,128)(2,1)S(1)} collective-permute-done((bf16[128,2048]{1,0:T(8,128)(2,1)S(1)}, bf16[128,2048]{1,0:T(8,128)(2,1)S(1)}, u32[]{:S(2)}, u32[]{:S(2)}) %collective-permute-start.11) | collective-permute-done | bytes 524320 | tf_op jit(solution)/shard_map/ppermute | solution.py:431
  73.4 1.6 collective-permute-start.10
  75.1 3.2 %collective-permute-start.9 = (bf16[768,256]{1,0:T(8,128)(2,1)S(1)}, bf16[768,256]{1,0:T(8,128)(2,1)S(1)}, u32[]{:S(2)}, u32[]{:S(2)}) collective-permute-start(bf16[768,256]{1,0:T(8,128)(2,1)S(1)} %shard_map.150.m0), channel_id=1, source_target_pairs={{0,3},{1,0},{2,1},{3,2},{4,7},{5,4},{6,5},{7,6},{8,11},{9,8},{10,9... | collective-permute-start | bytes 1179656 | tf_op jit(solution)/shard_map/ppermute | solution.py:452
  78.3 4.5 %collective-permute-done.10.m3 = bf16[768,256]{1,0:T(8,128)(2,1)S(1)} collective-permute-done((bf16[768,256]{1,0:T(8,128)(2,1)S(1)}, bf16[768,256]{1,0:T(8,128)(2,1)S(1)}, u32[]{:S(2)}, u32[]{:S(2)}) %collective-permute-start.10) | collective-permute-done | bytes 393248 | tf_op jit(solution)/shard_map/ppermute | solution.py:452
  82.8 4.1 %collective-permute-done.8.m1 = bf16[768,256]{1,0:T(8,128)(2,1)S(1)} collective-permute-done((bf16[768,256]{1,0:T(8,128)(2,1)S(1)}, bf16[768,256]{1,0:T(8,128)(2,1)S(1)}, u32[]{:S(2)}, u32[]{:S(2)}) %collective-permute-start.8) | collective-permute-done | bytes 393248 | tf_op jit(solution)/shard_map/ppermute | solution.py:452
  87.4 1.4 collective-permute-done.15.sib2
  89.6 7.3 %shard_map.151 = (bf16[768,2048]{1,0:T(8,128)(2,1)S(1)}, bf16[16,2048]{1,0:T(8,128)(2,1)S(1)}, f32[192,2048]{1,0:T(8,128)S(1)}) custom-call(bf16[768,256]{1,0:T(8,128)(2,1)S(1)} %shard_map.150.m0, bf16[768,256]{1,0:T(8,128)(2,1)S(1)} %collective-permute-done.8.m1, bf16[768,256]{1,0:T(8,128)(2,1)S(1)} %collective-permute-done.9.m2, ...), custom_call_target="tpu_custom_call" | custom-call | flops 3221225472 | bytes 12000000 | tf_op jit(solution)/shard_map/pallas_call | solution.py:460
  96.9 2.0 %collective-permute-start.17 = (bf16[16,2048]{1,0:T(8,128)(2,1)S(1)}, bf16[16,2048]{1,0:T(8,128)(2,1)S(1)}, u32[]{:S(2)}, u32[]{:S(2)}) collective-permute-start(bf16[16,2048]{1,0:T(8,128)(2,1)S(1)} %get-tuple-element.32), channel_id=1, source_target_pairs={{0,4},{4,8},{8,12},{12,16},{16,20},{20,24},{24,28},{28,32},{32,36}... | collective-permute-start | bytes 196616 | tf_op jit(solution)/shard_map/ppermute | solution.py:466
  99.0 1.3 slice.8
  100.4 1.7 %collective-permute-start.23 = (bf16[2,3,64,1408]{3,2,1,0:T(8,128)(2,1)S(1)}, bf16[2,3,64,1408]{3,2,1,0:T(8,128)(2,1)S(1)}, u32[]{:S(2)}, u32[]{:S(2)}) collective-permute-start(bf16[2,3,64,1408]{3,2,1,0:T(8,128)(2,1)S(1)} %slice.8), channel_id=1, source_target_pairs={{0,8},{4,36},{8,16},{12,44},{16,24},{20,52},{24,0},{28,60},{32,40}... | collective-permute-start | bytes 3244040 | tf_op jit(solution)/shard_map/ppermute | solution.py:456
  102.0 1.3 slice.9
  104.1 1.9 %collective-permute-start.26 = (bf16[4,3,64,1408]{3,2,1,0:T(8,128)(2,1)}, bf16[4,3,64,1408]{3,2,1,0:T(8,128)(2,1)S(1)}, u32[]{:S(2)}, u32[]{:S(2)}) collective-permute-start(bf16[4,3,64,1408]{3,2,1,0:T(8,128)(2,1)} %collective-permute-done.21.refs_1_), channel_id=1, source_target_pairs={{0,4},{4,0},{1,5},{5,1},{2,6},{6,2},{3,7},{7,3},{8,12},{12,8},{9,1... | collective-permute-start | bytes 6488072 | tf_op jit(solution)/shard_map/ppermute | solution.py:459
  106.0 9.8 %collective-permute-done.23.refs_3_ = bf16[2,3,64,1408]{3,2,1,0:T(8,128)(2,1)S(1)} collective-permute-done((bf16[2,3,64,1408]{3,2,1,0:T(8,128)(2,1)S(1)}, bf16[2,3,64,1408]{3,2,1,0:T(8,128)(2,1)S(1)}, u32[]{:S(2)}, u32[]{:S(2)}) %collective-permute-start.23) | collective-permute-done | bytes 1081376 | tf_op jit(solution)/shard_map/ppermute | solution.py:456
  115.8 1.6 collective-permute-start.28
  117.4 2.4 %collective-permute-done.24.refs_4_ = bf16[2,3,64,1408]{3,2,1,0:T(8,128)(2,1)S(1)} collective-permute-done((bf16[2,3,64,1408]{3,2,1,0:T(8,128)(2,1)S(1)}, bf16[2,3,64,1408]{3,2,1,0:T(8,128)(2,1)S(1)}, u32[]{:S(2)}, u32[]{:S(2)}) %collective-permute-start.24) | collective-permute-done | bytes 1081376 | tf_op jit(solution)/shard_map/ppermute | solution.py:457
  119.9 2.5 %collective-permute-done.29.refs_9_ = bf16[2,3,64,1408]{3,2,1,0:T(8,128)(2,1)S(1)} collective-permute-done((bf16[2,3,64,1408]{3,2,1,0:T(8,128)(2,1)S(1)}, bf16[2,3,64,1408]{3,2,1,0:T(8,128)(2,1)S(1)}, u32[]{:S(2)}, u32[]{:S(2)}) %collective-permute-start.29) | collective-permute-done | bytes 1081376 | tf_op jit(solution)/shard_map/ppermute | solution.py:467
  122.5 7.2 %feed.5 = (bf16[192,1024]{1,0:T(8,128)(2,1)S(1)}, bf16[192,1024]{1,0:T(8,128)(2,1)S(1)}) custom-call(bf16[768,2048]{1,0:T(8,128)(2,1)S(1)} %get-tuple-element.31.x_ref, bf16[16,2048]{1,0:T(8,128)(2,1)S(1)} %collective-permute-done.17.halo_ref, bf16[3,1408]{1,0:T(4,128)(2,1)S(1)} %copy-done.12, bf16[3,1408]{1,0:T(4,128)(2,1)S(1)} %copy-done.13, ...), custom_call_target="tpu_custom_call" | custom-call | flops 3598712832 | bytes 17301504 | tf_op jit(solution)/shard_map/feed/pallas_call | solution.py:380
  129.9 3.1 %collective-permute-start.31 = (bf16[192,1024]{1,0:T(8,128)(2,1)S(1)}, bf16[192,1024]{1,0:T(8,128)(2,1)S(1)}, u32[]{:S(2)}, u32[]{:S(2)}) collective-permute-start(bf16[192,1024]{1,0:T(8,128)(2,1)S(1)} %get-tuple-element.38), channel_id=1, source_target_pairs={{0,3},{1,0},{2,1},{3,2},{4,7},{5,4},{6,5},{7,6},{8,11},{9,8},{10,9... | collective-permute-start | bytes 1179656 | tf_op jit(solution)/shard_map/ppermute | solution.py:473
  133.0 10.5 %feed.4 = (f32[192,1024]{1,0:T(8,128)S(1)}, bf16[192,1024]{1,0:T(8,128)(2,1)S(1)}, bf16[192,1024]{1,0:T(8,128)(2,1)S(1)}, f32[192,1024]{1,0:T(8,128)S(1)}) custom-call(bf16[768,2048]{1,0:T(8,128)(2,1)S(1)} %get-tuple-element.31.x_ref, bf16[16,2048]{1,0:T(8,128)(2,1)S(1)} %collective-permute-done.17.halo_ref, bf16[3,1408]{1,0:T(4,128)(2,1)S(1)} %copy-done.12, ...), custom_call_target="tpu_custom_call" | custom-call | flops 7197425664 | bytes 17301504 | tf_op jit(solution)/shard_map/feed/pallas_call | solution.py:380
  143.8 3.2 %collective-permute-start.34 = (bf16[192,1024]{1,0:T(8,128)(2,1)S(1)}, bf16[192,1024]{1,0:T(8,128)(2,1)S(1)}, u32[]{:S(2)}, u32[]{:S(2)}) collective-permute-start(bf16[192,1024]{1,0:T(8,128)(2,1)S(1)} %get-tuple-element.41), channel_id=1, source_target_pairs={{0,3},{1,0},{2,1},{3,2},{4,7},{5,4},{6,5},{7,6},{8,11},{9,8},{10,9... | collective-permute-start | bytes 1179656 | tf_op jit(solution)/shard_map/ppermute | solution.py:478
  147.2 3.2 %collective-permute-start.35 = (bf16[192,1024]{1,0:T(8,128)(2,1)S(1)}, bf16[192,1024]{1,0:T(8,128)(2,1)S(1)}, u32[]{:S(2)}, u32[]{:S(2)}) collective-permute-start(bf16[192,1024]{1,0:T(8,128)(2,1)S(1)} %get-tuple-element.42), channel_id=1, source_target_pairs={{0,3},{1,0},{2,1},{3,2},{4,7},{5,4},{6,5},{7,6},{8,11},{9,8},{10,9... | collective-permute-start | bytes 1179656 | tf_op jit(solution)/shard_map/ppermute | solution.py:483
  150.4 7.2 %feed.3 = (f32[192,1024]{1,0:T(8,128)S(1)}, f32[192,1024]{1,0:T(8,128)S(1)}) custom-call(bf16[768,2048]{1,0:T(8,128)(2,1)S(1)} %get-tuple-element.31.x_ref, bf16[16,2048]{1,0:T(8,128)(2,1)S(1)} %collective-permute-done.17.halo_ref, bf16[3,1408]{1,0:T(4,128)(2,1)S(1)} %copy-done.12, bf16[3,1408]{1,0:T(4,128)(2,1)S(1)} %copy-done.13, ...), custom_call_target="tpu_custom_call" | custom-call | flops 3598712832 | bytes 17301504 | tf_op jit(solution)/shard_map/feed/pallas_call | solution.py:380
  157.6 6.4 %collective-permute-done.32.l_a = bf16[192,1024]{1,0:T(8,128)(2,1)S(1)} collective-permute-done((bf16[192,1024]{1,0:T(8,128)(2,1)S(1)}, bf16[192,1024]{1,0:T(8,128)(2,1)S(1)}, u32[]{:S(2)}, u32[]{:S(2)}) %collective-permute-start.32) | collective-permute-done | bytes 393248 | tf_op jit(solution)/shard_map/ppermute | solution.py:482
  164.0 1.7 shard_map.153
  (77 shorter events, 9.3 us)
Async XLA Ops:
  1.2 19.4 %collective-permute-start.20 = (bf16[3,64,1408]{2,1,0:T(8,128)(2,1)S(1)}, bf16[3,64,1408]{2,1,0:T(8,128)(2,1)S(1)}, u32[]{:S(2)}, u32[]{:S(2)}) collective-permute-start(bf16[3,64,1408]{2,1,0:T(8,128)(2,1)S(1)} %get-tuple-element.44), channel_id=1, source_target_pairs={{0,64},{4,20},{8,72},{12,28},{16,80},{20,4},{24,88},{28,12},{32,96... | collective-permute-start | bytes 1622024 | tf_op jit(solution)/shard_map/ppermute | solution.py:417
  5.1 19.6 %collective-permute-start.18 = (bf16[3,64,1408]{2,1,0:T(8,128)(2,1)S(1)}, bf16[3,64,1408]{2,1,0:T(8,128)(2,1)S(1)}, u32[]{:S(2)}, u32[]{:S(2)}) collective-permute-start(bf16[3,64,1408]{2,1,0:T(8,128)(2,1)S(1)} %get-tuple-element.44), channel_id=1, source_target_pairs={{0,32},{4,12},{8,40},{12,20},{16,48},{20,28},{24,56},{28,4},{32,64... | collective-permute-start | bytes 1622024 | tf_op jit(solution)/shard_map/ppermute | solution.py:417
  6.2 18.6 %collective-permute-start.19 = (bf16[3,64,1408]{2,1,0:T(8,128)(2,1)S(1)}, bf16[3,64,1408]{2,1,0:T(8,128)(2,1)S(1)}, u32[]{:S(2)}, u32[]{:S(2)}) collective-permute-start(bf16[3,64,1408]{2,1,0:T(8,128)(2,1)S(1)} %get-tuple-element.44), channel_id=1, source_target_pairs={{0,96},{4,28},{8,104},{12,4},{16,112},{20,12},{24,120},{28,20},{32... | collective-permute-start | bytes 1622024 | tf_op jit(solution)/shard_map/ppermute | solution.py:417
  8.4 1.0 copy-start
  13.8 1.3 collective-permute-start
  15.1 9.7 %copy-start.5 = (f32[136,128]{1,0:T(8,128)}, f32[136,128]{1,0:T(8,128)S(1)}, u32[]{:S(2)}) copy-start(f32[136,128]{1,0:T(8,128)S(1)} %collective-permute-done.other_ref) | copy-start | bytes 208900
  15.1 12.1 %collective-permute-start.1 = (f32[136,128]{1,0:T(8,128)S(1)}, f32[136,128]{1,0:T(8,128)S(1)}, u32[]{:S(2)}, u32[]{:S(2)}) collective-permute-start(f32[136,128]{1,0:T(8,128)S(1)} %shard_map.147.own_ref), channel_id=1, source_target_pairs={{0,24},{8,0},{16,8},{24,16},{32,56},{40,32},{48,40},{56,48},{64,88... | collective-permute-start | bytes 208904 | tf_op jit(solution)/shard_map/ppermute | solution.py:434
  17.8 9.5 %collective-permute-start.2 = (f32[136,128]{1,0:T(8,128)S(1)}, f32[136,128]{1,0:T(8,128)S(1)}, u32[]{:S(2)}, u32[]{:S(2)}) collective-permute-start(f32[136,128]{1,0:T(8,128)S(1)} %shard_map.147.own_ref), channel_id=1, source_target_pairs={{0,16},{8,24},{16,0},{24,8},{32,48},{40,56},{48,32},{56,40},{64,80... | collective-permute-start | bytes 208904 | tf_op jit(solution)/shard_map/ppermute | solution.py:434
  20.6 6.6 %collective-permute-start.3 = (f32[136,128]{1,0:T(8,128)S(1)}, f32[136,128]{1,0:T(8,128)S(1)}, u32[]{:S(2)}, u32[]{:S(2)}) collective-permute-start(f32[136,128]{1,0:T(8,128)S(1)} %shard_map.147.own_ref), channel_id=1, source_target_pairs={{0,8},{8,16},{16,24},{24,0},{32,40},{40,48},{48,56},{56,32},{64,72... | collective-permute-start | bytes 208904 | tf_op jit(solution)/shard_map/ppermute | solution.py:434
  24.8 25.0 %copy-start.1 = (bf16[768,256]{1,0:T(8,128)(2,1)S(1)}, bf16[768,256]{1,0:T(8,128)(2,1)}, u32[]{:S(2)}) copy-start(bf16[768,256]{1,0:T(8,128)(2,1)} %v_ref.1) | copy-start | bytes 1179652
  24.8 25.0 %copy-start.3 = (bf16[768,128]{1,0:T(8,128)(2,1)S(1)}, bf16[768,128]{1,0:T(8,128)(2,1)}, u32[]{:S(2)}) copy-start(bf16[768,128]{1,0:T(8,128)(2,1)} %k_ref.1) | copy-start | bytes 589828
  24.8 27.4 %copy-start.15 = (f32[128]{0:T(128)S(1)}, f32[128]{0:T(128)}, u32[]{:S(2)}) copy-start(f32[128]{0:T(128)} %param.22) | copy-start | bytes 1540
  25.1 27.0 %copy-start.4 = (bf16[768,256]{1,0:T(8,128)(2,1)S(1)}, bf16[768,256]{1,0:T(8,128)(2,1)}, u32[]{:S(2)}) copy-start(bf16[768,256]{1,0:T(8,128)(2,1)} %gate_ref.1) | copy-start | bytes 1179652
  25.2 73.9 %collective-permute-start.21 = (bf16[4,3,64,1408]{3,2,1,0:T(8,128)(2,1)S(1)}, bf16[4,3,64,1408]{3,2,1,0:T(8,128)(2,1)}, u32[]{:S(2)}, u32[]{:S(2)}) collective-permute-start(bf16[4,3,64,1408]{3,2,1,0:T(8,128)(2,1)S(1)} %pad_maximum_fusion.refs_0_), channel_id=1, source_target_pairs={{0,8},{4,36},{8,16},{12,44},{16,24},{20,52},{24,0},{28,60},{32,40}... | collective-permute-start | bytes 6488072 | tf_op jit(solution)/shard_map/ppermute | solution.py:447
  26.2 75.8 %collective-permute-start.22 = (bf16[4,3,64,1408]{3,2,1,0:T(8,128)(2,1)S(1)}, bf16[4,3,64,1408]{3,2,1,0:T(8,128)(2,1)}, u32[]{:S(2)}, u32[]{:S(2)}) collective-permute-start(bf16[4,3,64,1408]{3,2,1,0:T(8,128)(2,1)S(1)} %pad_maximum_fusion.refs_0_), channel_id=1, source_target_pairs={{0,24},{4,100},{8,0},{12,108},{16,8},{20,116},{24,16},{28,124},{32... | collective-permute-start | bytes 6488072 | tf_op jit(solution)/shard_map/ppermute | solution.py:447
  28.6 9.4 %collective-permute-start.4 = (f32[136,128]{1,0:T(8,128)}, f32[136,128]{1,0:T(8,128)}, u32[]{:S(2)}, u32[]{:S(2)}) collective-permute-start(f32[136,128]{1,0:T(8,128)} %get-tuple-element.28), channel_id=1, source_target_pairs={{0,32},{8,40},{16,48},{24,56},{32,64},{40,72},{48,80},{56,88},{64,... | collective-permute-start | bytes 208904 | tf_op jit(solution)/shard_map/ppermute | solution.py:443
  30.9 7.4 %collective-permute-start.5 = (f32[136,128]{1,0:T(8,128)}, f32[136,128]{1,0:T(8,128)}, u32[]{:S(2)}, u32[]{:S(2)}) collective-permute-start(f32[136,128]{1,0:T(8,128)} %get-tuple-element.28), channel_id=1, source_target_pairs={{0,64},{8,72},{16,80},{24,88},{32,96},{40,104},{48,112},{56,120},{... | collective-permute-start | bytes 208904 | tf_op jit(solution)/shard_map/ppermute | solution.py:443
  36.1 4.2 %collective-permute-start.6 = (f32[136,128]{1,0:T(8,128)}, f32[136,128]{1,0:T(8,128)}, u32[]{:S(2)}, u32[]{:S(2)}) collective-permute-start(f32[136,128]{1,0:T(8,128)} %get-tuple-element.28), channel_id=1, source_target_pairs={{0,96},{8,104},{16,112},{24,120},{1,97},{9,105},{17,113},{25,121},... | collective-permute-start | bytes 208904 | tf_op jit(solution)/shard_map/ppermute | solution.py:443
  38.0 14.2 %copy-start.6 = (f32[136,128]{1,0:T(8,128)S(1)}, f32[136,128]{1,0:T(8,128)}, u32[]{:S(2)}) copy-start(f32[136,128]{1,0:T(8,128)} %copy-done.5) | copy-start | bytes 208900
  41.1 48.5 %copy-start.17 = (f32[2048]{0:T(1024)S(1)}, f32[2048]{0:T(1024)}, u32[]{:S(2)}) copy-start(f32[2048]{0:T(1024)} %param.24) | copy-start | bytes 24580
  42.1 47.5 %copy-start.7 = (bf16[256,2048]{1,0:T(8,128)(2,1)S(1)}, bf16[256,2048]{1,0:T(8,128)(2,1)}, u32[]{:S(2)}) copy-start(bf16[256,2048]{1,0:T(8,128)(2,1)} %own_w.1) | copy-start | bytes 3145732
  42.1 5.8 %collective-permute-start.7 = (f32[128,128]{1,0:T(8,128)S(1)}, f32[128,128]{1,0:T(8,128)S(1)}, u32[]{:S(2)}, u32[]{:S(2)}) collective-permute-start(f32[128,128]{1,0:T(8,128)S(1)} %shard_map.149.mine_ref), channel_id=1, source_target_pairs={{0,4},{1,5},{2,6},{3,7},{8,12},{9,13},{10,14},{11,15},{16,20},{17,... | collective-permute-start | bytes 196616 | tf_op jit(solution)/shard_map/ppermute | solution.py:445
  44.6 28.8 %collective-permute-start.11 = (bf16[128,2048]{1,0:T(8,128)(2,1)S(1)}, bf16[128,2048]{1,0:T(8,128)(2,1)S(1)}, u32[]{:S(2)}, u32[]{:S(2)}) collective-permute-start(bf16[128,2048]{1,0:T(8,128)(2,1)S(1)} %constant_dynamic-slice_fusion), channel_id=1, source_target_pairs={{0,1},{1,2},{2,3},{3,0},{4,5},{5,6},{6,7},{7,4},{8,9},{9,10},{10,1... | collective-permute-start | bytes 1572872 | tf_op jit(solution)/shard_map/ppermute | solution.py:431
  46.2 28.8 %collective-permute-start.12 = (bf16[128,2048]{1,0:T(8,128)(2,1)S(1)}, bf16[128,2048]{1,0:T(8,128)(2,1)S(1)}, u32[]{:S(2)}, u32[]{:S(2)}) collective-permute-start(bf16[128,2048]{1,0:T(8,128)(2,1)S(1)} %constant_dynamic-slice_fusion), channel_id=1, source_target_pairs={{0,3},{1,0},{2,1},{3,2},{4,7},{5,4},{6,5},{7,6},{8,11},{9,8},{10,9... | collective-permute-start | bytes 1572872 | tf_op jit(solution)/shard_map/ppermute | solution.py:431
  48.0 27.1 %collective-permute-start.13 = (bf16[128,2048]{1,0:T(8,128)(2,1)S(1)}, bf16[128,2048]{1,0:T(8,128)(2,1)S(1)}, u32[]{:S(2)}, u32[]{:S(2)}) collective-permute-start(bf16[128,2048]{1,0:T(8,128)(2,1)S(1)} %constant_dynamic-slice_fusion), channel_id=1, source_target_pairs={{0,2},{1,3},{2,0},{3,1},{4,6},{5,7},{6,4},{7,5},{8,10},{9,11},{10,... | collective-permute-start | bytes 1572872 | tf_op jit(solution)/shard_map/ppermute | solution.py:431
  50.7 38.9 %copy-start.16 = (bf16[768,2048]{1,0:T(8,128)(2,1)S(1)}, bf16[768,2048]{1,0:T(8,128)(2,1)}, u32[]{:S(2)}) copy-start(bf16[768,2048]{1,0:T(8,128)(2,1)} %x_ref.1) | copy-start | bytes 9437188
  73.4 9.4 %collective-permute-start.10 = (bf16[768,256]{1,0:T(8,128)(2,1)S(1)}, bf16[768,256]{1,0:T(8,128)(2,1)S(1)}, u32[]{:S(2)}, u32[]{:S(2)}) collective-permute-start(bf16[768,256]{1,0:T(8,128)(2,1)S(1)} %shard_map.150.m0), channel_id=1, source_target_pairs={{0,2},{1,3},{2,0},{3,1},{4,6},{5,7},{6,4},{7,5},{8,10},{9,11},{10,... | collective-permute-start | bytes 1179656 | tf_op jit(solution)/shard_map/ppermute | solution.py:452
  75.0 11.9 %collective-permute-start.8 = (bf16[768,256]{1,0:T(8,128)(2,1)S(1)}, bf16[768,256]{1,0:T(8,128)(2,1)S(1)}, u32[]{:S(2)}, u32[]{:S(2)}) collective-permute-start(bf16[768,256]{1,0:T(8,128)(2,1)S(1)} %shard_map.150.m0), channel_id=1, source_target_pairs={{0,1},{1,2},{2,3},{3,0},{4,5},{5,6},{6,7},{7,4},{8,9},{9,10},{10,1... | collective-permute-start | bytes 1179656 | tf_op jit(solution)/shard_map/ppermute | solution.py:452
  75.1 11.9 %collective-permute-start.9 = (bf16[768,256]{1,0:T(8,128)(2,1)S(1)}, bf16[768,256]{1,0:T(8,128)(2,1)S(1)}, u32[]{:S(2)}, u32[]{:S(2)}) collective-permute-start(bf16[768,256]{1,0:T(8,128)(2,1)S(1)} %shard_map.150.m0), channel_id=1, source_target_pairs={{0,3},{1,0},{2,1},{3,2},{4,7},{5,4},{6,5},{7,6},{8,11},{9,8},{10,9... | collective-permute-start | bytes 1179656 | tf_op jit(solution)/shard_map/ppermute | solution.py:452
  82.8 4.6 %collective-permute-start.14 = (bf16[128,2048]{1,0:T(8,128)(2,1)S(1)}, bf16[128,2048]{1,0:T(8,128)(2,1)S(1)}, u32[]{:S(2)}, u32[]{:S(2)}) collective-permute-start(bf16[128,2048]{1,0:T(8,128)(2,1)S(1)} %collective-permute-done.11.got1), channel_id=1, source_target_pairs={{0,4},{4,0},{1,5},{5,1},{2,6},{6,2},{3,7},{7,3},{8,12},{12,8},{9,1... | collective-permute-start | bytes 1572872 | tf_op jit(solution)/shard_map/ppermute | solution.py:454
  86.9 1.9 %collective-permute-start.15 = (bf16[128,2048]{1,0:T(8,128)(2,1)S(1)}, bf16[128,2048]{1,0:T(8,128)(2,1)S(1)}, u32[]{:S(2)}, u32[]{:S(2)}) collective-permute-start(bf16[128,2048]{1,0:T(8,128)(2,1)S(1)} %collective-permute-done.12.got2), channel_id=1, source_target_pairs={{0,4},{4,0},{1,5},{5,1},{2,6},{6,2},{3,7},{7,3},{8,12},{12,8},{9,1... | collective-permute-start | bytes 1572872 | tf_op jit(solution)/shard_map/ppermute | solution.py:454
  86.9 2.7 %collective-permute-start.16 = (bf16[128,2048]{1,0:T(8,128)(2,1)S(1)}, bf16[128,2048]{1,0:T(8,128)(2,1)S(1)}, u32[]{:S(2)}, u32[]{:S(2)}) collective-permute-start(bf16[128,2048]{1,0:T(8,128)(2,1)S(1)} %collective-permute-done.13.got3), channel_id=1, source_target_pairs={{0,4},{4,0},{1,5},{5,1},{2,6},{6,2},{3,7},{7,3},{8,12},{12,8},{9,1... | collective-permute-start | bytes 1572872 | tf_op jit(solution)/shard_map/ppermute | solution.py:454
  96.9 25.6 %copy-start.12 = (bf16[3,1408]{1,0:T(4,128)(2,1)S(1)}, bf16[3,1408]{1,0:T(4,128)(2,1)}, u32[]{:S(2)}) copy-start(bf16[3,1408]{1,0:T(4,128)(2,1)} %tg_ref.5) | copy-start | bytes 25348
  96.9 25.6 %copy-start.13 = (bf16[3,1408]{1,0:T(4,128)(2,1)S(1)}, bf16[3,1408]{1,0:T(4,128)(2,1)}, u32[]{:S(2)}) copy-start(bf16[3,1408]{1,0:T(4,128)(2,1)} %tv_ref.5) | copy-start | bytes 25348
  96.9 9.0 %collective-permute-start.17 = (bf16[16,2048]{1,0:T(8,128)(2,1)S(1)}, bf16[16,2048]{1,0:T(8,128)(2,1)S(1)}, u32[]{:S(2)}, u32[]{:S(2)}) collective-permute-start(bf16[16,2048]{1,0:T(8,128)(2,1)S(1)} %get-tuple-element.32), channel_id=1, source_target_pairs={{0,4},{4,8},{8,12},{12,16},{16,20},{20,24},{24,28},{28,32},{32,36}... | collective-permute-start | bytes 196616 | tf_op jit(solution)/shard_map/ppermute | solution.py:466
  98.9 21.0 %collective-permute-start.25 = (bf16[4,3,64,1408]{3,2,1,0:T(8,128)(2,1)S(1)}, bf16[4,3,64,1408]{3,2,1,0:T(8,128)(2,1)S(1)}, u32[]{:S(2)}, u32[]{:S(2)}) collective-permute-start(bf16[4,3,64,1408]{3,2,1,0:T(8,128)(2,1)S(1)} %pad_maximum_fusion.refs_0_), channel_id=1, source_target_pairs={{0,4},{4,0},{1,5},{5,1},{2,6},{6,2},{3,7},{7,3},{8,12},{12,8},{9,1... | collective-permute-start | bytes 6488072 | tf_op jit(solution)/shard_map/ppermute | solution.py:453
  100.4 15.4 %collective-permute-start.23 = (bf16[2,3,64,1408]{3,2,1,0:T(8,128)(2,1)S(1)}, bf16[2,3,64,1408]{3,2,1,0:T(8,128)(2,1)S(1)}, u32[]{:S(2)}, u32[]{:S(2)}) collective-permute-start(bf16[2,3,64,1408]{3,2,1,0:T(8,128)(2,1)S(1)} %slice.8), channel_id=1, source_target_pairs={{0,8},{4,36},{8,16},{12,44},{16,24},{20,52},{24,0},{28,60},{32,40}... | collective-permute-start | bytes 3244040 | tf_op jit(solution)/shard_map/ppermute | solution.py:456
  103.3 16.4 %collective-permute-start.24 = (bf16[2,3,64,1408]{3,2,1,0:T(8,128)(2,1)S(1)}, bf16[2,3,64,1408]{3,2,1,0:T(8,128)(2,1)S(1)}, u32[]{:S(2)}, u32[]{:S(2)}) collective-permute-start(bf16[2,3,64,1408]{3,2,1,0:T(8,128)(2,1)S(1)} %slice.9), channel_id=1, source_target_pairs={{0,24},{4,100},{8,0},{12,108},{16,8},{20,116},{24,16},{28,124},{32... | collective-permute-start | bytes 3244040 | tf_op jit(solution)/shard_map/ppermute | solution.py:457
  104.1 18.4 %collective-permute-start.26 = (bf16[4,3,64,1408]{3,2,1,0:T(8,128)(2,1)}, bf16[4,3,64,1408]{3,2,1,0:T(8,128)(2,1)S(1)}, u32[]{:S(2)}, u32[]{:S(2)}) collective-permute-start(bf16[4,3,64,1408]{3,2,1,0:T(8,128)(2,1)} %collective-permute-done.21.refs_1_), channel_id=1, source_target_pairs={{0,4},{4,0},{1,5},{5,1},{2,6},{6,2},{3,7},{7,3},{8,12},{12,8},{9,1... | collective-permute-start | bytes 6488072 | tf_op jit(solution)/shard_map/ppermute | solution.py:459
  106.0 16.5 %collective-permute-start.27 = (bf16[4,3,64,1408]{3,2,1,0:T(8,128)(2,1)}, bf16[4,3,64,1408]{3,2,1,0:T(8,128)(2,1)S(1)}, u32[]{:S(2)}, u32[]{:S(2)}) collective-permute-start(bf16[4,3,64,1408]{3,2,1,0:T(8,128)(2,1)} %collective-permute-done.22.refs_2_), channel_id=1, source_target_pairs={{0,4},{4,0},{1,5},{5,1},{2,6},{6,2},{3,7},{7,3},{8,12},{12,8},{9,1... | collective-permute-start | bytes 6488072 | tf_op jit(solution)/shard_map/ppermute | solution.py:459
  115.8 4.2 %collective-permute-start.28 = (bf16[2,3,64,1408]{3,2,1,0:T(8,128)(2,1)S(1)}, bf16[2,3,64,1408]{3,2,1,0:T(8,128)(2,1)S(1)}, u32[]{:S(2)}, u32[]{:S(2)}) collective-permute-start(bf16[2,3,64,1408]{3,2,1,0:T(8,128)(2,1)S(1)} %collective-permute-done.23.refs_3_), channel_id=1, source_target_pairs={{0,4},{4,0},{1,5},{5,1},{2,6},{6,2},{3,7},{7,3},{8,12},{12,8},{9,1... | collective-permute-start | bytes 3244040 | tf_op jit(solution)/shard_map/ppermute | solution.py:467
  119.8 2.7 %collective-permute-start.29 = (bf16[2,3,64,1408]{3,2,1,0:T(8,128)(2,1)S(1)}, bf16[2,3,64,1408]{3,2,1,0:T(8,128)(2,1)S(1)}, u32[]{:S(2)}, u32[]{:S(2)}) collective-permute-start(bf16[2,3,64,1408]{3,2,1,0:T(8,128)(2,1)S(1)} %collective-permute-done.24.refs_4_), channel_id=1, source_target_pairs={{0,4},{4,0},{1,5},{5,1},{2,6},{6,2},{3,7},{7,3},{8,12},{12,8},{9,1... | collective-permute-start | bytes 3244040 | tf_op jit(solution)/shard_map/ppermute | solution.py:467
  129.7 17.3 %collective-permute-start.30 = (bf16[192,1024]{1,0:T(8,128)(2,1)S(1)}, bf16[192,1024]{1,0:T(8,128)(2,1)S(1)}, u32[]{:S(2)}, u32[]{:S(2)}) collective-permute-start(bf16[192,1024]{1,0:T(8,128)(2,1)S(1)} %get-tuple-element.36), channel_id=1, source_target_pairs={{0,1},{1,2},{2,3},{3,0},{4,5},{5,6},{6,7},{7,4},{8,9},{9,10},{10,1... | collective-permute-start | bytes 1179656 | tf_op jit(solution)/shard_map/ppermute | solution.py:472
  129.9 17.1 %collective-permute-start.31 = (bf16[192,1024]{1,0:T(8,128)(2,1)S(1)}, bf16[192,1024]{1,0:T(8,128)(2,1)S(1)}, u32[]{:S(2)}, u32[]{:S(2)}) collective-permute-start(bf16[192,1024]{1,0:T(8,128)(2,1)S(1)} %get-tuple-element.38), channel_id=1, source_target_pairs={{0,3},{1,0},{2,1},{3,2},{4,7},{5,4},{6,5},{7,6},{8,11},{9,8},{10,9... | collective-permute-start | bytes 1179656 | tf_op jit(solution)/shard_map/ppermute | solution.py:473
  143.5 14.1 %collective-permute-start.33 = (bf16[192,1024]{1,0:T(8,128)(2,1)S(1)}, bf16[192,1024]{1,0:T(8,128)(2,1)S(1)}, u32[]{:S(2)}, u32[]{:S(2)}) collective-permute-start(bf16[192,1024]{1,0:T(8,128)(2,1)S(1)} %get-tuple-element.40), channel_id=1, source_target_pairs={{0,1},{1,2},{2,3},{3,0},{4,5},{5,6},{6,7},{7,4},{8,9},{9,10},{10,1... | collective-permute-start | bytes 1179656 | tf_op jit(solution)/shard_map/ppermute | solution.py:477
  143.8 13.8 %collective-permute-start.34 = (bf16[192,1024]{1,0:T(8,128)(2,1)S(1)}, bf16[192,1024]{1,0:T(8,128)(2,1)S(1)}, u32[]{:S(2)}, u32[]{:S(2)}) collective-permute-start(bf16[192,1024]{1,0:T(8,128)(2,1)S(1)} %get-tuple-element.41), channel_id=1, source_target_pairs={{0,3},{1,0},{2,1},{3,2},{4,7},{5,4},{6,5},{7,6},{8,11},{9,8},{10,9... | collective-permute-start | bytes 1179656 | tf_op jit(solution)/shard_map/ppermute | solution.py:478
  147.1 16.9 %collective-permute-start.32 = (bf16[192,1024]{1,0:T(8,128)(2,1)S(1)}, bf16[192,1024]{1,0:T(8,128)(2,1)S(1)}, u32[]{:S(2)}, u32[]{:S(2)}) collective-permute-start(bf16[192,1024]{1,0:T(8,128)(2,1)S(1)} %get-tuple-element.39), channel_id=1, source_target_pairs={{0,1},{1,2},{2,3},{3,0},{4,5},{5,6},{6,7},{7,4},{8,9},{9,10},{10,1... | collective-permute-start | bytes 1179656 | tf_op jit(solution)/shard_map/ppermute | solution.py:482
  147.2 16.8 %collective-permute-start.35 = (bf16[192,1024]{1,0:T(8,128)(2,1)S(1)}, bf16[192,1024]{1,0:T(8,128)(2,1)S(1)}, u32[]{:S(2)}, u32[]{:S(2)}) collective-permute-start(bf16[192,1024]{1,0:T(8,128)(2,1)S(1)} %get-tuple-element.42), channel_id=1, source_target_pairs={{0,3},{1,0},{2,1},{3,2},{4,7},{5,4},{6,5},{7,6},{8,11},{9,8},{10,9... | collective-permute-start | bytes 1179656 | tf_op jit(solution)/shard_map/ppermute | solution.py:483
  (6 other events, 5.0 us)

commit v3 on v2

--- a/solution.py
+++ b/solution.py
@@ -340,12 +340,11 @@
         out_ref[:, cols] = (resid_ref[:, cols] + jnp.where(left, one, two)).astype(bf16)
 
 
-def by_first_core(along_y, along_z):
+def by_first_core(step):
     pairs = []
-    for z in range(4 - along_z):
+    for z in range(4 - step):
         for y in range(4):
-            to = (z + along_z) * 4 + (y + along_y) % 4
-            pairs.append(((z * 4 + y) * 2, to * 2))
+            pairs.append(((z * 4 + y) * 2, ((z + step) * 4 + y) * 2))
     return pairs
 
 
@@ -431,7 +430,7 @@
     w_got = [lax.ppermute(w_half, X, ring(s)) for s in steps]
 
     chip = call(chip_kernel, shape(PACK, 128, dtype=f32), 2, _cost(1e5, 2e5))(pack, other)
-    along_y = [lax.ppermute(chip, SP, by_first_core(s, 0)) for s in (3, 2, 1)]
+    along_y = [lax.ppermute(chip, Y, ring(s)) for s in (3, 2, 1)]
     mech, q_shard = call(
         local_kernel, (shape(TOK, 256, dtype=f32), shape(TOK, 128)), 4,
         _cost(12 * 2 * 128 * 128 * 64 * 8, 3e6),
@@ -440,7 +439,7 @@
         plane_kernel, (shape(PACK, 128, dtype=f32), shape(PACK, 128, dtype=f32)), 4,
         _cost(1e5, 4e5), [pltpu.VMEM((4, PACK, 128), f32)],
     )(chip, *along_y)
-    along_z = [lax.ppermute(plane, SP, by_first_core(0, s)) for s in (1, 2, 3)]
+    along_z = [lax.ppermute(plane, SP, by_first_core(s)) for s in (1, 2, 3)]
     entering = call(enter_kernel, shape(128, 128, dtype=f32), 4, _cost(1e5, 3e5))(*along_z, before)
     given = lax.ppermute(entering, C, [(0, 1)])
     stack = jnp.stack([shard, *first], axis=0)

time: 167 us -> 162 us (0.970)
  starting transfers between devices: 58.5 us -> 52.7 us
    ppermute x6, starting transfers between devices: 19 us -> 13.5 us  [the longest x3 9.55 us: per_device(): along_z = [lax.ppermute(plane, SP, by_first_core(s)) for s in (1, 2, 3)]]
  transfers between devices with their start and end apart: 36 -> 36, of which waited for: 12 -> 15; matrix products, arithmetic and copies ran while one was open for 2% -> 3% of each run, Pallas kernels for 19% -> 19%
where the time goes in v3:
time: 162 us; the launch traced here: 161 us
  waiting for transfers between devices  57.5 us (35%)
  starting transfers between devices  52.7 us (33%)
  Pallas kernels  39.5 us (24%)
  local copies, waits for them, and re-layouts  9.75 us (6%)
    pallas_call x3, Pallas kernels, feed(): pl.pallas_call(functools.partial(feed_kernel, rels, plan), out_shape=[sha...  24.8 us
    ppermute x3, waiting for transfers between devices, per_device(): w_got = [lax.ppermute(w_half, X, ring(s)) for s in steps]  20.5 us
    ppermute x1, waiting for transfers between devices, per_device(): lax.ppermute(sides[0][:2], SP, around(1, True))  9.77 us
    ppermute x3, starting transfers between devices, per_device(): along_z = [lax.ppermute(plane, SP, by_first_core(s)) for s in (1, 2, 3)]  9.55 us
    ppermute x3, waiting for transfers between devices, per_device(): mixed_got = [lax.ppermute(mixed, X, ring(s)) for s in steps]  8.62 us
    pallas_call x1, Pallas kernels, per_device(): call(attend_kernel, (shape(TOK, D), shape(HALO, D), shape(ROWS, D, dtype=...  7.3 us
    ppermute x3, starting transfers between devices, per_device(): first = [lax.ppermute(shard, SP, around(s, False)) for s in steps]  7.19 us
    ppermute x1, waiting for transfers between devices, per_device(): near_l_a = lax.ppermute(send_r, X, ring(1))  6.39 us
  transfers between devices with their start and end apart: 36, of which 15 were waited for; matrix products, arithmetic and copies ran while one was open for 3% of the time, Pallas kernels for 19%

profile of v3, /device:TPU:24, one launch (start us, length us, event | category | flops | bytes accessed | tf_op | source)
XLA Modules:
  0.0 161.2 jit_solution(10358802283104648319)
XLA Ops:
  0.0 1.2 fusion
  1.2 4.0 %collective-permute-start.20 = (bf16[3,64,1408]{2,1,0:T(8,128)(2,1)S(1)}, bf16[3,64,1408]{2,1,0:T(8,128)(2,1)S(1)}, u32[]{:S(2)}, u32[]{:S(2)}) collective-permute-start(bf16[3,64,1408]{2,1,0:T(8,128)(2,1)S(1)} %get-tuple-element.44), channel_id=1, source_target_pairs={{0,64},{4,20},{8,72},{12,28},{16,80},{20,4},{24,88},{28,12},{32,96... | collective-permute-start | bytes 1622024 | tf_op jit(solution)/shard_map/ppermute | solution.py:416
  5.1 1.0 collective-permute-start.18
  6.2 2.2 %collective-permute-start.19 = (bf16[3,64,1408]{2,1,0:T(8,128)(2,1)S(1)}, bf16[3,64,1408]{2,1,0:T(8,128)(2,1)S(1)}, u32[]{:S(2)}, u32[]{:S(2)}) collective-permute-start(bf16[3,64,1408]{2,1,0:T(8,128)(2,1)S(1)} %get-tuple-element.44), channel_id=1, source_target_pairs={{0,96},{4,28},{8,104},{12,4},{16,112},{20,12},{24,120},{28,20},{32... | collective-permute-start | bytes 1622024 | tf_op jit(solution)/shard_map/ppermute | solution.py:416
  8.4 1.0 copy-done
  9.4 0.9 copy-done.2
  10.3 0.9 copy-done.9
  11.9 1.8 %shard_map.145 = (f32[768,128]{1,0:T(8,128)S(1)}, f32[136,128]{1,0:T(8,128)S(1)}) custom-call(bf16[768,128]{1,0:T(8,128)(2,1)S(1)} %copy-done.9, f32[6,128]{1,0:T(8,128)S(1)} %bitcast.13, bf16[768,128]{1,0:T(8,128)(2,1)S(1)} %copy-done.2, bf16[768,256]{1,0:T(8,128)(2,1)S(1)} %copy-done), custom_call_target="tpu_custom_call" | custom-call | flops 50331648 | bytes 1000000 | tf_op jit(solution)/shard_map/pallas_call | solution.py:418
  13.8 1.2 collective-permute-done.other_ref
  15.9 0.9 collective-permute-start.2
  16.9 2.2 %collective-permute-start.3 = (f32[136,128]{1,0:T(8,128)S(1)}, f32[136,128]{1,0:T(8,128)S(1)}, u32[]{:S(2)}, u32[]{:S(2)}) collective-permute-start(f32[136,128]{1,0:T(8,128)S(1)} %shard_map.147.own_ref), channel_id=1, source_target_pairs={{0,8},{8,16},{16,24},{24,0},{1,9},{9,17},{17,25},{25,1},{2,10},{10... | collective-permute-start | bytes 208904 | tf_op jit(solution)/shard_map/ppermute | solution.py:433
  20.5 1.3 collective-permute-start.22
  24.0 2.7 %collective-permute-start.4 = (f32[136,128]{1,0:T(8,128)}, f32[136,128]{1,0:T(8,128)}, u32[]{:S(2)}, u32[]{:S(2)}) collective-permute-start(f32[136,128]{1,0:T(8,128)} %get-tuple-element.28), channel_id=1, source_target_pairs={{0,32},{8,40},{16,48},{24,56},{32,64},{40,72},{48,80},{56,88},{64,... | collective-permute-start | bytes 208904 | tf_op jit(solution)/shard_map/ppermute | solution.py:442
  26.7 5.0 %collective-permute-start.5 = (f32[136,128]{1,0:T(8,128)}, f32[136,128]{1,0:T(8,128)}, u32[]{:S(2)}, u32[]{:S(2)}) collective-permute-start(f32[136,128]{1,0:T(8,128)} %get-tuple-element.28), channel_id=1, source_target_pairs={{0,64},{8,72},{16,80},{24,88},{32,96},{40,104},{48,112},{56,120},{... | collective-permute-start | bytes 208904 | tf_op jit(solution)/shard_map/ppermute | solution.py:442
  31.7 1.9 %collective-permute-start.6 = (f32[136,128]{1,0:T(8,128)}, f32[136,128]{1,0:T(8,128)}, u32[]{:S(2)}, u32[]{:S(2)}) collective-permute-start(f32[136,128]{1,0:T(8,128)} %get-tuple-element.28), channel_id=1, source_target_pairs={{0,96},{8,104},{16,112},{24,120},{1,97},{9,105},{17,113},{25,121},... | collective-permute-start | bytes 208904 | tf_op jit(solution)/shard_map/ppermute | solution.py:442
  33.9 1.9 %collective-permute-done.6.z3_ref = f32[136,128]{1,0:T(8,128)} collective-permute-done((f32[136,128]{1,0:T(8,128)}, f32[136,128]{1,0:T(8,128)}, u32[]{:S(2)}, u32[]{:S(2)}) %collective-permute-start.6) | collective-permute-done | bytes 69664 | tf_op jit(solution)/shard_map/ppermute | solution.py:442
  36.7 1.0 shard_map.149.mine_ref
  37.7 1.4 collective-permute-start.7
  39.1 1.1 constant_dynamic-slice_fusion
  40.2 1.6 collective-permute-start.11
  41.8 1.7 %collective-permute-start.12 = (bf16[128,2048]{1,0:T(8,128)(2,1)S(1)}, bf16[128,2048]{1,0:T(8,128)(2,1)S(1)}, u32[]{:S(2)}, u32[]{:S(2)}) collective-permute-start(bf16[128,2048]{1,0:T(8,128)(2,1)S(1)} %constant_dynamic-slice_fusion), channel_id=1, source_target_pairs={{0,3},{1,0},{2,1},{3,2},{4,7},{5,4},{6,5},{7,6},{8,11},{9,8},{10,9... | collective-permute-start | bytes 1572872 | tf_op jit(solution)/shard_map/ppermute | solution.py:430
  43.5 1.8 %collective-permute-start.13 = (bf16[128,2048]{1,0:T(8,128)(2,1)S(1)}, bf16[128,2048]{1,0:T(8,128)(2,1)S(1)}, u32[]{:S(2)}, u32[]{:S(2)}) collective-permute-start(bf16[128,2048]{1,0:T(8,128)(2,1)S(1)} %constant_dynamic-slice_fusion), channel_id=1, source_target_pairs={{0,2},{1,3},{2,0},{3,1},{4,6},{5,7},{6,4},{7,5},{8,10},{9,11},{10,... | collective-permute-start | bytes 1572872 | tf_op jit(solution)/shard_map/ppermute | solution.py:430
  45.4 0.9 copy-done.8
  46.3 1.5 shard_map.146
  48.5 20.5 %collective-permute-done.11.got1 = bf16[128,2048]{1,0:T(8,128)(2,1)S(1)} collective-permute-done((bf16[128,2048]{1,0:T(8,128)(2,1)S(1)}, bf16[128,2048]{1,0:T(8,128)(2,1)S(1)}, u32[]{:S(2)}, u32[]{:S(2)}) %collective-permute-start.11) | collective-permute-done | bytes 524320 | tf_op jit(solution)/shard_map/ppermute | solution.py:430
  69.0 1.6 %collective-permute-start.10 = (bf16[768,256]{1,0:T(8,128)(2,1)S(1)}, bf16[768,256]{1,0:T(8,128)(2,1)S(1)}, u32[]{:S(2)}, u32[]{:S(2)}) collective-permute-start(bf16[768,256]{1,0:T(8,128)(2,1)S(1)} %shard_map.150.m0), channel_id=1, source_target_pairs={{0,2},{1,3},{2,0},{3,1},{4,6},{5,7},{6,4},{7,5},{8,10},{9,11},{10,... | collective-permute-start | bytes 1179656 | tf_op jit(solution)/shard_map/ppermute | solution.py:451
  70.6 3.2 %collective-permute-start.9 = (bf16[768,256]{1,0:T(8,128)(2,1)S(1)}, bf16[768,256]{1,0:T(8,128)(2,1)S(1)}, u32[]{:S(2)}, u32[]{:S(2)}) collective-permute-start(bf16[768,256]{1,0:T(8,128)(2,1)S(1)} %shard_map.150.m0), channel_id=1, source_target_pairs={{0,3},{1,0},{2,1},{3,2},{4,7},{5,4},{6,5},{7,6},{8,11},{9,8},{10,9... | collective-permute-start | bytes 1179656 | tf_op jit(solution)/shard_map/ppermute | solution.py:451
  73.9 4.5 %collective-permute-done.10.m3 = bf16[768,256]{1,0:T(8,128)(2,1)S(1)} collective-permute-done((bf16[768,256]{1,0:T(8,128)(2,1)S(1)}, bf16[768,256]{1,0:T(8,128)(2,1)S(1)}, u32[]{:S(2)}, u32[]{:S(2)}) %collective-permute-start.10) | collective-permute-done | bytes 393248 | tf_op jit(solution)/shard_map/ppermute | solution.py:451
  78.4 4.1 %collective-permute-done.8.m1 = bf16[768,256]{1,0:T(8,128)(2,1)S(1)} collective-permute-done((bf16[768,256]{1,0:T(8,128)(2,1)S(1)}, bf16[768,256]{1,0:T(8,128)(2,1)S(1)}, u32[]{:S(2)}, u32[]{:S(2)}) %collective-permute-start.8) | collective-permute-done | bytes 393248 | tf_op jit(solution)/shard_map/ppermute | solution.py:451
  83.0 1.4 collective-permute-done.15.sib2
  85.2 7.3 %shard_map.151 = (bf16[768,2048]{1,0:T(8,128)(2,1)S(1)}, bf16[16,2048]{1,0:T(8,128)(2,1)S(1)}, f32[192,2048]{1,0:T(8,128)S(1)}) custom-call(bf16[768,256]{1,0:T(8,128)(2,1)S(1)} %shard_map.150.m0, bf16[768,256]{1,0:T(8,128)(2,1)S(1)} %collective-permute-done.8.m1, bf16[768,256]{1,0:T(8,128)(2,1)S(1)} %collective-permute-done.9.m2, ...), custom_call_target="tpu_custom_call" | custom-call | flops 3221225472 | bytes 12000000 | tf_op jit(solution)/shard_map/pallas_call | solution.py:459
  92.5 2.0 %collective-permute-start.17 = (bf16[16,2048]{1,0:T(8,128)(2,1)S(1)}, bf16[16,2048]{1,0:T(8,128)(2,1)S(1)}, u32[]{:S(2)}, u32[]{:S(2)}) collective-permute-start(bf16[16,2048]{1,0:T(8,128)(2,1)S(1)} %get-tuple-element.32), channel_id=1, source_target_pairs={{0,4},{4,8},{8,12},{12,16},{16,20},{20,24},{24,28},{28,32},{32,36}... | collective-permute-start | bytes 196616 | tf_op jit(solution)/shard_map/ppermute | solution.py:465
  94.6 1.3 slice.8
  95.9 1.8 %collective-permute-start.23 = (bf16[2,3,64,1408]{3,2,1,0:T(8,128)(2,1)S(1)}, bf16[2,3,64,1408]{3,2,1,0:T(8,128)(2,1)S(1)}, u32[]{:S(2)}, u32[]{:S(2)}) collective-permute-start(bf16[2,3,64,1408]{3,2,1,0:T(8,128)(2,1)S(1)} %slice.8), channel_id=1, source_target_pairs={{0,8},{4,36},{8,16},{12,44},{16,24},{20,52},{24,0},{28,60},{32,40}... | collective-permute-start | bytes 3244040 | tf_op jit(solution)/shard_map/ppermute | solution.py:455
  97.8 1.3 slice.9
  99.4 1.9 %collective-permute-start.26 = (bf16[4,3,64,1408]{3,2,1,0:T(8,128)(2,1)}, bf16[4,3,64,1408]{3,2,1,0:T(8,128)(2,1)S(1)}, u32[]{:S(2)}, u32[]{:S(2)}) collective-permute-start(bf16[4,3,64,1408]{3,2,1,0:T(8,128)(2,1)} %collective-permute-done.21.refs_1_), channel_id=1, source_target_pairs={{0,4},{4,0},{1,5},{5,1},{2,6},{6,2},{3,7},{7,3},{8,12},{12,8},{9,1... | collective-permute-start | bytes 6488072 | tf_op jit(solution)/shard_map/ppermute | solution.py:458
  101.4 9.8 %collective-permute-done.23.refs_3_ = bf16[2,3,64,1408]{3,2,1,0:T(8,128)(2,1)S(1)} collective-permute-done((bf16[2,3,64,1408]{3,2,1,0:T(8,128)(2,1)S(1)}, bf16[2,3,64,1408]{3,2,1,0:T(8,128)(2,1)S(1)}, u32[]{:S(2)}, u32[]{:S(2)}) %collective-permute-start.23) | collective-permute-done | bytes 1081376 | tf_op jit(solution)/shard_map/ppermute | solution.py:455
  111.2 1.6 %collective-permute-start.28 = (bf16[2,3,64,1408]{3,2,1,0:T(8,128)(2,1)S(1)}, bf16[2,3,64,1408]{3,2,1,0:T(8,128)(2,1)S(1)}, u32[]{:S(2)}, u32[]{:S(2)}) collective-permute-start(bf16[2,3,64,1408]{3,2,1,0:T(8,128)(2,1)S(1)} %collective-permute-done.23.refs_3_), channel_id=1, source_target_pairs={{0,4},{4,0},{1,5},{5,1},{2,6},{6,2},{3,7},{7,3},{8,12},{12,8},{9,1... | collective-permute-start | bytes 3244040 | tf_op jit(solution)/shard_map/ppermute | solution.py:466
  112.8 2.7 %collective-permute-done.24.refs_4_ = bf16[2,3,64,1408]{3,2,1,0:T(8,128)(2,1)S(1)} collective-permute-done((bf16[2,3,64,1408]{3,2,1,0:T(8,128)(2,1)S(1)}, bf16[2,3,64,1408]{3,2,1,0:T(8,128)(2,1)S(1)}, u32[]{:S(2)}, u32[]{:S(2)}) %collective-permute-start.24) | collective-permute-done | bytes 1081376 | tf_op jit(solution)/shard_map/ppermute | solution.py:456
  115.6 2.6 %collective-permute-done.29.refs_9_ = bf16[2,3,64,1408]{3,2,1,0:T(8,128)(2,1)S(1)} collective-permute-done((bf16[2,3,64,1408]{3,2,1,0:T(8,128)(2,1)S(1)}, bf16[2,3,64,1408]{3,2,1,0:T(8,128)(2,1)S(1)}, u32[]{:S(2)}, u32[]{:S(2)}) %collective-permute-start.29) | collective-permute-done | bytes 1081376 | tf_op jit(solution)/shard_map/ppermute | solution.py:466
  118.2 7.2 %feed.5 = (bf16[192,1024]{1,0:T(8,128)(2,1)S(1)}, bf16[192,1024]{1,0:T(8,128)(2,1)S(1)}) custom-call(bf16[768,2048]{1,0:T(8,128)(2,1)S(1)} %get-tuple-element.31.x_ref, bf16[16,2048]{1,0:T(8,128)(2,1)S(1)} %collective-permute-done.17.halo_ref, bf16[3,1408]{1,0:T(4,128)(2,1)S(1)} %copy-done.12, bf16[3,1408]{1,0:T(4,128)(2,1)S(1)} %copy-done.13, ...), custom_call_target="tpu_custom_call" | custom-call | flops 3598712832 | bytes 17301504 | tf_op jit(solution)/shard_map/feed/pallas_call | solution.py:379
  125.6 3.1 %collective-permute-start.31 = (bf16[192,1024]{1,0:T(8,128)(2,1)S(1)}, bf16[192,1024]{1,0:T(8,128)(2,1)S(1)}, u32[]{:S(2)}, u32[]{:S(2)}) collective-permute-start(bf16[192,1024]{1,0:T(8,128)(2,1)S(1)} %get-tuple-element.38), channel_id=1, source_target_pairs={{0,3},{1,0},{2,1},{3,2},{4,7},{5,4},{6,5},{7,6},{8,11},{9,8},{10,9... | collective-permute-start | bytes 1179656 | tf_op jit(solution)/shard_map/ppermute | solution.py:472
  128.7 10.5 %feed.4 = (f32[192,1024]{1,0:T(8,128)S(1)}, bf16[192,1024]{1,0:T(8,128)(2,1)S(1)}, bf16[192,1024]{1,0:T(8,128)(2,1)S(1)}, f32[192,1024]{1,0:T(8,128)S(1)}) custom-call(bf16[768,2048]{1,0:T(8,128)(2,1)S(1)} %get-tuple-element.31.x_ref, bf16[16,2048]{1,0:T(8,128)(2,1)S(1)} %collective-permute-done.17.halo_ref, bf16[3,1408]{1,0:T(4,128)(2,1)S(1)} %copy-done.12, ...), custom_call_target="tpu_custom_call" | custom-call | flops 7197425664 | bytes 17301504 | tf_op jit(solution)/shard_map/feed/pallas_call | solution.py:379
  139.3 3.2 %collective-permute-start.34 = (bf16[192,1024]{1,0:T(8,128)(2,1)S(1)}, bf16[192,1024]{1,0:T(8,128)(2,1)S(1)}, u32[]{:S(2)}, u32[]{:S(2)}) collective-permute-start(bf16[192,1024]{1,0:T(8,128)(2,1)S(1)} %get-tuple-element.41), channel_id=1, source_target_pairs={{0,3},{1,0},{2,1},{3,2},{4,7},{5,4},{6,5},{7,6},{8,11},{9,8},{10,9... | collective-permute-start | bytes 1179656 | tf_op jit(solution)/shard_map/ppermute | solution.py:477
  142.7 3.2 %collective-permute-start.35 = (bf16[192,1024]{1,0:T(8,128)(2,1)S(1)}, bf16[192,1024]{1,0:T(8,128)(2,1)S(1)}, u32[]{:S(2)}, u32[]{:S(2)}) collective-permute-start(bf16[192,1024]{1,0:T(8,128)(2,1)S(1)} %get-tuple-element.42), channel_id=1, source_target_pairs={{0,3},{1,0},{2,1},{3,2},{4,7},{5,4},{6,5},{7,6},{8,11},{9,8},{10,9... | collective-permute-start | bytes 1179656 | tf_op jit(solution)/shard_map/ppermute | solution.py:482
  145.9 7.1 %feed.3 = (f32[192,1024]{1,0:T(8,128)S(1)}, f32[192,1024]{1,0:T(8,128)S(1)}) custom-call(bf16[768,2048]{1,0:T(8,128)(2,1)S(1)} %get-tuple-element.31.x_ref, bf16[16,2048]{1,0:T(8,128)(2,1)S(1)} %collective-permute-done.17.halo_ref, bf16[3,1408]{1,0:T(4,128)(2,1)S(1)} %copy-done.12, bf16[3,1408]{1,0:T(4,128)(2,1)S(1)} %copy-done.13, ...), custom_call_target="tpu_custom_call" | custom-call | flops 3598712832 | bytes 17301504 | tf_op jit(solution)/shard_map/feed/pallas_call | solution.py:379
  153.1 6.4 %collective-permute-done.32.l_a = bf16[192,1024]{1,0:T(8,128)(2,1)S(1)} collective-permute-done((bf16[192,1024]{1,0:T(8,128)(2,1)S(1)}, bf16[192,1024]{1,0:T(8,128)(2,1)S(1)}, u32[]{:S(2)}, u32[]{:S(2)}) %collective-permute-start.32) | collective-permute-done | bytes 393248 | tf_op jit(solution)/shard_map/ppermute | solution.py:481
  159.5 1.7 %shard_map.153 = bf16[192,2048]{1,0:T(8,128)(2,1)} custom-call(f32[192,2048]{1,0:T(8,128)S(1)} %get-tuple-element.30.resid_ref, f32[192,1024]{1,0:T(8,128)S(1)} %get-tuple-element.33.own_a, f32[192,1024]{1,0:T(8,128)S(1)} %get-tuple-element.34.own_b, bf16[192,1024]{1,0:T(8,128)(2,1)S(1)} %collective-permute-done.32.l_a, ...), custom_call_target="tpu_custom_call" | custom-call | flops 1000000 | bytes 5000000 | tf_op jit(solution)/shard_map/pallas_call | solution.py:484
  (77 shorter events, 9.6 us)
Async XLA Ops:
  1.2 15.7 %collective-permute-start.20 = (bf16[3,64,1408]{2,1,0:T(8,128)(2,1)S(1)}, bf16[3,64,1408]{2,1,0:T(8,128)(2,1)S(1)}, u32[]{:S(2)}, u32[]{:S(2)}) collective-permute-start(bf16[3,64,1408]{2,1,0:T(8,128)(2,1)S(1)} %get-tuple-element.44), channel_id=1, source_target_pairs={{0,64},{4,20},{8,72},{12,28},{16,80},{20,4},{24,88},{28,12},{32,96... | collective-permute-start | bytes 1622024 | tf_op jit(solution)/shard_map/ppermute | solution.py:416
  5.1 13.9 %collective-permute-start.18 = (bf16[3,64,1408]{2,1,0:T(8,128)(2,1)S(1)}, bf16[3,64,1408]{2,1,0:T(8,128)(2,1)S(1)}, u32[]{:S(2)}, u32[]{:S(2)}) collective-permute-start(bf16[3,64,1408]{2,1,0:T(8,128)(2,1)S(1)} %get-tuple-element.44), channel_id=1, source_target_pairs={{0,32},{4,12},{8,40},{12,20},{16,48},{20,28},{24,56},{28,4},{32,64... | collective-permute-start | bytes 1622024 | tf_op jit(solution)/shard_map/ppermute | solution.py:416
  6.2 13.2 %collective-permute-start.19 = (bf16[3,64,1408]{2,1,0:T(8,128)(2,1)S(1)}, bf16[3,64,1408]{2,1,0:T(8,128)(2,1)S(1)}, u32[]{:S(2)}, u32[]{:S(2)}) collective-permute-start(bf16[3,64,1408]{2,1,0:T(8,128)(2,1)S(1)} %get-tuple-element.44), channel_id=1, source_target_pairs={{0,96},{4,28},{8,104},{12,4},{16,112},{20,12},{24,120},{28,20},{32... | collective-permute-start | bytes 1622024 | tf_op jit(solution)/shard_map/ppermute | solution.py:416
  8.4 1.0 copy-start
  13.8 1.3 collective-permute-start
  15.1 4.2 %copy-start.5 = (f32[136,128]{1,0:T(8,128)}, f32[136,128]{1,0:T(8,128)S(1)}, u32[]{:S(2)}) copy-start(f32[136,128]{1,0:T(8,128)S(1)} %collective-permute-done.other_ref) | copy-start | bytes 208900
  15.1 7.0 %collective-permute-start.1 = (f32[136,128]{1,0:T(8,128)S(1)}, f32[136,128]{1,0:T(8,128)S(1)}, u32[]{:S(2)}, u32[]{:S(2)}) collective-permute-start(f32[136,128]{1,0:T(8,128)S(1)} %shard_map.147.own_ref), channel_id=1, source_target_pairs={{0,24},{8,0},{16,8},{24,16},{1,25},{9,1},{17,9},{25,17},{2,26},{10... | collective-permute-start | bytes 208904 | tf_op jit(solution)/shard_map/ppermute | solution.py:433
  15.9 6.2 %collective-permute-start.2 = (f32[136,128]{1,0:T(8,128)S(1)}, f32[136,128]{1,0:T(8,128)S(1)}, u32[]{:S(2)}, u32[]{:S(2)}) collective-permute-start(f32[136,128]{1,0:T(8,128)S(1)} %shard_map.147.own_ref), channel_id=1, source_target_pairs={{0,16},{8,24},{16,0},{24,8},{1,17},{9,25},{17,1},{25,9},{2,18},{10... | collective-permute-start | bytes 208904 | tf_op jit(solution)/shard_map/ppermute | solution.py:433
  16.9 5.8 %collective-permute-start.3 = (f32[136,128]{1,0:T(8,128)S(1)}, f32[136,128]{1,0:T(8,128)S(1)}, u32[]{:S(2)}, u32[]{:S(2)}) collective-permute-start(f32[136,128]{1,0:T(8,128)S(1)} %shard_map.147.own_ref), channel_id=1, source_target_pairs={{0,8},{8,16},{16,24},{24,0},{1,9},{9,17},{17,25},{25,1},{2,10},{10... | collective-permute-start | bytes 208904 | tf_op jit(solution)/shard_map/ppermute | solution.py:433
  19.3 26.0 %copy-start.1 = (bf16[768,256]{1,0:T(8,128)(2,1)S(1)}, bf16[768,256]{1,0:T(8,128)(2,1)}, u32[]{:S(2)}) copy-start(bf16[768,256]{1,0:T(8,128)(2,1)} %v_ref.1) | copy-start | bytes 1179652
  19.3 26.0 %copy-start.3 = (bf16[768,128]{1,0:T(8,128)(2,1)S(1)}, bf16[768,128]{1,0:T(8,128)(2,1)}, u32[]{:S(2)}) copy-start(bf16[768,128]{1,0:T(8,128)(2,1)} %k_ref.1) | copy-start | bytes 589828
  19.3 28.4 %copy-start.15 = (f32[128]{0:T(128)S(1)}, f32[128]{0:T(128)}, u32[]{:S(2)}) copy-start(f32[128]{0:T(128)} %param.22) | copy-start | bytes 1540
  19.7 28.1 %copy-start.4 = (bf16[768,256]{1,0:T(8,128)(2,1)S(1)}, bf16[768,256]{1,0:T(8,128)(2,1)}, u32[]{:S(2)}) copy-start(bf16[768,256]{1,0:T(8,128)(2,1)} %gate_ref.1) | copy-start | bytes 1179652
  19.7 74.9 %collective-permute-start.21 = (bf16[4,3,64,1408]{3,2,1,0:T(8,128)(2,1)S(1)}, bf16[4,3,64,1408]{3,2,1,0:T(8,128)(2,1)}, u32[]{:S(2)}, u32[]{:S(2)}) collective-permute-start(bf16[4,3,64,1408]{3,2,1,0:T(8,128)(2,1)S(1)} %pad_maximum_fusion.refs_0_), channel_id=1, source_target_pairs={{0,8},{4,36},{8,16},{12,44},{16,24},{20,52},{24,0},{28,60},{32,40}... | collective-permute-start | bytes 6488072 | tf_op jit(solution)/shard_map/ppermute | solution.py:446
  20.5 77.3 %collective-permute-start.22 = (bf16[4,3,64,1408]{3,2,1,0:T(8,128)(2,1)S(1)}, bf16[4,3,64,1408]{3,2,1,0:T(8,128)(2,1)}, u32[]{:S(2)}, u32[]{:S(2)}) collective-permute-start(bf16[4,3,64,1408]{3,2,1,0:T(8,128)(2,1)S(1)} %pad_maximum_fusion.refs_0_), channel_id=1, source_target_pairs={{0,24},{4,100},{8,0},{12,108},{16,8},{20,116},{24,16},{28,124},{32... | collective-permute-start | bytes 6488072 | tf_op jit(solution)/shard_map/ppermute | solution.py:446
  24.0 9.6 %collective-permute-start.4 = (f32[136,128]{1,0:T(8,128)}, f32[136,128]{1,0:T(8,128)}, u32[]{:S(2)}, u32[]{:S(2)}) collective-permute-start(f32[136,128]{1,0:T(8,128)} %get-tuple-element.28), channel_id=1, source_target_pairs={{0,32},{8,40},{16,48},{24,56},{32,64},{40,72},{48,80},{56,88},{64,... | collective-permute-start | bytes 208904 | tf_op jit(solution)/shard_map/ppermute | solution.py:442
  26.7 7.2 %collective-permute-start.5 = (f32[136,128]{1,0:T(8,128)}, f32[136,128]{1,0:T(8,128)}, u32[]{:S(2)}, u32[]{:S(2)}) collective-permute-start(f32[136,128]{1,0:T(8,128)} %get-tuple-element.28), channel_id=1, source_target_pairs={{0,64},{8,72},{16,80},{24,88},{32,96},{40,104},{48,112},{56,120},{... | collective-permute-start | bytes 208904 | tf_op jit(solution)/shard_map/ppermute | solution.py:442
  31.7 4.2 %collective-permute-start.6 = (f32[136,128]{1,0:T(8,128)}, f32[136,128]{1,0:T(8,128)}, u32[]{:S(2)}, u32[]{:S(2)}) collective-permute-start(f32[136,128]{1,0:T(8,128)} %get-tuple-element.28), channel_id=1, source_target_pairs={{0,96},{8,104},{16,112},{24,120},{1,97},{9,105},{17,113},{25,121},... | collective-permute-start | bytes 208904 | tf_op jit(solution)/shard_map/ppermute | solution.py:442
  33.6 14.2 %copy-start.6 = (f32[136,128]{1,0:T(8,128)S(1)}, f32[136,128]{1,0:T(8,128)}, u32[]{:S(2)}) copy-start(f32[136,128]{1,0:T(8,128)} %copy-done.5) | copy-start | bytes 208900
  36.7 48.5 %copy-start.17 = (f32[2048]{0:T(1024)S(1)}, f32[2048]{0:T(1024)}, u32[]{:S(2)}) copy-start(f32[2048]{0:T(1024)} %param.24) | copy-start | bytes 24580
  37.7 47.5 %copy-start.7 = (bf16[256,2048]{1,0:T(8,128)(2,1)S(1)}, bf16[256,2048]{1,0:T(8,128)(2,1)}, u32[]{:S(2)}) copy-start(bf16[256,2048]{1,0:T(8,128)(2,1)} %own_w.1) | copy-start | bytes 3145732
  37.7 5.8 %collective-permute-start.7 = (f32[128,128]{1,0:T(8,128)S(1)}, f32[128,128]{1,0:T(8,128)S(1)}, u32[]{:S(2)}, u32[]{:S(2)}) collective-permute-start(f32[128,128]{1,0:T(8,128)S(1)} %shard_map.149.mine_ref), channel_id=1, source_target_pairs={{0,4},{1,5},{2,6},{3,7},{8,12},{9,13},{10,14},{11,15},{16,20},{17,... | collective-permute-start | bytes 196616 | tf_op jit(solution)/shard_map/ppermute | solution.py:444
  40.2 28.8 %collective-permute-start.11 = (bf16[128,2048]{1,0:T(8,128)(2,1)S(1)}, bf16[128,2048]{1,0:T(8,128)(2,1)S(1)}, u32[]{:S(2)}, u32[]{:S(2)}) collective-permute-start(bf16[128,2048]{1,0:T(8,128)(2,1)S(1)} %constant_dynamic-slice_fusion), channel_id=1, source_target_pairs={{0,1},{1,2},{2,3},{3,0},{4,5},{5,6},{6,7},{7,4},{8,9},{9,10},{10,1... | collective-permute-start | bytes 1572872 | tf_op jit(solution)/shard_map/ppermute | solution.py:430
  41.8 28.8 %collective-permute-start.12 = (bf16[128,2048]{1,0:T(8,128)(2,1)S(1)}, bf16[128,2048]{1,0:T(8,128)(2,1)S(1)}, u32[]{:S(2)}, u32[]{:S(2)}) collective-permute-start(bf16[128,2048]{1,0:T(8,128)(2,1)S(1)} %constant_dynamic-slice_fusion), channel_id=1, source_target_pairs={{0,3},{1,0},{2,1},{3,2},{4,7},{5,4},{6,5},{7,6},{8,11},{9,8},{10,9... | collective-permute-start | bytes 1572872 | tf_op jit(solution)/shard_map/ppermute | solution.py:430
  43.5 27.1 %collective-permute-start.13 = (bf16[128,2048]{1,0:T(8,128)(2,1)S(1)}, bf16[128,2048]{1,0:T(8,128)(2,1)S(1)}, u32[]{:S(2)}, u32[]{:S(2)}) collective-permute-start(bf16[128,2048]{1,0:T(8,128)(2,1)S(1)} %constant_dynamic-slice_fusion), channel_id=1, source_target_pairs={{0,2},{1,3},{2,0},{3,1},{4,6},{5,7},{6,4},{7,5},{8,10},{9,11},{10,... | collective-permute-start | bytes 1572872 | tf_op jit(solution)/shard_map/ppermute | solution.py:430
  46.3 38.9 %copy-start.16 = (bf16[768,2048]{1,0:T(8,128)(2,1)S(1)}, bf16[768,2048]{1,0:T(8,128)(2,1)}, u32[]{:S(2)}) copy-start(bf16[768,2048]{1,0:T(8,128)(2,1)} %x_ref.1) | copy-start | bytes 9437188
  69.0 9.4 %collective-permute-start.10 = (bf16[768,256]{1,0:T(8,128)(2,1)S(1)}, bf16[768,256]{1,0:T(8,128)(2,1)S(1)}, u32[]{:S(2)}, u32[]{:S(2)}) collective-permute-start(bf16[768,256]{1,0:T(8,128)(2,1)S(1)} %shard_map.150.m0), channel_id=1, source_target_pairs={{0,2},{1,3},{2,0},{3,1},{4,6},{5,7},{6,4},{7,5},{8,10},{9,11},{10,... | collective-permute-start | bytes 1179656 | tf_op jit(solution)/shard_map/ppermute | solution.py:451
  70.6 11.9 %collective-permute-start.8 = (bf16[768,256]{1,0:T(8,128)(2,1)S(1)}, bf16[768,256]{1,0:T(8,128)(2,1)S(1)}, u32[]{:S(2)}, u32[]{:S(2)}) collective-permute-start(bf16[768,256]{1,0:T(8,128)(2,1)S(1)} %shard_map.150.m0), channel_id=1, source_target_pairs={{0,1},{1,2},{2,3},{3,0},{4,5},{5,6},{6,7},{7,4},{8,9},{9,10},{10,1... | collective-permute-start | bytes 1179656 | tf_op jit(solution)/shard_map/ppermute | solution.py:451
  70.6 11.9 %collective-permute-start.9 = (bf16[768,256]{1,0:T(8,128)(2,1)S(1)}, bf16[768,256]{1,0:T(8,128)(2,1)S(1)}, u32[]{:S(2)}, u32[]{:S(2)}) collective-permute-start(bf16[768,256]{1,0:T(8,128)(2,1)S(1)} %shard_map.150.m0), channel_id=1, source_target_pairs={{0,3},{1,0},{2,1},{3,2},{4,7},{5,4},{6,5},{7,6},{8,11},{9,8},{10,9... | collective-permute-start | bytes 1179656 | tf_op jit(solution)/shard_map/ppermute | solution.py:451
  78.4 4.6 %collective-permute-start.14 = (bf16[128,2048]{1,0:T(8,128)(2,1)S(1)}, bf16[128,2048]{1,0:T(8,128)(2,1)S(1)}, u32[]{:S(2)}, u32[]{:S(2)}) collective-permute-start(bf16[128,2048]{1,0:T(8,128)(2,1)S(1)} %collective-permute-done.11.got1), channel_id=1, source_target_pairs={{0,4},{4,0},{1,5},{5,1},{2,6},{6,2},{3,7},{7,3},{8,12},{12,8},{9,1... | collective-permute-start | bytes 1572872 | tf_op jit(solution)/shard_map/ppermute | solution.py:453
  82.5 1.9 %collective-permute-start.15 = (bf16[128,2048]{1,0:T(8,128)(2,1)S(1)}, bf16[128,2048]{1,0:T(8,128)(2,1)S(1)}, u32[]{:S(2)}, u32[]{:S(2)}) collective-permute-start(bf16[128,2048]{1,0:T(8,128)(2,1)S(1)} %collective-permute-done.12.got2), channel_id=1, source_target_pairs={{0,4},{4,0},{1,5},{5,1},{2,6},{6,2},{3,7},{7,3},{8,12},{12,8},{9,1... | collective-permute-start | bytes 1572872 | tf_op jit(solution)/shard_map/ppermute | solution.py:453
  82.5 2.7 %collective-permute-start.16 = (bf16[128,2048]{1,0:T(8,128)(2,1)S(1)}, bf16[128,2048]{1,0:T(8,128)(2,1)S(1)}, u32[]{:S(2)}, u32[]{:S(2)}) collective-permute-start(bf16[128,2048]{1,0:T(8,128)(2,1)S(1)} %collective-permute-done.13.got3), channel_id=1, source_target_pairs={{0,4},{4,0},{1,5},{5,1},{2,6},{6,2},{3,7},{7,3},{8,12},{12,8},{9,1... | collective-permute-start | bytes 1572872 | tf_op jit(solution)/shard_map/ppermute | solution.py:453
  92.5 25.8 %copy-start.12 = (bf16[3,1408]{1,0:T(4,128)(2,1)S(1)}, bf16[3,1408]{1,0:T(4,128)(2,1)}, u32[]{:S(2)}) copy-start(bf16[3,1408]{1,0:T(4,128)(2,1)} %tg_ref.5) | copy-start | bytes 25348
  92.5 25.7 %copy-start.13 = (bf16[3,1408]{1,0:T(4,128)(2,1)S(1)}, bf16[3,1408]{1,0:T(4,128)(2,1)}, u32[]{:S(2)}) copy-start(bf16[3,1408]{1,0:T(4,128)(2,1)} %tv_ref.5) | copy-start | bytes 25348
  92.5 8.9 %collective-permute-start.17 = (bf16[16,2048]{1,0:T(8,128)(2,1)S(1)}, bf16[16,2048]{1,0:T(8,128)(2,1)S(1)}, u32[]{:S(2)}, u32[]{:S(2)}) collective-permute-start(bf16[16,2048]{1,0:T(8,128)(2,1)S(1)} %get-tuple-element.32), channel_id=1, source_target_pairs={{0,4},{4,8},{8,12},{12,16},{16,20},{20,24},{24,28},{28,32},{32,36}... | collective-permute-start | bytes 196616 | tf_op jit(solution)/shard_map/ppermute | solution.py:465
  94.5 21.1 %collective-permute-start.25 = (bf16[4,3,64,1408]{3,2,1,0:T(8,128)(2,1)S(1)}, bf16[4,3,64,1408]{3,2,1,0:T(8,128)(2,1)S(1)}, u32[]{:S(2)}, u32[]{:S(2)}) collective-permute-start(bf16[4,3,64,1408]{3,2,1,0:T(8,128)(2,1)S(1)} %pad_maximum_fusion.refs_0_), channel_id=1, source_target_pairs={{0,4},{4,0},{1,5},{5,1},{2,6},{6,2},{3,7},{7,3},{8,12},{12,8},{9,1... | collective-permute-start | bytes 6488072 | tf_op jit(solution)/shard_map/ppermute | solution.py:452
  95.9 15.2 %collective-permute-start.23 = (bf16[2,3,64,1408]{3,2,1,0:T(8,128)(2,1)S(1)}, bf16[2,3,64,1408]{3,2,1,0:T(8,128)(2,1)S(1)}, u32[]{:S(2)}, u32[]{:S(2)}) collective-permute-start(bf16[2,3,64,1408]{3,2,1,0:T(8,128)(2,1)S(1)} %slice.8), channel_id=1, source_target_pairs={{0,8},{4,36},{8,16},{12,44},{16,24},{20,52},{24,0},{28,60},{32,40}... | collective-permute-start | bytes 3244040 | tf_op jit(solution)/shard_map/ppermute | solution.py:455
  99.1 16.4 %collective-permute-start.24 = (bf16[2,3,64,1408]{3,2,1,0:T(8,128)(2,1)S(1)}, bf16[2,3,64,1408]{3,2,1,0:T(8,128)(2,1)S(1)}, u32[]{:S(2)}, u32[]{:S(2)}) collective-permute-start(bf16[2,3,64,1408]{3,2,1,0:T(8,128)(2,1)S(1)} %slice.9), channel_id=1, source_target_pairs={{0,24},{4,100},{8,0},{12,108},{16,8},{20,116},{24,16},{28,124},{32... | collective-permute-start | bytes 3244040 | tf_op jit(solution)/shard_map/ppermute | solution.py:456
  99.4 18.8 %collective-permute-start.26 = (bf16[4,3,64,1408]{3,2,1,0:T(8,128)(2,1)}, bf16[4,3,64,1408]{3,2,1,0:T(8,128)(2,1)S(1)}, u32[]{:S(2)}, u32[]{:S(2)}) collective-permute-start(bf16[4,3,64,1408]{3,2,1,0:T(8,128)(2,1)} %collective-permute-done.21.refs_1_), channel_id=1, source_target_pairs={{0,4},{4,0},{1,5},{5,1},{2,6},{6,2},{3,7},{7,3},{8,12},{12,8},{9,1... | collective-permute-start | bytes 6488072 | tf_op jit(solution)/shard_map/ppermute | solution.py:458
  101.4 16.8 %collective-permute-start.27 = (bf16[4,3,64,1408]{3,2,1,0:T(8,128)(2,1)}, bf16[4,3,64,1408]{3,2,1,0:T(8,128)(2,1)S(1)}, u32[]{:S(2)}, u32[]{:S(2)}) collective-permute-start(bf16[4,3,64,1408]{3,2,1,0:T(8,128)(2,1)} %collective-permute-done.22.refs_2_), channel_id=1, source_target_pairs={{0,4},{4,0},{1,5},{5,1},{2,6},{6,2},{3,7},{7,3},{8,12},{12,8},{9,1... | collective-permute-start | bytes 6488072 | tf_op jit(solution)/shard_map/ppermute | solution.py:458
  111.2 4.5 %collective-permute-start.28 = (bf16[2,3,64,1408]{3,2,1,0:T(8,128)(2,1)S(1)}, bf16[2,3,64,1408]{3,2,1,0:T(8,128)(2,1)S(1)}, u32[]{:S(2)}, u32[]{:S(2)}) collective-permute-start(bf16[2,3,64,1408]{3,2,1,0:T(8,128)(2,1)S(1)} %collective-permute-done.23.refs_3_), channel_id=1, source_target_pairs={{0,4},{4,0},{1,5},{5,1},{2,6},{6,2},{3,7},{7,3},{8,12},{12,8},{9,1... | collective-permute-start | bytes 3244040 | tf_op jit(solution)/shard_map/ppermute | solution.py:466
  115.5 2.7 %collective-permute-start.29 = (bf16[2,3,64,1408]{3,2,1,0:T(8,128)(2,1)S(1)}, bf16[2,3,64,1408]{3,2,1,0:T(8,128)(2,1)S(1)}, u32[]{:S(2)}, u32[]{:S(2)}) collective-permute-start(bf16[2,3,64,1408]{3,2,1,0:T(8,128)(2,1)S(1)} %collective-permute-done.24.refs_4_), channel_id=1, source_target_pairs={{0,4},{4,0},{1,5},{5,1},{2,6},{6,2},{3,7},{7,3},{8,12},{12,8},{9,1... | collective-permute-start | bytes 3244040 | tf_op jit(solution)/shard_map/ppermute | solution.py:466
  125.4 17.1 %collective-permute-start.30 = (bf16[192,1024]{1,0:T(8,128)(2,1)S(1)}, bf16[192,1024]{1,0:T(8,128)(2,1)S(1)}, u32[]{:S(2)}, u32[]{:S(2)}) collective-permute-start(bf16[192,1024]{1,0:T(8,128)(2,1)S(1)} %get-tuple-element.36), channel_id=1, source_target_pairs={{0,1},{1,2},{2,3},{3,0},{4,5},{5,6},{6,7},{7,4},{8,9},{9,10},{10,1... | collective-permute-start | bytes 1179656 | tf_op jit(solution)/shard_map/ppermute | solution.py:471
  125.6 16.9 %collective-permute-start.31 = (bf16[192,1024]{1,0:T(8,128)(2,1)S(1)}, bf16[192,1024]{1,0:T(8,128)(2,1)S(1)}, u32[]{:S(2)}, u32[]{:S(2)}) collective-permute-start(bf16[192,1024]{1,0:T(8,128)(2,1)S(1)} %get-tuple-element.38), channel_id=1, source_target_pairs={{0,3},{1,0},{2,1},{3,2},{4,7},{5,4},{6,5},{7,6},{8,11},{9,8},{10,9... | collective-permute-start | bytes 1179656 | tf_op jit(solution)/shard_map/ppermute | solution.py:472
  139.2 13.9 %collective-permute-start.33 = (bf16[192,1024]{1,0:T(8,128)(2,1)S(1)}, bf16[192,1024]{1,0:T(8,128)(2,1)S(1)}, u32[]{:S(2)}, u32[]{:S(2)}) collective-permute-start(bf16[192,1024]{1,0:T(8,128)(2,1)S(1)} %get-tuple-element.40), channel_id=1, source_target_pairs={{0,1},{1,2},{2,3},{3,0},{4,5},{5,6},{6,7},{7,4},{8,9},{9,10},{10,1... | collective-permute-start | bytes 1179656 | tf_op jit(solution)/shard_map/ppermute | solution.py:476
  139.3 13.8 %collective-permute-start.34 = (bf16[192,1024]{1,0:T(8,128)(2,1)S(1)}, bf16[192,1024]{1,0:T(8,128)(2,1)S(1)}, u32[]{:S(2)}, u32[]{:S(2)}) collective-permute-start(bf16[192,1024]{1,0:T(8,128)(2,1)S(1)} %get-tuple-element.41), channel_id=1, source_target_pairs={{0,3},{1,0},{2,1},{3,2},{4,7},{5,4},{6,5},{7,6},{8,11},{9,8},{10,9... | collective-permute-start | bytes 1179656 | tf_op jit(solution)/shard_map/ppermute | solution.py:477
  142.6 16.9 %collective-permute-start.32 = (bf16[192,1024]{1,0:T(8,128)(2,1)S(1)}, bf16[192,1024]{1,0:T(8,128)(2,1)S(1)}, u32[]{:S(2)}, u32[]{:S(2)}) collective-permute-start(bf16[192,1024]{1,0:T(8,128)(2,1)S(1)} %get-tuple-element.39), channel_id=1, source_target_pairs={{0,1},{1,2},{2,3},{3,0},{4,5},{5,6},{6,7},{7,4},{8,9},{9,10},{10,1... | collective-permute-start | bytes 1179656 | tf_op jit(solution)/shard_map/ppermute | solution.py:481
  142.7 16.8 %collective-permute-start.35 = (bf16[192,1024]{1,0:T(8,128)(2,1)S(1)}, bf16[192,1024]{1,0:T(8,128)(2,1)S(1)}, u32[]{:S(2)}, u32[]{:S(2)}) collective-permute-start(bf16[192,1024]{1,0:T(8,128)(2,1)S(1)} %get-tuple-element.42), channel_id=1, source_target_pairs={{0,3},{1,0},{2,1},{3,2},{4,7},{5,4},{6,5},{7,6},{8,11},{9,8},{10,9... | collective-permute-start | bytes 1179656 | tf_op jit(solution)/shard_map/ppermute | solution.py:482
  (6 other events, 5.0 us)

commit v4 on v3

--- a/solution.py
+++ b/solution.py
@@ -217,26 +217,38 @@
 ROWS = TOK // 4
 
 
-def attend_kernel(
-    m0, m1, m2, m3, own_w, got1, got2, got3, sib1, sib2, sib3, x_ref, gain_ref,
-    *refs,
+def place_rows(w_ref, got, sib):
+    c = lax.axis_index(C)
+    w_ref[pl.ds(pl.multiple_of(c * 128, 128), 128), :] = got[...]
+    w_ref[pl.ds(pl.multiple_of((1 - c) * 128, 128), 128), :] = sib[...]
+
+
+def attend_kernel(m0, m1, m2, own_w, got1, got2, sib1, sib2, x_ref, part_ref, w_ref):
+    w_ref[0] = own_w[...]
+    place_rows(w_ref.at[1], got1, sib1)
+    place_rows(w_ref.at[2], got2, sib2)
+
+    def block(n, _):
+        rows = pl.ds(pl.multiple_of(n * ROWS, ROWS), ROWS)
+        mixed = jnp.concatenate([m[rows, :] for m in (m0, m1, m2)], axis=1)
+        part_ref[rows, :] = x_ref[rows, :].astype(f32) + _dot(mixed, w_ref[...].reshape(768, D))
+        return 0
+
+    lax.fori_loop(0, 4, block, 0)
+
+
+def norm_kernel(
+    part_ref, early, late, got3, sib3, gain_ref, normed_ref, tail_ref, resid_ref, w_ref, n_ref
 ):
-    normed_ref, tail_ref, resid_ref, w_ref, n_ref = refs
-    c = lax.axis_index(C)
-    mine = pl.multiple_of(c * 128, 128)
-    theirs = pl.multiple_of((1 - c) * 128, 128)
-    w_ref[0] = own_w[...]
-    for j, (got, sib) in enumerate(((got1, sib1), (got2, sib2), (got3, sib3))):
-        w_ref[j + 1, pl.ds(mine, 128), :] = got[...]
-        w_ref[j + 1, pl.ds(theirs, 128), :] = sib[...]
+    place_rows(w_ref, got3, sib3)
     gain = gain_ref[...]
     xi = lax.axis_index(X)
-    w = w_ref[...].reshape(1024, D)
 
     def block(n, _):
         rows = pl.ds(pl.multiple_of(n * ROWS, ROWS), ROWS)
-        mixed = jnp.concatenate([m[rows, :] for m in (m0, m1, m2, m3)], axis=1)
-        acc = x_ref[rows, :].astype(f32) + _dot(mixed, w)
+        within = pl.ds(pl.multiple_of(lax.rem(n, 2) * ROWS, ROWS), ROWS)
+        mixed = jnp.where(n < 2, early[within, :], late[within, :])
+        acc = part_ref[rows, :] + _dot(mixed, w_ref[...])
 
         @pl.when(xi == n)
         def _():
@@ -260,7 +272,7 @@
 
 
 def feed_kernel(rels, plan, x_ref, halo_ref, tg_ref, tv_ref, *refs):
-    own, sib, refs = refs[:5], refs[5:10], refs[10:]
+    own, sib, refs = refs[:8], refs[8:16], refs[16:]
     out_refs, refs = refs[: len(plan)], refs[len(plan) :]
     xs_ref, hf_ref, hs_ref, g_ref, h_ref = refs
     hf_ref[...] = halo_ref[...].astype(f32)
@@ -307,7 +319,7 @@
     mix_columns(len(CHUNKS) - 1)
     for half, arrays in enumerate((own, sib)):
         rows = blocks(arrays, 2, slice(0, HID))
-        for n, w in enumerate((rows[:2], rows[2:])):
+        for n, w in enumerate((rows[:4], rows[4:])):
             new = _dot(h_ref[...], jnp.concatenate(w, axis=0), NT)
             cols = slice(n * 512, n * 512 + 512)
             for (block, want), out_ref in zip(plan, out_refs):
@@ -379,7 +391,7 @@
     return pl.pallas_call(
         functools.partial(feed_kernel, rels, plan),
         out_shape=[shape(ROWS, 1024, dtype=d) for d in dtypes],
-        in_specs=[VMEM] * 14,
+        in_specs=[VMEM] * 20,
         out_specs=[VMEM for _ in plan],
         scratch_shapes=[
             pltpu.VMEM((rows, D), bf16),
@@ -442,29 +454,36 @@
     along_z = [lax.ppermute(plane, SP, by_first_core(s)) for s in (1, 2, 3)]
     entering = call(enter_kernel, shape(128, 128, dtype=f32), 4, _cost(1e5, 3e5))(*along_z, before)
     given = lax.ppermute(entering, C, [(0, 1)])
-    stack = jnp.stack([shard, *first], axis=0)
-    sides = [lax.ppermute(stack, SP, around(s, True)) for s in (1, 3)]
+    stacks = [jnp.stack([shard, first[0]], axis=0), jnp.stack(first[1:], axis=0)]
+    right, left = around(1, True), around(3, True)
+    right_a = lax.ppermute(stacks[0], SP, right)
+    left_b = lax.ppermute(stacks[1], SP, left)
+    right_b = lax.ppermute(stacks[1], SP, right)
+    left_a = lax.ppermute(stacks[0], SP, left)
     mixed = call(
         finish_kernel, shape(TOK, 256), 7, _cost(2 * TOK * 128 * 256, 3e6)
     )(mech, q_shard, entering, given, other, switch, head_gain.reshape(1, DV))
 
-    mixed_got = [lax.ppermute(mixed, X, ring(s)) for s in steps]
-    sib_stack = lax.ppermute(stack, C, swap)
+    from_left, from_right = lax.ppermute(mixed, X, ring(1)), lax.ppermute(mixed, X, ring(3))
+    opposite = [
+        lax.ppermute(from_left[: TOK // 2], X, ring(1)),
+        lax.ppermute(from_right[TOK // 2 :], X, ring(3)),
+    ]
     w_sib = [lax.ppermute(w, C, swap) for w in w_got]
-    far = [
-        lax.ppermute(sides[0][:2], SP, around(1, True)),
-        lax.ppermute(sides[1][2:], SP, around(3, True)),
-    ]
-    sib_sides = [lax.ppermute(w, C, swap) for w in sides]
+    far = [lax.ppermute(right_a, SP, right), lax.ppermute(left_b, SP, left)]
+    mine = [*stacks, right_a, right_b, left_a, left_b, *far]
+    pieces = mine + [lax.ppermute(w, C, swap) for w in mine]
+    (part,) = call(
+        attend_kernel, [shape(TOK, D, dtype=f32)], 9,
+        _cost(2 * TOK * 768 * D, 1.2e7), [pltpu.VMEM((3, 256, D), bf16)], ATTEND_MIB,
+    )(mixed, from_left, from_right, w_out, *w_got[:2], *w_sib[:2], x)
     normed, tail, resid = call(
-        attend_kernel,
-        (shape(TOK, D), shape(HALO, D), shape(ROWS, D, dtype=f32)), 13,
-        _cost(2 * TOK * 1024 * D, 1.2e7),
-        [pltpu.VMEM((4, 256, D), bf16), pltpu.VMEM((ROWS, D), f32)], ATTEND_MIB,
-    )(mixed, *mixed_got, w_out, *w_got, *w_sib, x, ff_gain.reshape(1, D))
+        norm_kernel,
+        (shape(TOK, D), shape(HALO, D), shape(ROWS, D, dtype=f32)), 6,
+        _cost(2 * TOK * 256 * D, 1.2e7),
+        [pltpu.VMEM((256, D), bf16), pltpu.VMEM((ROWS, D), f32)], ATTEND_MIB,
+    )(part, *opposite, w_got[2], w_sib[2], ff_gain.reshape(1, D))
     halo = lax.ppermute(tail, SP, [(i, i + 1) for i in range(31)])
-    sib_far = [lax.ppermute(w, C, swap) for w in far]
-    pieces = [stack, *sides, *far, sib_stack, *sib_sides, *sib_far]
 
     feeds = functools.partial(feed, normed, halo, t_gate, t_value, pieces)
     opp_a, opp_b = feeds((2,), ((0, 0), (0, 1)), (bf16, bf16))

time: 162 us -> 169 us (1.043)
  the two profiles are of different devices: /device:TPU:24 before, /device:TPU:6 now
where the time goes in v4:
time: 169 us
  waiting for transfers between devices  74.8 us (44%)
  starting transfers between devices  56.4 us (33%)
  Pallas kernels  32.1 us (19%)
  local copies, waits for them, and re-layouts  4.71 us (3%)
    pallas_call x3, Pallas kernels, feed(): pl.pallas_call(functools.partial(feed_kernel, rels, plan), out_shape=[sha...  18.5 us
    ppermute x3, starting transfers between devices, per_device(): along_z = [lax.ppermute(plane, SP, by_first_core(s)) for s in (1, 2, 3)]  16.8 us
    ppermute x2, waiting for transfers between devices, per_device(): far = [lax.ppermute(right_a, SP, right), lax.ppermute(left_b, SP, left)]  13.5 us
    ppermute x1, waiting for transfers between devices, per_device(): lax.ppermute(mixed, X, ring(3))  12.7 us
    ppermute x1, waiting for transfers between devices, per_device(): right_b = lax.ppermute(stacks[1], SP, right)  8.59 us
    ppermute x1, waiting for transfers between devices, per_device(): lax.ppermute(mixed, X, ring(1))  8.42 us
    ppermute x3, waiting for transfers between devices, per_device(): along_z = [lax.ppermute(plane, SP, by_first_core(s)) for s in (1, 2, 3)]  5.21 us
    ppermute x3, starting transfers between devices, per_device(): along_y = [lax.ppermute(chip, Y, ring(s)) for s in (3, 2, 1)]  4.69 us
  transfers between devices with their start and end apart: 42, of which 21 were waited for; matrix products, arithmetic and copies ran while one was open for 1% of the time, Pallas kernels for 14%

profile of v4, /device:TPU:6, one launch (start us, length us, event | category | flops | bytes accessed | tf_op | source)
XLA Modules:
  0.0 168.8 jit_solution(17377302583359763071)
XLA Ops:
  0.0 1.0 copy-done.2
  1.0 0.9 copy-done.4
  1.9 0.9 copy-done.8
  3.5 1.9 %shard_map.145 = (f32[768,128]{1,0:T(8,128)S(1)}, f32[136,128]{1,0:T(8,128)S(1)}) custom-call(bf16[768,128]{1,0:T(8,128)(2,1)S(1)} %copy-done.8, f32[6,128]{1,0:T(8,128)S(1)} %bitcast.14, bf16[768,128]{1,0:T(8,128)(2,1)S(1)} %copy-done.4, bf16[768,256]{1,0:T(8,128)(2,1)S(1)} %copy-done.2), custom_call_target="tpu_custom_call" | custom-call | flops 50331648 | bytes 1000000 | tf_op jit(solution)/shard_map/pallas_call | solution.py:430
  5.5 1.2 collective-permute-done.other_ref
  6.8 3.1 %collective-permute-start.1 = (f32[136,128]{1,0:T(8,128)S(1)}, f32[136,128]{1,0:T(8,128)S(1)}, u32[]{:S(2)}, u32[]{:S(2)}) collective-permute-start(f32[136,128]{1,0:T(8,128)S(1)} %shard_map.147.own_ref), channel_id=1, source_target_pairs={{0,24},{8,0},{16,8},{24,16},{1,25},{9,1},{17,9},{25,17},{2,26},{10... | collective-permute-start | bytes 208904 | tf_op jit(solution)/shard_map/ppermute | solution.py:445
  10.5 1.0 collective-permute-start.3
  11.5 1.1 constant_dynamic-slice_fusion
  13.1 1.5 collective-permute-start.11
  14.7 1.4 collective-permute-done.2.opp_ref
  16.9 3.8 %collective-permute-start.4 = (f32[136,128]{1,0:T(8,128)S(1)}, f32[136,128]{1,0:T(8,128)S(1)}, u32[]{:S(2)}, u32[]{:S(2)}) collective-permute-start(f32[136,128]{1,0:T(8,128)S(1)} %get-tuple-element.28), channel_id=1, source_target_pairs={{0,32},{8,40},{16,48},{24,56},{32,64},{40,72},{48,80},{56,88},{64,... | collective-permute-start | bytes 208904 | tf_op jit(solution)/shard_map/ppermute | solution.py:454
  20.9 3.7 %collective-permute-start.21 = (bf16[3,64,1408]{2,1,0:T(8,128)(2,1)S(1)}, bf16[3,64,1408]{2,1,0:T(8,128)(2,1)S(1)}, u32[]{:S(2)}, u32[]{:S(2)}) collective-permute-start(bf16[3,64,1408]{2,1,0:T(8,128)(2,1)S(1)} %get-tuple-element.44), channel_id=1, source_target_pairs={{0,64},{4,20},{8,72},{12,28},{16,80},{20,4},{24,88},{28,12},{32,96... | collective-permute-start | bytes 1622024 | tf_op jit(solution)/shard_map/ppermute | solution.py:428
  24.5 1.0 collective-permute-start.20
  25.5 3.3 %collective-permute-start.5 = (f32[136,128]{1,0:T(8,128)S(1)}, f32[136,128]{1,0:T(8,128)S(1)}, u32[]{:S(2)}, u32[]{:S(2)}) collective-permute-start(f32[136,128]{1,0:T(8,128)S(1)} %get-tuple-element.28), channel_id=1, source_target_pairs={{0,64},{8,72},{16,80},{24,88},{32,96},{40,104},{48,112},{56,120},{... | collective-permute-start | bytes 208904 | tf_op jit(solution)/shard_map/ppermute | solution.py:454
  28.9 3.3 %collective-permute-done.5.z2_ref = f32[136,128]{1,0:T(8,128)S(1)} collective-permute-done((f32[136,128]{1,0:T(8,128)S(1)}, f32[136,128]{1,0:T(8,128)S(1)}, u32[]{:S(2)}, u32[]{:S(2)}) %collective-permute-start.5) | collective-permute-done | bytes 69664 | tf_op jit(solution)/shard_map/ppermute | solution.py:454
  32.1 9.6 %collective-permute-start.6 = (f32[136,128]{1,0:T(8,128)S(1)}, f32[136,128]{1,0:T(8,128)S(1)}, u32[]{:S(2)}, u32[]{:S(2)}) collective-permute-start(f32[136,128]{1,0:T(8,128)S(1)} %get-tuple-element.28), channel_id=1, source_target_pairs={{0,96},{8,104},{16,112},{24,120},{1,97},{9,105},{17,113},{25,121},... | collective-permute-start | bytes 208904 | tf_op jit(solution)/shard_map/ppermute | solution.py:454
  41.8 1.9 %collective-permute-done.6.z3_ref = f32[136,128]{1,0:T(8,128)S(1)} collective-permute-done((f32[136,128]{1,0:T(8,128)S(1)}, f32[136,128]{1,0:T(8,128)S(1)}, u32[]{:S(2)}, u32[]{:S(2)}) %collective-permute-start.6) | collective-permute-done | bytes 69664 | tf_op jit(solution)/shard_map/ppermute | solution.py:454
  43.7 1.3 collective-permute-start.7
  45.9 1.5 shard_map.146
  48.7 1.5 collective-permute-start.9
  50.2 1.4 collective-permute-start.16
  51.7 8.4 %collective-permute-done.8.m1 = bf16[768,256]{1,0:T(8,128)(2,1)S(1)} collective-permute-done((bf16[768,256]{1,0:T(8,128)(2,1)S(1)}, bf16[768,256]{1,0:T(8,128)(2,1)S(1)}, u32[]{:S(2)}, u32[]{:S(2)}) %collective-permute-start.8) | collective-permute-done | bytes 393248 | tf_op jit(solution)/shard_map/ppermute | solution.py:467
  60.2 12.7 %collective-permute-done.9.m2 = bf16[768,256]{1,0:T(8,128)(2,1)S(1)} collective-permute-done((bf16[768,256]{1,0:T(8,128)(2,1)S(1)}, bf16[768,256]{1,0:T(8,128)(2,1)S(1)}, u32[]{:S(2)}, u32[]{:S(2)}) %collective-permute-start.9) | collective-permute-done | bytes 393248 | tf_op jit(solution)/shard_map/ppermute | solution.py:467
  72.9 2.1 %collective-permute-start.15 = (bf16[384,256]{1,0:T(8,128)(2,1)S(1)}, bf16[384,256]{1,0:T(8,128)(2,1)S(1)}, u32[]{:S(2)}, u32[]{:S(2)}) collective-permute-start(bf16[384,256]{1,0:T(8,128)(2,1)S(1)} %slice.9), channel_id=1, source_target_pairs={{0,3},{1,0},{2,1},{3,2},{4,7},{5,4},{6,5},{7,6},{8,11},{9,8},{10,9... | collective-permute-start | bytes 589832 | tf_op jit(solution)/shard_map/ppermute | solution.py:470
  75.2 4.4 %collective-permute-done.14.early = bf16[384,256]{1,0:T(8,128)(2,1)S(1)} collective-permute-done((bf16[384,256]{1,0:T(8,128)(2,1)S(1)}, bf16[384,256]{1,0:T(8,128)(2,1)S(1)}, u32[]{:S(2)}, u32[]{:S(2)}) %collective-permute-start.14) | collective-permute-done | bytes 196640 | tf_op jit(solution)/shard_map/ppermute | solution.py:469
  79.6 1.3 collective-permute-done.15.late
  80.9 3.2 %collective-permute-start.24 = (bf16[2,3,64,1408]{3,2,1,0:T(8,128)(2,1)S(1)}, bf16[2,3,64,1408]{3,2,1,0:T(8,128)(2,1)S(1)}, u32[]{:S(2)}, u32[]{:S(2)}) collective-permute-start(bf16[2,3,64,1408]{3,2,1,0:T(8,128)(2,1)S(1)} %pad_maximum_fusion.refs_0_), channel_id=1, source_target_pairs={{0,24},{4,100},{8,0},{12,108},{16,8},{20,116},{24,16},{28,124},{32... | collective-permute-start | bytes 3244040 | tf_op jit(solution)/shard_map/ppermute | solution.py:462
  84.2 3.4 %shard_map.151.part_ref = f32[768,2048]{1,0:T(8,128)S(1)} custom-call(bf16[768,256]{1,0:T(8,128)(2,1)S(1)} %shard_map.150.m0, bf16[768,256]{1,0:T(8,128)(2,1)S(1)} %collective-permute-done.8.m1, bf16[768,256]{1,0:T(8,128)(2,1)S(1)} %collective-permute-done.9.m2, bf16[256,2048]{1,0:T(8,128)(2,1)S(1)} %copy-done.1, ...), custom_call_target="tpu_custom_call" | custom-call | flops 2415919104 | bytes 12000000 | tf_op jit(solution)/shard_map/pallas_call | solution.py:476
  87.6 4.3 %shard_map.152 = (bf16[768,2048]{1,0:T(8,128)(2,1)S(1)}, bf16[16,2048]{1,0:T(8,128)(2,1)S(1)}, f32[192,2048]{1,0:T(8,128)S(1)}) custom-call(f32[768,2048]{1,0:T(8,128)S(1)} %shard_map.151.part_ref, bf16[384,256]{1,0:T(8,128)(2,1)S(1)} %collective-permute-done.14.early, bf16[384,256]{1,0:T(8,128)(2,1)S(1)} %collective-permute-done.15.late, ...), custom_call_target="tpu_custom_call" | custom-call | flops 805306368 | bytes 12000000 | tf_op jit(solution)/shard_map/pallas_call | solution.py:480
  91.9 2.4 %collective-permute-start.18 = (bf16[16,2048]{1,0:T(8,128)(2,1)S(1)}, bf16[16,2048]{1,0:T(8,128)(2,1)S(1)}, u32[]{:S(2)}, u32[]{:S(2)}) collective-permute-start(bf16[16,2048]{1,0:T(8,128)(2,1)S(1)} %get-tuple-element.32), channel_id=1, source_target_pairs={{0,4},{4,8},{8,12},{12,16},{16,20},{20,24},{24,28},{28,32},{32,36}... | collective-permute-start | bytes 196616 | tf_op jit(solution)/shard_map/ppermute | solution.py:486
  95.2 1.0 collective-permute-start.29
  96.3 3.4 %collective-permute-start.27 = (bf16[2,3,64,1408]{3,2,1,0:T(8,128)(2,1)S(1)}, bf16[2,3,64,1408]{3,2,1,0:T(8,128)(2,1)S(1)}, u32[]{:S(2)}, u32[]{:S(2)}) collective-permute-start(bf16[2,3,64,1408]{3,2,1,0:T(8,128)(2,1)S(1)} %collective-permute-done.25.refs_5_), channel_id=1, source_target_pairs={{0,24},{4,100},{8,0},{12,108},{16,8},{20,116},{24,16},{28,124},{32... | collective-permute-start | bytes 3244040 | tf_op jit(solution)/shard_map/ppermute | solution.py:473
  99.6 8.6 %collective-permute-done.23.refs_3_ = bf16[2,3,64,1408]{3,2,1,0:T(8,128)(2,1)S(1)} collective-permute-done((bf16[2,3,64,1408]{3,2,1,0:T(8,128)(2,1)S(1)}, bf16[2,3,64,1408]{3,2,1,0:T(8,128)(2,1)S(1)}, u32[]{:S(2)}, u32[]{:S(2)}) %collective-permute-start.23) | collective-permute-done | bytes 1081376 | tf_op jit(solution)/shard_map/ppermute | solution.py:461
  108.9 4.7 %collective-permute-done.27.refs_7_ = bf16[2,3,64,1408]{3,2,1,0:T(8,128)(2,1)S(1)} collective-permute-done((bf16[2,3,64,1408]{3,2,1,0:T(8,128)(2,1)S(1)}, bf16[2,3,64,1408]{3,2,1,0:T(8,128)(2,1)S(1)}, u32[]{:S(2)}, u32[]{:S(2)}) %collective-permute-start.27) | collective-permute-done | bytes 1081376 | tf_op jit(solution)/shard_map/ppermute | solution.py:473
  113.5 2.2 %collective-permute-start.32 = (bf16[2,3,64,1408]{3,2,1,0:T(8,128)(2,1)S(1)}, bf16[2,3,64,1408]{3,2,1,0:T(8,128)(2,1)S(1)}, u32[]{:S(2)}, u32[]{:S(2)}) collective-permute-start(bf16[2,3,64,1408]{3,2,1,0:T(8,128)(2,1)S(1)} %collective-permute-done.24.refs_4_), channel_id=1, source_target_pairs={{0,4},{4,0},{1,5},{5,1},{2,6},{6,2},{3,7},{7,3},{8,12},{12,8},{9,1... | collective-permute-start | bytes 3244040 | tf_op jit(solution)/shard_map/ppermute | solution.py:475
  115.8 8.8 %collective-permute-done.26.refs_6_ = bf16[2,3,64,1408]{3,2,1,0:T(8,128)(2,1)S(1)} collective-permute-done((bf16[2,3,64,1408]{3,2,1,0:T(8,128)(2,1)S(1)}, bf16[2,3,64,1408]{3,2,1,0:T(8,128)(2,1)S(1)}, u32[]{:S(2)}, u32[]{:S(2)}) %collective-permute-start.26) | collective-permute-done | bytes 1081376 | tf_op jit(solution)/shard_map/ppermute | solution.py:473
  125.1 2.2 %collective-permute-done.35.refs_15_ = bf16[2,3,64,1408]{3,2,1,0:T(8,128)(2,1)S(1)} collective-permute-done((bf16[2,3,64,1408]{3,2,1,0:T(8,128)(2,1)S(1)}, bf16[2,3,64,1408]{3,2,1,0:T(8,128)(2,1)S(1)}, u32[]{:S(2)}, u32[]{:S(2)}) %collective-permute-start.35) | collective-permute-done | bytes 1081376 | tf_op jit(solution)/shard_map/ppermute | solution.py:475
  127.3 1.5 collective-permute-done.34.refs_14_
  128.9 5.1 %feed.5 = (bf16[192,1024]{1,0:T(8,128)(2,1)S(1)}, bf16[192,1024]{1,0:T(8,128)(2,1)S(1)}) custom-call(bf16[768,2048]{1,0:T(8,128)(2,1)S(1)} %get-tuple-element.31.x_ref, bf16[16,2048]{1,0:T(8,128)(2,1)S(1)} %collective-permute-done.18.halo_ref, bf16[3,1408]{1,0:T(4,128)(2,1)S(1)} %copy-done.9, bf16[3,1408]{1,0:T(4,128)(2,1)S(1)} %copy-done.10, ...), custom_call_target="tpu_custom_call" | custom-call | flops 3598712832 | bytes 17301504 | tf_op jit(solution)/shard_map/feed/pallas_call | solution.py:391
  134.0 1.6 collective-permute-start.36
  136.1 8.3 %feed.4 = (f32[192,1024]{1,0:T(8,128)S(1)}, bf16[192,1024]{1,0:T(8,128)(2,1)S(1)}, bf16[192,1024]{1,0:T(8,128)(2,1)S(1)}, f32[192,1024]{1,0:T(8,128)S(1)}) custom-call(bf16[768,2048]{1,0:T(8,128)(2,1)S(1)} %get-tuple-element.31.x_ref, bf16[16,2048]{1,0:T(8,128)(2,1)S(1)} %collective-permute-done.18.halo_ref, bf16[3,1408]{1,0:T(4,128)(2,1)S(1)} %copy-done.9, ...), custom_call_target="tpu_custom_call" | custom-call | flops 7197425664 | bytes 17301504 | tf_op jit(solution)/shard_map/feed/pallas_call | solution.py:391
  144.4 2.8 %collective-permute-start.39 = (bf16[192,1024]{1,0:T(8,128)(2,1)S(1)}, bf16[192,1024]{1,0:T(8,128)(2,1)S(1)}, u32[]{:S(2)}, u32[]{:S(2)}) collective-permute-start(bf16[192,1024]{1,0:T(8,128)(2,1)S(1)} %get-tuple-element.40), channel_id=1, source_target_pairs={{0,1},{1,2},{2,3},{3,0},{4,5},{5,6},{6,7},{7,4},{8,9},{9,10},{10,1... | collective-permute-start | bytes 1179656 | tf_op jit(solution)/shard_map/ppermute | solution.py:495
  147.8 2.8 %collective-permute-start.38 = (bf16[192,1024]{1,0:T(8,128)(2,1)S(1)}, bf16[192,1024]{1,0:T(8,128)(2,1)S(1)}, u32[]{:S(2)}, u32[]{:S(2)}) collective-permute-start(bf16[192,1024]{1,0:T(8,128)(2,1)S(1)} %get-tuple-element.39), channel_id=1, source_target_pairs={{0,1},{1,2},{2,3},{3,0},{4,5},{5,6},{6,7},{7,4},{8,9},{9,10},{10,1... | collective-permute-start | bytes 1179656 | tf_op jit(solution)/shard_map/ppermute | solution.py:500
  150.6 5.1 %feed.3 = (f32[192,1024]{1,0:T(8,128)S(1)}, f32[192,1024]{1,0:T(8,128)S(1)}) custom-call(bf16[768,2048]{1,0:T(8,128)(2,1)S(1)} %get-tuple-element.31.x_ref, bf16[16,2048]{1,0:T(8,128)(2,1)S(1)} %collective-permute-done.18.halo_ref, bf16[3,1408]{1,0:T(4,128)(2,1)S(1)} %copy-done.9, bf16[3,1408]{1,0:T(4,128)(2,1)S(1)} %copy-done.10, ...), custom_call_target="tpu_custom_call" | custom-call | flops 3598712832 | bytes 17301504 | tf_op jit(solution)/shard_map/feed/pallas_call | solution.py:391
  156.7 3.7 %collective-permute-done.40.r_a = bf16[192,1024]{1,0:T(8,128)(2,1)S(1)} collective-permute-done((bf16[192,1024]{1,0:T(8,128)(2,1)S(1)}, bf16[192,1024]{1,0:T(8,128)(2,1)S(1)}, u32[]{:S(2)}, u32[]{:S(2)}) %collective-permute-start.40) | collective-permute-done | bytes 393248 | tf_op jit(solution)/shard_map/ppermute | solution.py:496
  160.4 3.3 %collective-permute-done.38.l_a = bf16[192,1024]{1,0:T(8,128)(2,1)S(1)} collective-permute-done((bf16[192,1024]{1,0:T(8,128)(2,1)S(1)}, bf16[192,1024]{1,0:T(8,128)(2,1)S(1)}, u32[]{:S(2)}, u32[]{:S(2)}) %collective-permute-start.38) | collective-permute-done | bytes 393248 | tf_op jit(solution)/shard_map/ppermute | solution.py:500
  163.7 3.4 %collective-permute-done.41.r_b = bf16[192,1024]{1,0:T(8,128)(2,1)S(1)} collective-permute-done((bf16[192,1024]{1,0:T(8,128)(2,1)S(1)}, bf16[192,1024]{1,0:T(8,128)(2,1)S(1)}, u32[]{:S(2)}, u32[]{:S(2)}) %collective-permute-start.41) | collective-permute-done | bytes 393248 | tf_op jit(solution)/shard_map/ppermute | solution.py:501
  167.1 1.7 %shard_map.154 = bf16[192,2048]{1,0:T(8,128)(2,1)} custom-call(f32[192,2048]{1,0:T(8,128)S(1)} %get-tuple-element.30.resid_ref, f32[192,1024]{1,0:T(8,128)S(1)} %get-tuple-element.33.own_a, f32[192,1024]{1,0:T(8,128)S(1)} %get-tuple-element.34.own_b, bf16[192,1024]{1,0:T(8,128)(2,1)S(1)} %collective-permute-done.38.l_a, ...), custom_call_target="tpu_custom_call" | custom-call | flops 1000000 | bytes 5000000 | tf_op jit(solution)/shard_map/pallas_call | solution.py:503
  (89 shorter events, 9.5 us)
Async XLA Ops:
  5.4 1.3 collective-permute-start
  6.8 7.9 %collective-permute-start.1 = (f32[136,128]{1,0:T(8,128)S(1)}, f32[136,128]{1,0:T(8,128)S(1)}, u32[]{:S(2)}, u32[]{:S(2)}) collective-permute-start(f32[136,128]{1,0:T(8,128)S(1)} %shard_map.147.own_ref), channel_id=1, source_target_pairs={{0,24},{8,0},{16,8},{24,16},{1,25},{9,1},{17,9},{25,17},{2,26},{10... | collective-permute-start | bytes 208904 | tf_op jit(solution)/shard_map/ppermute | solution.py:445
  9.9 6.2 %collective-permute-start.2 = (f32[136,128]{1,0:T(8,128)S(1)}, f32[136,128]{1,0:T(8,128)S(1)}, u32[]{:S(2)}, u32[]{:S(2)}) collective-permute-start(f32[136,128]{1,0:T(8,128)S(1)} %shard_map.147.own_ref), channel_id=1, source_target_pairs={{0,16},{8,24},{16,0},{24,8},{1,17},{9,25},{17,1},{25,9},{2,18},{10... | collective-permute-start | bytes 208904 | tf_op jit(solution)/shard_map/ppermute | solution.py:445
  10.5 6.3 %collective-permute-start.3 = (f32[136,128]{1,0:T(8,128)S(1)}, f32[136,128]{1,0:T(8,128)S(1)}, u32[]{:S(2)}, u32[]{:S(2)}) collective-permute-start(f32[136,128]{1,0:T(8,128)S(1)} %shard_map.147.own_ref), channel_id=1, source_target_pairs={{0,8},{8,16},{16,24},{24,0},{1,9},{9,17},{17,25},{25,1},{2,10},{10... | collective-permute-start | bytes 208904 | tf_op jit(solution)/shard_map/ppermute | solution.py:445
  12.5 33.4 %copy-start.3 = (bf16[768,256]{1,0:T(8,128)(2,1)S(1)}, bf16[768,256]{1,0:T(8,128)(2,1)}, u32[]{:S(2)}) copy-start(bf16[768,256]{1,0:T(8,128)(2,1)} %v_ref.1) | copy-start | bytes 1179652
  12.5 33.4 %copy-start.5 = (bf16[768,128]{1,0:T(8,128)(2,1)S(1)}, bf16[768,128]{1,0:T(8,128)(2,1)}, u32[]{:S(2)}) copy-start(bf16[768,128]{1,0:T(8,128)(2,1)} %k_ref.1) | copy-start | bytes 589828
  12.6 33.4 %copy-start.7 = (bf16[768,128]{1,0:T(8,128)(2,1)S(1)}, bf16[768,128]{1,0:T(8,128)(2,1)}, u32[]{:S(2)}) copy-start(bf16[768,128]{1,0:T(8,128)(2,1)} %q_ref.1) | copy-start | bytes 589828
  12.6 35.5 %collective-permute-start.10 = (bf16[128,2048]{1,0:T(8,128)(2,1)S(1)}, bf16[128,2048]{1,0:T(8,128)(2,1)S(1)}, u32[]{:S(2)}, u32[]{:S(2)}) collective-permute-start(bf16[128,2048]{1,0:T(8,128)(2,1)S(1)} %constant_dynamic-slice_fusion), channel_id=1, source_target_pairs={{0,1},{1,2},{2,3},{3,0},{4,5},{5,6},{6,7},{7,4},{8,9},{9,10},{10,1... | collective-permute-start | bytes 1572872 | tf_op jit(solution)/shard_map/ppermute | solution.py:442
  13.1 35.5 %collective-permute-start.11 = (bf16[128,2048]{1,0:T(8,128)(2,1)S(1)}, bf16[128,2048]{1,0:T(8,128)(2,1)S(1)}, u32[]{:S(2)}, u32[]{:S(2)}) collective-permute-start(bf16[128,2048]{1,0:T(8,128)(2,1)S(1)} %constant_dynamic-slice_fusion), channel_id=1, source_target_pairs={{0,3},{1,0},{2,1},{3,2},{4,7},{5,4},{6,5},{7,6},{8,11},{9,8},{10,9... | collective-permute-start | bytes 1572872 | tf_op jit(solution)/shard_map/ppermute | solution.py:442
  16.9 8.7 %collective-permute-start.4 = (f32[136,128]{1,0:T(8,128)S(1)}, f32[136,128]{1,0:T(8,128)S(1)}, u32[]{:S(2)}, u32[]{:S(2)}) collective-permute-start(f32[136,128]{1,0:T(8,128)S(1)} %get-tuple-element.28), channel_id=1, source_target_pairs={{0,32},{8,40},{16,48},{24,56},{32,64},{40,72},{48,80},{56,88},{64,... | collective-permute-start | bytes 208904 | tf_op jit(solution)/shard_map/ppermute | solution.py:454
  20.9 29.4 %collective-permute-start.21 = (bf16[3,64,1408]{2,1,0:T(8,128)(2,1)S(1)}, bf16[3,64,1408]{2,1,0:T(8,128)(2,1)S(1)}, u32[]{:S(2)}, u32[]{:S(2)}) collective-permute-start(bf16[3,64,1408]{2,1,0:T(8,128)(2,1)S(1)} %get-tuple-element.44), channel_id=1, source_target_pairs={{0,64},{4,20},{8,72},{12,28},{16,80},{20,4},{24,88},{28,12},{32,96... | collective-permute-start | bytes 1622024 | tf_op jit(solution)/shard_map/ppermute | solution.py:428
  24.5 27.1 %collective-permute-start.20 = (bf16[3,64,1408]{2,1,0:T(8,128)(2,1)S(1)}, bf16[3,64,1408]{2,1,0:T(8,128)(2,1)S(1)}, u32[]{:S(2)}, u32[]{:S(2)}) collective-permute-start(bf16[3,64,1408]{2,1,0:T(8,128)(2,1)S(1)} %get-tuple-element.44), channel_id=1, source_target_pairs={{0,96},{4,28},{8,104},{12,4},{16,112},{20,12},{24,120},{28,20},{32... | collective-permute-start | bytes 1622024 | tf_op jit(solution)/shard_map/ppermute | solution.py:428
  25.5 6.6 %collective-permute-start.5 = (f32[136,128]{1,0:T(8,128)S(1)}, f32[136,128]{1,0:T(8,128)S(1)}, u32[]{:S(2)}, u32[]{:S(2)}) collective-permute-start(f32[136,128]{1,0:T(8,128)S(1)} %get-tuple-element.28), channel_id=1, source_target_pairs={{0,64},{8,72},{16,80},{24,88},{32,96},{40,104},{48,112},{56,120},{... | collective-permute-start | bytes 208904 | tf_op jit(solution)/shard_map/ppermute | solution.py:454
  32.1 11.6 %collective-permute-start.6 = (f32[136,128]{1,0:T(8,128)S(1)}, f32[136,128]{1,0:T(8,128)S(1)}, u32[]{:S(2)}, u32[]{:S(2)}) collective-permute-start(f32[136,128]{1,0:T(8,128)S(1)} %get-tuple-element.28), channel_id=1, source_target_pairs={{0,96},{8,104},{16,112},{24,120},{1,97},{9,105},{17,113},{25,121},... | collective-permute-start | bytes 208904 | tf_op jit(solution)/shard_map/ppermute | solution.py:454
  43.7 2.2 %collective-permute-start.7 = (f32[128,128]{1,0:T(8,128)S(1)}, f32[128,128]{1,0:T(8,128)S(1)}, u32[]{:S(2)}, u32[]{:S(2)}) collective-permute-start(f32[128,128]{1,0:T(8,128)S(1)} %shard_map.149.mine_ref), channel_id=1, source_target_pairs={{0,4},{1,5},{2,6},{3,7},{8,12},{9,13},{10,14},{11,15},{16,20},{17,... | collective-permute-start | bytes 196616 | tf_op jit(solution)/shard_map/ppermute | solution.py:456
  45.9 27.0 %collective-permute-start.19 = (bf16[3,64,1408]{2,1,0:T(8,128)(2,1)S(1)}, bf16[3,64,1408]{2,1,0:T(8,128)(2,1)S(1)}, u32[]{:S(2)}, u32[]{:S(2)}) collective-permute-start(bf16[3,64,1408]{2,1,0:T(8,128)(2,1)S(1)} %get-tuple-element.44), channel_id=1, source_target_pairs={{0,32},{4,12},{8,40},{12,20},{16,48},{20,28},{24,56},{28,4},{32,64... | collective-permute-start | bytes 1622024 | tf_op jit(solution)/shard_map/ppermute | solution.py:428
  48.1 12.1 %collective-permute-start.8 = (bf16[768,256]{1,0:T(8,128)(2,1)S(1)}, bf16[768,256]{1,0:T(8,128)(2,1)S(1)}, u32[]{:S(2)}, u32[]{:S(2)}) collective-permute-start(bf16[768,256]{1,0:T(8,128)(2,1)S(1)} %shard_map.150.m0), channel_id=1, source_target_pairs={{0,1},{1,2},{2,3},{3,0},{4,5},{5,6},{6,7},{7,4},{8,9},{9,10},{10,1... | collective-permute-start | bytes 1179656 | tf_op jit(solution)/shard_map/ppermute | solution.py:467
  48.7 24.2 %collective-permute-start.9 = (bf16[768,256]{1,0:T(8,128)(2,1)S(1)}, bf16[768,256]{1,0:T(8,128)(2,1)S(1)}, u32[]{:S(2)}, u32[]{:S(2)}) collective-permute-start(bf16[768,256]{1,0:T(8,128)(2,1)S(1)} %shard_map.150.m0), channel_id=1, source_target_pairs={{0,3},{1,0},{2,1},{3,2},{4,7},{5,4},{6,5},{7,6},{8,11},{9,8},{10,9... | collective-permute-start | bytes 1179656 | tf_op jit(solution)/shard_map/ppermute | solution.py:467
  50.2 24.9 %collective-permute-start.16 = (bf16[128,2048]{1,0:T(8,128)(2,1)S(1)}, bf16[128,2048]{1,0:T(8,128)(2,1)S(1)}, u32[]{:S(2)}, u32[]{:S(2)}) collective-permute-start(bf16[128,2048]{1,0:T(8,128)(2,1)S(1)} %constant_dynamic-slice_fusion), channel_id=1, source_target_pairs={{0,2},{1,3},{2,0},{3,1},{4,6},{5,7},{6,4},{7,5},{8,10},{9,11},{10,... | collective-permute-start | bytes 1572872 | tf_op jit(solution)/shard_map/ppermute | solution.py:442
  51.6 29.3 %collective-permute-start.12 = (bf16[128,2048]{1,0:T(8,128)(2,1)S(1)}, bf16[128,2048]{1,0:T(8,128)(2,1)S(1)}, u32[]{:S(2)}, u32[]{:S(2)}) collective-permute-start(bf16[128,2048]{1,0:T(8,128)(2,1)S(1)} %collective-permute-done.10.got1), channel_id=1, source_target_pairs={{0,4},{4,0},{1,5},{5,1},{2,6},{6,2},{3,7},{7,3},{8,12},{12,8},{9,1... | collective-permute-start | bytes 1572872 | tf_op jit(solution)/shard_map/ppermute | solution.py:472
  51.6 32.5 %copy-start = (bf16[768,2048]{1,0:T(8,128)(2,1)S(1)}, bf16[768,2048]{1,0:T(8,128)(2,1)}, u32[]{:S(2)}) copy-start(bf16[768,2048]{1,0:T(8,128)(2,1)} %x_ref.1) | copy-start | bytes 9437188
  60.2 24.0 %collective-permute-start.13 = (bf16[128,2048]{1,0:T(8,128)(2,1)S(1)}, bf16[128,2048]{1,0:T(8,128)(2,1)S(1)}, u32[]{:S(2)}, u32[]{:S(2)}) collective-permute-start(bf16[128,2048]{1,0:T(8,128)(2,1)S(1)} %collective-permute-done.11.got2), channel_id=1, source_target_pairs={{0,4},{4,0},{1,5},{5,1},{2,6},{6,2},{3,7},{7,3},{8,12},{12,8},{9,1... | collective-permute-start | bytes 1572872 | tf_op jit(solution)/shard_map/ppermute | solution.py:472
  72.9 6.7 %collective-permute-start.14 = (bf16[384,256]{1,0:T(8,128)(2,1)S(1)}, bf16[384,256]{1,0:T(8,128)(2,1)S(1)}, u32[]{:S(2)}, u32[]{:S(2)}) collective-permute-start(bf16[384,256]{1,0:T(8,128)(2,1)S(1)} %slice.8), channel_id=1, source_target_pairs={{0,1},{1,2},{2,3},{3,0},{4,5},{5,6},{6,7},{7,4},{8,9},{9,10},{10,1... | collective-permute-start | bytes 589832 | tf_op jit(solution)/shard_map/ppermute | solution.py:469
  72.9 8.0 %collective-permute-start.15 = (bf16[384,256]{1,0:T(8,128)(2,1)S(1)}, bf16[384,256]{1,0:T(8,128)(2,1)S(1)}, u32[]{:S(2)}, u32[]{:S(2)}) collective-permute-start(bf16[384,256]{1,0:T(8,128)(2,1)S(1)} %slice.9), channel_id=1, source_target_pairs={{0,3},{1,0},{2,1},{3,2},{4,7},{5,4},{6,5},{7,6},{8,11},{9,8},{10,9... | collective-permute-start | bytes 589832 | tf_op jit(solution)/shard_map/ppermute | solution.py:470
  75.1 21.1 %collective-permute-start.25 = (bf16[2,3,64,1408]{3,2,1,0:T(8,128)(2,1)S(1)}, bf16[2,3,64,1408]{3,2,1,0:T(8,128)(2,1)S(1)}, u32[]{:S(2)}, u32[]{:S(2)}) collective-permute-start(bf16[2,3,64,1408]{3,2,1,0:T(8,128)(2,1)S(1)} %pad_maximum_fusion.1.refs_1_), channel_id=1, source_target_pairs={{0,24},{4,100},{8,0},{12,108},{16,8},{20,116},{24,16},{28,124},{32... | collective-permute-start | bytes 3244040 | tf_op jit(solution)/shard_map/ppermute | solution.py:460
  79.6 16.7 %collective-permute-start.22 = (bf16[2,3,64,1408]{3,2,1,0:T(8,128)(2,1)S(1)}, bf16[2,3,64,1408]{3,2,1,0:T(8,128)(2,1)S(1)}, u32[]{:S(2)}, u32[]{:S(2)}) collective-permute-start(bf16[2,3,64,1408]{3,2,1,0:T(8,128)(2,1)S(1)} %pad_maximum_fusion.refs_0_), channel_id=1, source_target_pairs={{0,8},{4,36},{8,16},{12,44},{16,24},{20,52},{24,0},{28,60},{32,40}... | collective-permute-start | bytes 3244040 | tf_op jit(solution)/shard_map/ppermute | solution.py:459
  80.9 27.3 %collective-permute-start.23 = (bf16[2,3,64,1408]{3,2,1,0:T(8,128)(2,1)S(1)}, bf16[2,3,64,1408]{3,2,1,0:T(8,128)(2,1)S(1)}, u32[]{:S(2)}, u32[]{:S(2)}) collective-permute-start(bf16[2,3,64,1408]{3,2,1,0:T(8,128)(2,1)S(1)} %pad_maximum_fusion.1.refs_1_), channel_id=1, source_target_pairs={{0,8},{4,36},{8,16},{12,44},{16,24},{20,52},{24,0},{28,60},{32,40}... | collective-permute-start | bytes 3244040 | tf_op jit(solution)/shard_map/ppermute | solution.py:461
  80.9 27.3 %collective-permute-start.24 = (bf16[2,3,64,1408]{3,2,1,0:T(8,128)(2,1)S(1)}, bf16[2,3,64,1408]{3,2,1,0:T(8,128)(2,1)S(1)}, u32[]{:S(2)}, u32[]{:S(2)}) collective-permute-start(bf16[2,3,64,1408]{3,2,1,0:T(8,128)(2,1)S(1)} %pad_maximum_fusion.refs_0_), channel_id=1, source_target_pairs={{0,24},{4,100},{8,0},{12,108},{16,8},{20,116},{24,16},{28,124},{32... | collective-permute-start | bytes 3244040 | tf_op jit(solution)/shard_map/ppermute | solution.py:462
  84.2 3.4 %collective-permute-start.17 = (bf16[128,2048]{1,0:T(8,128)(2,1)S(1)}, bf16[128,2048]{1,0:T(8,128)(2,1)S(1)}, u32[]{:S(2)}, u32[]{:S(2)}) collective-permute-start(bf16[128,2048]{1,0:T(8,128)(2,1)S(1)} %collective-permute-done.16.got3), channel_id=1, source_target_pairs={{0,4},{4,0},{1,5},{5,1},{2,6},{6,2},{3,7},{7,3},{8,12},{12,8},{9,1... | collective-permute-start | bytes 1572872 | tf_op jit(solution)/shard_map/ppermute | solution.py:472
  87.6 41.3 %copy-start.9 = (bf16[3,1408]{1,0:T(4,128)(2,1)S(1)}, bf16[3,1408]{1,0:T(4,128)(2,1)}, u32[]{:S(2)}) copy-start(bf16[3,1408]{1,0:T(4,128)(2,1)} %tg_ref.5) | copy-start | bytes 25348
  87.6 41.2 %copy-start.10 = (bf16[3,1408]{1,0:T(4,128)(2,1)S(1)}, bf16[3,1408]{1,0:T(4,128)(2,1)}, u32[]{:S(2)}) copy-start(bf16[3,1408]{1,0:T(4,128)(2,1)} %tv_ref.5) | copy-start | bytes 25348
  91.9 3.3 %collective-permute-start.18 = (bf16[16,2048]{1,0:T(8,128)(2,1)S(1)}, bf16[16,2048]{1,0:T(8,128)(2,1)S(1)}, u32[]{:S(2)}, u32[]{:S(2)}) collective-permute-start(bf16[16,2048]{1,0:T(8,128)(2,1)S(1)} %get-tuple-element.32), channel_id=1, source_target_pairs={{0,4},{4,8},{8,12},{12,16},{16,20},{20,24},{24,28},{28,32},{32,36}... | collective-permute-start | bytes 196616 | tf_op jit(solution)/shard_map/ppermute | solution.py:486
  95.2 13.0 %collective-permute-start.29 = (bf16[2,3,64,1408]{3,2,1,0:T(8,128)(2,1)S(1)}, bf16[2,3,64,1408]{3,2,1,0:T(8,128)(2,1)S(1)}, u32[]{:S(2)}, u32[]{:S(2)}) collective-permute-start(bf16[2,3,64,1408]{3,2,1,0:T(8,128)(2,1)S(1)} %pad_maximum_fusion.1.refs_1_), channel_id=1, source_target_pairs={{0,4},{4,0},{1,5},{5,1},{2,6},{6,2},{3,7},{7,3},{8,12},{12,8},{9,1... | collective-permute-start | bytes 3244040 | tf_op jit(solution)/shard_map/ppermute | solution.py:475
  96.3 12.5 %collective-permute-start.28 = (bf16[2,3,64,1408]{3,2,1,0:T(8,128)(2,1)S(1)}, bf16[2,3,64,1408]{3,2,1,0:T(8,128)(2,1)S(1)}, u32[]{:S(2)}, u32[]{:S(2)}) collective-permute-start(bf16[2,3,64,1408]{3,2,1,0:T(8,128)(2,1)S(1)} %pad_maximum_fusion.refs_0_), channel_id=1, source_target_pairs={{0,4},{4,0},{1,5},{5,1},{2,6},{6,2},{3,7},{7,3},{8,12},{12,8},{9,1... | collective-permute-start | bytes 3244040 | tf_op jit(solution)/shard_map/ppermute | solution.py:475
  96.3 17.3 %collective-permute-start.27 = (bf16[2,3,64,1408]{3,2,1,0:T(8,128)(2,1)S(1)}, bf16[2,3,64,1408]{3,2,1,0:T(8,128)(2,1)S(1)}, u32[]{:S(2)}, u32[]{:S(2)}) collective-permute-start(bf16[2,3,64,1408]{3,2,1,0:T(8,128)(2,1)S(1)} %collective-permute-done.25.refs_5_), channel_id=1, source_target_pairs={{0,24},{4,100},{8,0},{12,108},{16,8},{20,116},{24,16},{28,124},{32... | collective-permute-start | bytes 3244040 | tf_op jit(solution)/shard_map/ppermute | solution.py:473
  108.2 16.4 %collective-permute-start.26 = (bf16[2,3,64,1408]{3,2,1,0:T(8,128)(2,1)S(1)}, bf16[2,3,64,1408]{3,2,1,0:T(8,128)(2,1)S(1)}, u32[]{:S(2)}, u32[]{:S(2)}) collective-permute-start(bf16[2,3,64,1408]{3,2,1,0:T(8,128)(2,1)S(1)} %collective-permute-done.22.refs_2_), channel_id=1, source_target_pairs={{0,8},{4,36},{8,16},{12,44},{16,24},{20,52},{24,0},{28,60},{32,40}... | collective-permute-start | bytes 3244040 | tf_op jit(solution)/shard_map/ppermute | solution.py:473
  108.3 16.4 %collective-permute-start.33 = (bf16[2,3,64,1408]{3,2,1,0:T(8,128)(2,1)S(1)}, bf16[2,3,64,1408]{3,2,1,0:T(8,128)(2,1)S(1)}, u32[]{:S(2)}, u32[]{:S(2)}) collective-permute-start(bf16[2,3,64,1408]{3,2,1,0:T(8,128)(2,1)S(1)} %collective-permute-done.25.refs_5_), channel_id=1, source_target_pairs={{0,4},{4,0},{1,5},{5,1},{2,6},{6,2},{3,7},{7,3},{8,12},{12,8},{9,1... | collective-permute-start | bytes 3244040 | tf_op jit(solution)/shard_map/ppermute | solution.py:475
  108.3 16.9 %collective-permute-start.30 = (bf16[2,3,64,1408]{3,2,1,0:T(8,128)(2,1)S(1)}, bf16[2,3,64,1408]{3,2,1,0:T(8,128)(2,1)S(1)}, u32[]{:S(2)}, u32[]{:S(2)}) collective-permute-start(bf16[2,3,64,1408]{3,2,1,0:T(8,128)(2,1)S(1)} %collective-permute-done.22.refs_2_), channel_id=1, source_target_pairs={{0,4},{4,0},{1,5},{5,1},{2,6},{6,2},{3,7},{7,3},{8,12},{12,8},{9,1... | collective-permute-start | bytes 3244040 | tf_op jit(solution)/shard_map/ppermute | solution.py:475
  108.8 16.4 %collective-permute-start.31 = (bf16[2,3,64,1408]{3,2,1,0:T(8,128)(2,1)S(1)}, bf16[2,3,64,1408]{3,2,1,0:T(8,128)(2,1)S(1)}, u32[]{:S(2)}, u32[]{:S(2)}) collective-permute-start(bf16[2,3,64,1408]{3,2,1,0:T(8,128)(2,1)S(1)} %collective-permute-done.23.refs_3_), channel_id=1, source_target_pairs={{0,4},{4,0},{1,5},{5,1},{2,6},{6,2},{3,7},{7,3},{8,12},{12,8},{9,1... | collective-permute-start | bytes 3244040 | tf_op jit(solution)/shard_map/ppermute | solution.py:475
  113.5 11.6 %collective-permute-start.32 = (bf16[2,3,64,1408]{3,2,1,0:T(8,128)(2,1)S(1)}, bf16[2,3,64,1408]{3,2,1,0:T(8,128)(2,1)S(1)}, u32[]{:S(2)}, u32[]{:S(2)}) collective-permute-start(bf16[2,3,64,1408]{3,2,1,0:T(8,128)(2,1)S(1)} %collective-permute-done.24.refs_4_), channel_id=1, source_target_pairs={{0,4},{4,0},{1,5},{5,1},{2,6},{6,2},{3,7},{7,3},{8,12},{12,8},{9,1... | collective-permute-start | bytes 3244040 | tf_op jit(solution)/shard_map/ppermute | solution.py:475
  124.6 2.7 %collective-permute-start.35 = (bf16[2,3,64,1408]{3,2,1,0:T(8,128)(2,1)S(1)}, bf16[2,3,64,1408]{3,2,1,0:T(8,128)(2,1)S(1)}, u32[]{:S(2)}, u32[]{:S(2)}) collective-permute-start(bf16[2,3,64,1408]{3,2,1,0:T(8,128)(2,1)S(1)} %collective-permute-done.27.refs_7_), channel_id=1, source_target_pairs={{0,4},{4,0},{1,5},{5,1},{2,6},{6,2},{3,7},{7,3},{8,12},{12,8},{9,1... | collective-permute-start | bytes 3244040 | tf_op jit(solution)/shard_map/ppermute | solution.py:475
  124.6 4.2 %collective-permute-start.34 = (bf16[2,3,64,1408]{3,2,1,0:T(8,128)(2,1)S(1)}, bf16[2,3,64,1408]{3,2,1,0:T(8,128)(2,1)S(1)}, u32[]{:S(2)}, u32[]{:S(2)}) collective-permute-start(bf16[2,3,64,1408]{3,2,1,0:T(8,128)(2,1)S(1)} %collective-permute-done.26.refs_6_), channel_id=1, source_target_pairs={{0,4},{4,0},{1,5},{5,1},{2,6},{6,2},{3,7},{7,3},{8,12},{12,8},{9,1... | collective-permute-start | bytes 3244040 | tf_op jit(solution)/shard_map/ppermute | solution.py:475
  134.0 13.2 %collective-permute-start.36 = (bf16[192,1024]{1,0:T(8,128)(2,1)S(1)}, bf16[192,1024]{1,0:T(8,128)(2,1)S(1)}, u32[]{:S(2)}, u32[]{:S(2)}) collective-permute-start(bf16[192,1024]{1,0:T(8,128)(2,1)S(1)} %get-tuple-element.36), channel_id=1, source_target_pairs={{0,1},{1,2},{2,3},{3,0},{4,5},{5,6},{6,7},{7,4},{8,9},{9,10},{10,1... | collective-permute-start | bytes 1179656 | tf_op jit(solution)/shard_map/ppermute | solution.py:490
  135.6 12.1 %collective-permute-start.37 = (bf16[192,1024]{1,0:T(8,128)(2,1)S(1)}, bf16[192,1024]{1,0:T(8,128)(2,1)S(1)}, u32[]{:S(2)}, u32[]{:S(2)}) collective-permute-start(bf16[192,1024]{1,0:T(8,128)(2,1)S(1)} %get-tuple-element.38), channel_id=1, source_target_pairs={{0,3},{1,0},{2,1},{3,2},{4,7},{5,4},{6,5},{7,6},{8,11},{9,8},{10,9... | collective-permute-start | bytes 1179656 | tf_op jit(solution)/shard_map/ppermute | solution.py:491
  144.4 12.3 %collective-permute-start.39 = (bf16[192,1024]{1,0:T(8,128)(2,1)S(1)}, bf16[192,1024]{1,0:T(8,128)(2,1)S(1)}, u32[]{:S(2)}, u32[]{:S(2)}) collective-permute-start(bf16[192,1024]{1,0:T(8,128)(2,1)S(1)} %get-tuple-element.40), channel_id=1, source_target_pairs={{0,1},{1,2},{2,3},{3,0},{4,5},{5,6},{6,7},{7,4},{8,9},{9,10},{10,1... | collective-permute-start | bytes 1179656 | tf_op jit(solution)/shard_map/ppermute | solution.py:495
  147.2 13.2 %collective-permute-start.40 = (bf16[192,1024]{1,0:T(8,128)(2,1)S(1)}, bf16[192,1024]{1,0:T(8,128)(2,1)S(1)}, u32[]{:S(2)}, u32[]{:S(2)}) collective-permute-start(bf16[192,1024]{1,0:T(8,128)(2,1)S(1)} %get-tuple-element.41), channel_id=1, source_target_pairs={{0,3},{1,0},{2,1},{3,2},{4,7},{5,4},{6,5},{7,6},{8,11},{9,8},{10,9... | collective-permute-start | bytes 1179656 | tf_op jit(solution)/shard_map/ppermute | solution.py:496
  147.8 15.9 %collective-permute-start.38 = (bf16[192,1024]{1,0:T(8,128)(2,1)S(1)}, bf16[192,1024]{1,0:T(8,128)(2,1)S(1)}, u32[]{:S(2)}, u32[]{:S(2)}) collective-permute-start(bf16[192,1024]{1,0:T(8,128)(2,1)S(1)} %get-tuple-element.39), channel_id=1, source_target_pairs={{0,1},{1,2},{2,3},{3,0},{4,5},{5,6},{6,7},{7,4},{8,9},{9,10},{10,1... | collective-permute-start | bytes 1179656 | tf_op jit(solution)/shard_map/ppermute | solution.py:500
  150.6 16.5 %collective-permute-start.41 = (bf16[192,1024]{1,0:T(8,128)(2,1)S(1)}, bf16[192,1024]{1,0:T(8,128)(2,1)S(1)}, u32[]{:S(2)}, u32[]{:S(2)}) collective-permute-start(bf16[192,1024]{1,0:T(8,128)(2,1)S(1)} %get-tuple-element.42), channel_id=1, source_target_pairs={{0,3},{1,0},{2,1},{3,2},{4,7},{5,4},{6,5},{7,6},{8,11},{9,8},{10,9... | collective-permute-start | bytes 1179656 | tf_op jit(solution)/shard_map/ppermute | solution.py:501
  (11 other events, 129.8 us)

commit v5 on v4

--- a/solution.py
+++ b/solution.py
@@ -267,6 +267,13 @@
     lax.fori_loop(0, 4, block, 0)
 
 
+def stack_kernel(own_ref, one_ref, two_ref, three_ref, near_ref, far_ref):
+    near_ref[0] = own_ref[...]
+    near_ref[1] = one_ref[...]
+    far_ref[0] = two_ref[...]
+    far_ref[1] = three_ref[...]
+
+
 SEG = HALO + ROWS
 CHUNKS = tuple((a, min(256, HID - a)) for a in range(0, HID, 256))
 
@@ -332,14 +339,14 @@
     out_m[...] = (m_ref[...] + am_ref[...].astype(f32)).astype(bf16)
 
 
-def last_kernel(resid_ref, own_a, own_b, l_a, l_b, r_a, r_b, out_ref):
+def add_in_order(base_ref, parts_a, parts_b, out_ref):
     first = lax.axis_index(C) == 0
     left = left_half()
 
     def total(g):
         cols = slice(g * 128, (g + 1) * 128)
-        a = own_a[:, cols] + l_a[:, cols].astype(f32) + r_a[:, cols].astype(f32)
-        b = own_b[:, cols] + l_b[:, cols].astype(f32) + r_b[:, cols].astype(f32)
+        a = sum(ref[:, cols].astype(f32) for ref in parts_a)
+        b = sum(ref[:, cols].astype(f32) for ref in parts_b)
         return jnp.where(first, a, b), jnp.where(first, b, a)
 
     totals = [total(g) for g in range(8)]
@@ -349,7 +356,15 @@
         one = one if low % 2 == 0 else pltpu.roll(one, 64, 1)
         two = two if high % 2 == 1 else pltpu.roll(two, 64, 1)
         cols = chip_columns(chip_of(0, j, i))
-        out_ref[:, cols] = (resid_ref[:, cols] + jnp.where(left, one, two)).astype(bf16)
+        out_ref[:, cols] = (base_ref[:, cols] + jnp.where(left, one, two)).astype(out_ref.dtype)
+
+
+def base_kernel(resid_ref, own_a, own_b, r_a, l_b, out_ref):
+    add_in_order(resid_ref, (own_a, r_a), (own_b, l_b), out_ref)
+
+
+def last_kernel(base_ref, l_a, r_b, out_ref):
+    add_in_order(base_ref, (l_a,), (r_b,), out_ref)
 
 
 def by_first_core(step):
@@ -368,7 +383,7 @@
     return jax.ShapeDtypeStruct(dims, dtype)
 
 
-def call(kernel, out_shape, n_in, cost, scratch=(), mib=8, n_hbm=0):
+def call(kernel, out_shape, n_in, cost, scratch=(), mib=5, n_hbm=0):
     out_specs = jax.tree.map(lambda _: VMEM, out_shape)
     return pl.pallas_call(
         kernel,
@@ -382,8 +397,8 @@
 
 
 HBM = pl.BlockSpec(memory_space=pltpu.HBM)
-FEED_MIB = 20
-ATTEND_MIB = 20
+FEED_MIB = 12
+ATTEND_MIB = 10
 
 
 def feed(normed, halo, t_gate, t_value, pieces, rels, plan, dtypes):
@@ -434,7 +449,7 @@
         [
             pltpu.VMEM((TOK, 128), bf16), pltpu.VMEM((TOK, 128), bf16), pltpu.VMEM((6, 128), f32),
             pltpu.VMEM((TOK, 128), bf16), pltpu.VMEM((TOK, 256), bf16), pltpu.SemaphoreType.DMA((4,)),
-        ], 8, 4,
+        ], 5, 4,
     )(pre, fade.reshape(6, 128), k, v)
     other = lax.ppermute(pack, C, swap)
 
@@ -454,7 +469,9 @@
     along_z = [lax.ppermute(plane, SP, by_first_core(s)) for s in (1, 2, 3)]
     entering = call(enter_kernel, shape(128, 128, dtype=f32), 4, _cost(1e5, 3e5))(*along_z, before)
     given = lax.ppermute(entering, C, [(0, 1)])
-    stacks = [jnp.stack([shard, first[0]], axis=0), jnp.stack(first[1:], axis=0)]
+    stacks = call(
+        stack_kernel, [shape(2, 3, 64, HID)] * 2, 4, _cost(1e5, 4 * 3 * 64 * HID * 4)
+    )(shard, *first)
     right, left = around(1, True), around(3, True)
     right_a = lax.ppermute(stacks[0], SP, right)
     left_b = lax.ppermute(stacks[1], SP, left)
@@ -500,9 +517,10 @@
     near_l_a = lax.ppermute(send_r, X, ring(1))
     near_r_b = lax.ppermute(send_l, X, ring(3))
     own_a, own_b = feeds((0,), ((0, 0), (0, 1)), (f32, f32))
-    return call(last_kernel, shape(ROWS, D), 7, _cost(1e6, 5e6))(
-        resid, own_a, own_b, near_l_a, near_l_b, near_r_a, near_r_b
+    base = call(base_kernel, shape(ROWS, D, dtype=f32), 5, _cost(1e6, 6e6))(
+        resid, own_a, own_b, near_r_a, near_l_b
     )
+    return call(last_kernel, shape(ROWS, D), 3, _cost(1e6, 3e6))(base, near_l_a, near_r_b)
 
 
 def solution(mesh):

time: 169 us -> 152 us (0.90)
  the two profiles are of different devices: /device:TPU:6 before, /device:TPU:24 now
where the time goes in v5:
time: 152 us; the launch traced here: 150 us
  starting transfers between devices  57.5 us (38%)
  waiting for transfers between devices  54.6 us (36%)
  Pallas kernels  32.8 us (22%)
  local copies, waits for them, and re-layouts  4.71 us (3%)
    pallas_call x3, Pallas kernels, feed(): pl.pallas_call(functools.partial(feed_kernel, rels, plan), out_shape=[sha...  18.5 us
    ppermute x2, waiting for transfers between devices, per_device(): far = [lax.ppermute(right_a, SP, right), lax.ppermute(left_b, SP, left)]  12.6 us
    ppermute x1, waiting for transfers between devices, per_device(): lax.ppermute(mixed, X, ring(3))  10.7 us
    ppermute x3, starting transfers between devices, per_device(): along_z = [lax.ppermute(plane, SP, by_first_core(s)) for s in (1, 2, 3)]  9.98 us
    ppermute x1, waiting for transfers between devices, per_device(): near_l_a = lax.ppermute(send_r, X, ring(1))  6.07 us
    ppermute x3, starting transfers between devices, per_device(): first = [lax.ppermute(shard, SP, around(s, False)) for s in steps]  5.61 us
    ppermute x1, waiting for transfers between devices, per_device(): lax.ppermute(mixed, X, ring(1))  5.07 us
    ppermute x3, starting transfers between devices, per_device(): w_got = [lax.ppermute(w_half, X, ring(s)) for s in steps]  4.33 us
  transfers between devices with their start and end apart: 42, of which 15 were waited for; matrix products, arithmetic and copies ran while one was open for 1% of the time, Pallas kernels for 16%

profile of v5, /device:TPU:24, one launch (start us, length us, event | category | flops | bytes accessed | tf_op | source)
XLA Modules:
  0.0 150.1 jit_solution(9158814427835441200)
XLA Ops:
  0.0 1.0 copy-done.2
  1.0 0.9 copy-done.4
  1.9 0.9 copy-done.8
  3.5 1.9 %shard_map.145 = (f32[768,128]{1,0:T(8,128)S(1)}, f32[136,128]{1,0:T(8,128)S(1)}) custom-call(bf16[768,128]{1,0:T(8,128)(2,1)S(1)} %copy-done.8, f32[6,128]{1,0:T(8,128)S(1)} %bitcast.9, bf16[768,128]{1,0:T(8,128)(2,1)S(1)} %copy-done.4, bf16[768,256]{1,0:T(8,128)(2,1)S(1)} %copy-done.2), custom_call_target="tpu_custom_call" | custom-call | flops 50331648 | bytes 1000000 | tf_op jit(solution)/shard_map/pallas_call | solution.py:445
  5.5 1.2 collective-permute-done.other_ref
  7.6 0.8 collective-permute-start.2
  8.4 2.3 %collective-permute-start.3 = (f32[136,128]{1,0:T(8,128)S(1)}, f32[136,128]{1,0:T(8,128)S(1)}, u32[]{:S(2)}, u32[]{:S(2)}) collective-permute-start(f32[136,128]{1,0:T(8,128)S(1)} %shard_map.147.own_ref), channel_id=1, source_target_pairs={{0,8},{8,16},{16,24},{24,0},{1,9},{9,17},{17,25},{25,1},{2,10},{10... | collective-permute-start | bytes 208904 | tf_op jit(solution)/shard_map/ppermute | solution.py:460
  10.7 1.1 constant_dynamic-slice_fusion
  11.8 1.6 %collective-permute-start.10 = (bf16[128,2048]{1,0:T(8,128)(2,1)S(1)}, bf16[128,2048]{1,0:T(8,128)(2,1)S(1)}, u32[]{:S(2)}, u32[]{:S(2)}) collective-permute-start(bf16[128,2048]{1,0:T(8,128)(2,1)S(1)} %constant_dynamic-slice_fusion), channel_id=1, source_target_pairs={{0,1},{1,2},{2,3},{3,0},{4,5},{5,6},{6,7},{7,4},{8,9},{9,10},{10,1... | collective-permute-start | bytes 1572872 | tf_op jit(solution)/shard_map/ppermute | solution.py:457
  13.4 1.7 %collective-permute-start.11 = (bf16[128,2048]{1,0:T(8,128)(2,1)S(1)}, bf16[128,2048]{1,0:T(8,128)(2,1)S(1)}, u32[]{:S(2)}, u32[]{:S(2)}) collective-permute-start(bf16[128,2048]{1,0:T(8,128)(2,1)S(1)} %constant_dynamic-slice_fusion), channel_id=1, source_target_pairs={{0,3},{1,0},{2,1},{3,2},{4,7},{5,4},{6,5},{7,6},{8,11},{9,8},{10,9... | collective-permute-start | bytes 1572872 | tf_op jit(solution)/shard_map/ppermute | solution.py:457
  15.2 3.8 %collective-permute-start.4 = (f32[136,128]{1,0:T(8,128)S(1)}, f32[136,128]{1,0:T(8,128)S(1)}, u32[]{:S(2)}, u32[]{:S(2)}) collective-permute-start(f32[136,128]{1,0:T(8,128)S(1)} %get-tuple-element.30), channel_id=1, source_target_pairs={{0,32},{8,40},{16,48},{24,56},{32,64},{40,72},{48,80},{56,88},{64,... | collective-permute-start | bytes 208904 | tf_op jit(solution)/shard_map/ppermute | solution.py:469
  19.2 2.0 %collective-permute-start.19 = (bf16[3,64,1408]{2,1,0:T(8,128)(2,1)S(1)}, bf16[3,64,1408]{2,1,0:T(8,128)(2,1)S(1)}, u32[]{:S(2)}, u32[]{:S(2)}) collective-permute-start(bf16[3,64,1408]{2,1,0:T(8,128)(2,1)S(1)} %pad_maximum_fusion.own_ref), channel_id=1, source_target_pairs={{0,32},{4,12},{8,40},{12,20},{16,48},{20,28},{24,56},{28,4},{32,64... | collective-permute-start | bytes 1622024 | tf_op jit(solution)/shard_map/ppermute | solution.py:443
  21.2 3.6 %collective-permute-start.5 = (f32[136,128]{1,0:T(8,128)S(1)}, f32[136,128]{1,0:T(8,128)S(1)}, u32[]{:S(2)}, u32[]{:S(2)}) collective-permute-start(f32[136,128]{1,0:T(8,128)S(1)} %get-tuple-element.30), channel_id=1, source_target_pairs={{0,64},{8,72},{16,80},{24,88},{32,96},{40,104},{48,112},{56,120},{... | collective-permute-start | bytes 208904 | tf_op jit(solution)/shard_map/ppermute | solution.py:469
  24.8 2.6 %collective-permute-start.6 = (f32[136,128]{1,0:T(8,128)S(1)}, f32[136,128]{1,0:T(8,128)S(1)}, u32[]{:S(2)}, u32[]{:S(2)}) collective-permute-start(f32[136,128]{1,0:T(8,128)S(1)} %get-tuple-element.30), channel_id=1, source_target_pairs={{0,96},{8,104},{16,112},{24,120},{1,97},{9,105},{17,113},{25,121},... | collective-permute-start | bytes 208904 | tf_op jit(solution)/shard_map/ppermute | solution.py:469
  27.4 1.4 collective-permute-done.5.z2_ref
  29.3 1.3 collective-permute-start.7
  30.6 1.5 shard_map.146
  33.6 3.6 %collective-permute-start.20 = (bf16[3,64,1408]{2,1,0:T(8,128)(2,1)S(1)}, bf16[3,64,1408]{2,1,0:T(8,128)(2,1)S(1)}, u32[]{:S(2)}, u32[]{:S(2)}) collective-permute-start(bf16[3,64,1408]{2,1,0:T(8,128)(2,1)S(1)} %pad_maximum_fusion.own_ref), channel_id=1, source_target_pairs={{0,96},{4,28},{8,104},{12,4},{16,112},{20,12},{24,120},{28,20},{32... | collective-permute-start | bytes 1622024 | tf_op jit(solution)/shard_map/ppermute | solution.py:443
  37.2 2.6 %collective-permute-start.9 = (bf16[768,256]{1,0:T(8,128)(2,1)S(1)}, bf16[768,256]{1,0:T(8,128)(2,1)S(1)}, u32[]{:S(2)}, u32[]{:S(2)}) collective-permute-start(bf16[768,256]{1,0:T(8,128)(2,1)S(1)} %shard_map.150.m0), channel_id=1, source_target_pairs={{0,3},{1,0},{2,1},{3,2},{4,7},{5,4},{6,5},{7,6},{8,11},{9,8},{10,9... | collective-permute-start | bytes 1179656 | tf_op jit(solution)/shard_map/ppermute | solution.py:484
  39.8 1.0 collective-permute-start.16
  40.8 5.1 %collective-permute-done.8.m1 = bf16[768,256]{1,0:T(8,128)(2,1)S(1)} collective-permute-done((bf16[768,256]{1,0:T(8,128)(2,1)S(1)}, bf16[768,256]{1,0:T(8,128)(2,1)S(1)}, u32[]{:S(2)}, u32[]{:S(2)}) %collective-permute-start.8) | collective-permute-done | bytes 393248 | tf_op jit(solution)/shard_map/ppermute | solution.py:484
  45.9 10.7 %collective-permute-done.9.m2 = bf16[768,256]{1,0:T(8,128)(2,1)S(1)} collective-permute-done((bf16[768,256]{1,0:T(8,128)(2,1)S(1)}, bf16[768,256]{1,0:T(8,128)(2,1)S(1)}, u32[]{:S(2)}, u32[]{:S(2)}) %collective-permute-start.9) | collective-permute-done | bytes 393248 | tf_op jit(solution)/shard_map/ppermute | solution.py:484
  56.6 4.3 %collective-permute-start.15 = (bf16[384,256]{1,0:T(8,128)(2,1)S(1)}, bf16[384,256]{1,0:T(8,128)(2,1)S(1)}, u32[]{:S(2)}, u32[]{:S(2)}) collective-permute-start(bf16[384,256]{1,0:T(8,128)(2,1)S(1)} %slice.9), channel_id=1, source_target_pairs={{0,3},{1,0},{2,1},{3,2},{4,7},{5,4},{6,5},{7,6},{8,11},{9,8},{10,9... | collective-permute-start | bytes 589832 | tf_op jit(solution)/shard_map/ppermute | solution.py:487
  61.1 4.0 %collective-permute-start.22 = (bf16[2,3,64,1408]{3,2,1,0:T(8,128)(2,1)S(1)}, bf16[2,3,64,1408]{3,2,1,0:T(8,128)(2,1)S(1)}, u32[]{:S(2)}, u32[]{:S(2)}) collective-permute-start(bf16[2,3,64,1408]{3,2,1,0:T(8,128)(2,1)S(1)} %get-tuple-element.35.refs_0_), channel_id=1, source_target_pairs={{0,8},{4,36},{8,16},{12,44},{16,24},{20,52},{24,0},{28,60},{32,40}... | collective-permute-start | bytes 3244040 | tf_op jit(solution)/shard_map/ppermute | solution.py:476
  65.1 1.5 collective-permute-start.25
  66.5 1.9 %collective-permute-start.23 = (bf16[2,3,64,1408]{3,2,1,0:T(8,128)(2,1)S(1)}, bf16[2,3,64,1408]{3,2,1,0:T(8,128)(2,1)S(1)}, u32[]{:S(2)}, u32[]{:S(2)}) collective-permute-start(bf16[2,3,64,1408]{3,2,1,0:T(8,128)(2,1)S(1)} %get-tuple-element.36.refs_1_), channel_id=1, source_target_pairs={{0,8},{4,36},{8,16},{12,44},{16,24},{20,52},{24,0},{28,60},{32,40}... | collective-permute-start | bytes 3244040 | tf_op jit(solution)/shard_map/ppermute | solution.py:478
  68.6 3.7 %collective-permute-start.17 = (bf16[128,2048]{1,0:T(8,128)(2,1)S(1)}, bf16[128,2048]{1,0:T(8,128)(2,1)S(1)}, u32[]{:S(2)}, u32[]{:S(2)}) collective-permute-start(bf16[128,2048]{1,0:T(8,128)(2,1)S(1)} %collective-permute-done.16.got3), channel_id=1, source_target_pairs={{0,4},{4,0},{1,5},{5,1},{2,6},{6,2},{3,7},{7,3},{8,12},{12,8},{9,1... | collective-permute-start | bytes 1572872 | tf_op jit(solution)/shard_map/ppermute | solution.py:489
  72.3 3.5 %shard_map.151.part_ref = f32[768,2048]{1,0:T(8,128)S(1)} custom-call(bf16[768,256]{1,0:T(8,128)(2,1)S(1)} %shard_map.150.m0, bf16[768,256]{1,0:T(8,128)(2,1)S(1)} %collective-permute-done.8.m1, bf16[768,256]{1,0:T(8,128)(2,1)S(1)} %collective-permute-done.9.m2, bf16[256,2048]{1,0:T(8,128)(2,1)S(1)} %copy-done.1, ...), custom_call_target="tpu_custom_call" | custom-call | flops 2415919104 | bytes 12000000 | tf_op jit(solution)/shard_map/pallas_call | solution.py:493
  75.8 4.3 %shard_map.152 = (bf16[768,2048]{1,0:T(8,128)(2,1)S(1)}, bf16[16,2048]{1,0:T(8,128)(2,1)S(1)}, f32[192,2048]{1,0:T(8,128)S(1)}) custom-call(f32[768,2048]{1,0:T(8,128)S(1)} %shard_map.151.part_ref, bf16[384,256]{1,0:T(8,128)(2,1)S(1)} %collective-permute-done.14.early, bf16[384,256]{1,0:T(8,128)(2,1)S(1)} %collective-permute-done.15.late, ...), custom_call_target="tpu_custom_call" | custom-call | flops 805306368 | bytes 12000000 | tf_op jit(solution)/shard_map/pallas_call | solution.py:497
  80.2 2.0 %collective-permute-start.18 = (bf16[16,2048]{1,0:T(8,128)(2,1)S(1)}, bf16[16,2048]{1,0:T(8,128)(2,1)S(1)}, u32[]{:S(2)}, u32[]{:S(2)}) collective-permute-start(bf16[16,2048]{1,0:T(8,128)(2,1)S(1)} %get-tuple-element.34), channel_id=1, source_target_pairs={{0,4},{4,8},{8,12},{12,16},{16,20},{20,24},{24,28},{28,32},{32,36}... | collective-permute-start | bytes 196616 | tf_op jit(solution)/shard_map/ppermute | solution.py:503
  82.2 4.3 %collective-permute-done.18.halo_ref = bf16[16,2048]{1,0:T(8,128)(2,1)S(1)} collective-permute-done((bf16[16,2048]{1,0:T(8,128)(2,1)S(1)}, bf16[16,2048]{1,0:T(8,128)(2,1)S(1)}, u32[]{:S(2)}, u32[]{:S(2)}) %collective-permute-start.18) | collective-permute-done | bytes 65568 | tf_op jit(solution)/shard_map/ppermute | solution.py:503
  87.0 3.1 %collective-permute-done.23.refs_3_ = bf16[2,3,64,1408]{3,2,1,0:T(8,128)(2,1)S(1)} collective-permute-done((bf16[2,3,64,1408]{3,2,1,0:T(8,128)(2,1)S(1)}, bf16[2,3,64,1408]{3,2,1,0:T(8,128)(2,1)S(1)}, u32[]{:S(2)}, u32[]{:S(2)}) %collective-permute-start.23) | collective-permute-done | bytes 1081376 | tf_op jit(solution)/shard_map/ppermute | solution.py:478
  90.7 2.4 %collective-permute-done.24.refs_4_ = bf16[2,3,64,1408]{3,2,1,0:T(8,128)(2,1)S(1)} collective-permute-done((bf16[2,3,64,1408]{3,2,1,0:T(8,128)(2,1)S(1)}, bf16[2,3,64,1408]{3,2,1,0:T(8,128)(2,1)S(1)}, u32[]{:S(2)}, u32[]{:S(2)}) %collective-permute-start.24) | collective-permute-done | bytes 1081376 | tf_op jit(solution)/shard_map/ppermute | solution.py:479
  93.8 8.3 %collective-permute-done.26.refs_6_ = bf16[2,3,64,1408]{3,2,1,0:T(8,128)(2,1)S(1)} collective-permute-done((bf16[2,3,64,1408]{3,2,1,0:T(8,128)(2,1)S(1)}, bf16[2,3,64,1408]{3,2,1,0:T(8,128)(2,1)S(1)}, u32[]{:S(2)}, u32[]{:S(2)}) %collective-permute-start.26) | collective-permute-done | bytes 1081376 | tf_op jit(solution)/shard_map/ppermute | solution.py:490
  102.5 4.3 %collective-permute-done.27.refs_7_ = bf16[2,3,64,1408]{3,2,1,0:T(8,128)(2,1)S(1)} collective-permute-done((bf16[2,3,64,1408]{3,2,1,0:T(8,128)(2,1)S(1)}, bf16[2,3,64,1408]{3,2,1,0:T(8,128)(2,1)S(1)}, u32[]{:S(2)}, u32[]{:S(2)}) %collective-permute-start.27) | collective-permute-done | bytes 1081376 | tf_op jit(solution)/shard_map/ppermute | solution.py:490
  107.4 2.2 %collective-permute-done.34.refs_14_ = bf16[2,3,64,1408]{3,2,1,0:T(8,128)(2,1)S(1)} collective-permute-done((bf16[2,3,64,1408]{3,2,1,0:T(8,128)(2,1)S(1)}, bf16[2,3,64,1408]{3,2,1,0:T(8,128)(2,1)S(1)}, u32[]{:S(2)}, u32[]{:S(2)}) %collective-permute-start.34) | collective-permute-done | bytes 1081376 | tf_op jit(solution)/shard_map/ppermute | solution.py:492
  109.6 1.5 %collective-permute-done.35.refs_15_ = bf16[2,3,64,1408]{3,2,1,0:T(8,128)(2,1)S(1)} collective-permute-done((bf16[2,3,64,1408]{3,2,1,0:T(8,128)(2,1)S(1)}, bf16[2,3,64,1408]{3,2,1,0:T(8,128)(2,1)S(1)}, u32[]{:S(2)}, u32[]{:S(2)}) %collective-permute-start.35) | collective-permute-done | bytes 1081376 | tf_op jit(solution)/shard_map/ppermute | solution.py:492
  111.1 5.1 %feed.5 = (bf16[192,1024]{1,0:T(8,128)(2,1)S(1)}, bf16[192,1024]{1,0:T(8,128)(2,1)S(1)}) custom-call(bf16[768,2048]{1,0:T(8,128)(2,1)S(1)} %get-tuple-element.33.x_ref, bf16[16,2048]{1,0:T(8,128)(2,1)S(1)} %collective-permute-done.18.halo_ref, bf16[3,1408]{1,0:T(4,128)(2,1)S(1)} %copy-done.9, bf16[3,1408]{1,0:T(4,128)(2,1)S(1)} %copy-done.10, ...), custom_call_target="tpu_custom_call" | custom-call | flops 3598712832 | bytes 17301504 | tf_op jit(solution)/shard_map/feed/pallas_call | solution.py:406
  116.3 3.2 %collective-permute-start.39 = (bf16[192,1024]{1,0:T(8,128)(2,1)S(1)}, bf16[192,1024]{1,0:T(8,128)(2,1)S(1)}, u32[]{:S(2)}, u32[]{:S(2)}) collective-permute-start(bf16[192,1024]{1,0:T(8,128)(2,1)S(1)} %get-tuple-element.44), channel_id=1, source_target_pairs={{0,3},{1,0},{2,1},{3,2},{4,7},{5,4},{6,5},{7,6},{8,11},{9,8},{10,9... | collective-permute-start | bytes 1179656 | tf_op jit(solution)/shard_map/ppermute | solution.py:508
  119.5 8.3 %feed.4 = (f32[192,1024]{1,0:T(8,128)S(1)}, bf16[192,1024]{1,0:T(8,128)(2,1)S(1)}, bf16[192,1024]{1,0:T(8,128)(2,1)S(1)}, f32[192,1024]{1,0:T(8,128)S(1)}) custom-call(bf16[768,2048]{1,0:T(8,128)(2,1)S(1)} %get-tuple-element.33.x_ref, bf16[16,2048]{1,0:T(8,128)(2,1)S(1)} %collective-permute-done.18.halo_ref, bf16[3,1408]{1,0:T(4,128)(2,1)S(1)} %copy-done.9, ...), custom_call_target="tpu_custom_call" | custom-call | flops 7197425664 | bytes 17301504 | tf_op jit(solution)/shard_map/feed/pallas_call | solution.py:406
  127.8 0.9 collective-permute-start.36
  128.7 1.2 collective-permute-start.37
  130.1 3.2 %collective-permute-start.41 = (bf16[192,1024]{1,0:T(8,128)(2,1)S(1)}, bf16[192,1024]{1,0:T(8,128)(2,1)S(1)}, u32[]{:S(2)}, u32[]{:S(2)}) collective-permute-start(bf16[192,1024]{1,0:T(8,128)(2,1)S(1)} %get-tuple-element.46), channel_id=1, source_target_pairs={{0,3},{1,0},{2,1},{3,2},{4,7},{5,4},{6,5},{7,6},{8,11},{9,8},{10,9... | collective-permute-start | bytes 1179656 | tf_op jit(solution)/shard_map/ppermute | solution.py:518
  133.4 5.1 %feed.3 = (f32[192,1024]{1,0:T(8,128)S(1)}, f32[192,1024]{1,0:T(8,128)S(1)}) custom-call(bf16[768,2048]{1,0:T(8,128)(2,1)S(1)} %get-tuple-element.33.x_ref, bf16[16,2048]{1,0:T(8,128)(2,1)S(1)} %collective-permute-done.18.halo_ref, bf16[3,1408]{1,0:T(4,128)(2,1)S(1)} %copy-done.9, bf16[3,1408]{1,0:T(4,128)(2,1)S(1)} %copy-done.10, ...), custom_call_target="tpu_custom_call" | custom-call | flops 3598712832 | bytes 17301504 | tf_op jit(solution)/shard_map/feed/pallas_call | solution.py:406
  138.5 1.4 collective-permute-done.36.r_a
  139.9 2.0 %collective-permute-done.37.l_b = bf16[192,1024]{1,0:T(8,128)(2,1)S(1)} collective-permute-done((bf16[192,1024]{1,0:T(8,128)(2,1)S(1)}, bf16[192,1024]{1,0:T(8,128)(2,1)S(1)}, u32[]{:S(2)}, u32[]{:S(2)}) %collective-permute-start.37) | collective-permute-done | bytes 393248 | tf_op jit(solution)/shard_map/ppermute | solution.py:512
  142.6 6.1 %collective-permute-done.40.l_a = bf16[192,1024]{1,0:T(8,128)(2,1)S(1)} collective-permute-done((bf16[192,1024]{1,0:T(8,128)(2,1)S(1)}, bf16[192,1024]{1,0:T(8,128)(2,1)S(1)}, u32[]{:S(2)}, u32[]{:S(2)}) %collective-permute-start.40) | collective-permute-done | bytes 393248 | tf_op jit(solution)/shard_map/ppermute | solution.py:517
  148.7 1.4 shard_map.156
  (89 shorter events, 8.0 us)
Async XLA Ops:
  5.4 1.3 collective-permute-start
  6.8 8.4 %collective-permute-start.1 = (f32[136,128]{1,0:T(8,128)S(1)}, f32[136,128]{1,0:T(8,128)S(1)}, u32[]{:S(2)}, u32[]{:S(2)}) collective-permute-start(f32[136,128]{1,0:T(8,128)S(1)} %shard_map.147.own_ref), channel_id=1, source_target_pairs={{0,24},{8,0},{16,8},{24,16},{1,25},{9,1},{17,9},{25,17},{2,26},{10... | collective-permute-start | bytes 208904 | tf_op jit(solution)/shard_map/ppermute | solution.py:460
  7.6 7.5 %collective-permute-start.2 = (f32[136,128]{1,0:T(8,128)S(1)}, f32[136,128]{1,0:T(8,128)S(1)}, u32[]{:S(2)}, u32[]{:S(2)}) collective-permute-start(f32[136,128]{1,0:T(8,128)S(1)} %shard_map.147.own_ref), channel_id=1, source_target_pairs={{0,16},{8,24},{16,0},{24,8},{1,17},{9,25},{17,1},{25,9},{2,18},{10... | collective-permute-start | bytes 208904 | tf_op jit(solution)/shard_map/ppermute | solution.py:460
  8.4 6.7 %collective-permute-start.3 = (f32[136,128]{1,0:T(8,128)S(1)}, f32[136,128]{1,0:T(8,128)S(1)}, u32[]{:S(2)}, u32[]{:S(2)}) collective-permute-start(f32[136,128]{1,0:T(8,128)S(1)} %shard_map.147.own_ref), channel_id=1, source_target_pairs={{0,8},{8,16},{16,24},{24,0},{1,9},{9,17},{17,25},{25,1},{2,10},{10... | collective-permute-start | bytes 208904 | tf_op jit(solution)/shard_map/ppermute | solution.py:460
  11.8 18.8 %copy-start.3 = (bf16[768,256]{1,0:T(8,128)(2,1)S(1)}, bf16[768,256]{1,0:T(8,128)(2,1)}, u32[]{:S(2)}) copy-start(bf16[768,256]{1,0:T(8,128)(2,1)} %v_ref.1) | copy-start | bytes 1179652
  11.8 18.8 %copy-start.5 = (bf16[768,128]{1,0:T(8,128)(2,1)S(1)}, bf16[768,128]{1,0:T(8,128)(2,1)}, u32[]{:S(2)}) copy-start(bf16[768,128]{1,0:T(8,128)(2,1)} %k_ref.1) | copy-start | bytes 589828
  11.8 18.8 %copy-start.7 = (bf16[768,128]{1,0:T(8,128)(2,1)S(1)}, bf16[768,128]{1,0:T(8,128)(2,1)}, u32[]{:S(2)}) copy-start(bf16[768,128]{1,0:T(8,128)(2,1)} %q_ref.1) | copy-start | bytes 589828
  11.8 25.4 %collective-permute-start.10 = (bf16[128,2048]{1,0:T(8,128)(2,1)S(1)}, bf16[128,2048]{1,0:T(8,128)(2,1)S(1)}, u32[]{:S(2)}, u32[]{:S(2)}) collective-permute-start(bf16[128,2048]{1,0:T(8,128)(2,1)S(1)} %constant_dynamic-slice_fusion), channel_id=1, source_target_pairs={{0,1},{1,2},{2,3},{3,0},{4,5},{5,6},{6,7},{7,4},{8,9},{9,10},{10,1... | collective-permute-start | bytes 1572872 | tf_op jit(solution)/shard_map/ppermute | solution.py:457
  13.4 23.8 %collective-permute-start.11 = (bf16[128,2048]{1,0:T(8,128)(2,1)S(1)}, bf16[128,2048]{1,0:T(8,128)(2,1)S(1)}, u32[]{:S(2)}, u32[]{:S(2)}) collective-permute-start(bf16[128,2048]{1,0:T(8,128)(2,1)S(1)} %constant_dynamic-slice_fusion), channel_id=1, source_target_pairs={{0,3},{1,0},{2,1},{3,2},{4,7},{5,4},{6,5},{7,6},{8,11},{9,8},{10,9... | collective-permute-start | bytes 1572872 | tf_op jit(solution)/shard_map/ppermute | solution.py:457
  15.2 9.6 %collective-permute-start.4 = (f32[136,128]{1,0:T(8,128)S(1)}, f32[136,128]{1,0:T(8,128)S(1)}, u32[]{:S(2)}, u32[]{:S(2)}) collective-permute-start(f32[136,128]{1,0:T(8,128)S(1)} %get-tuple-element.30), channel_id=1, source_target_pairs={{0,32},{8,40},{16,48},{24,56},{32,64},{40,72},{48,80},{56,88},{64,... | collective-permute-start | bytes 208904 | tf_op jit(solution)/shard_map/ppermute | solution.py:469
  19.2 20.6 %collective-permute-start.19 = (bf16[3,64,1408]{2,1,0:T(8,128)(2,1)S(1)}, bf16[3,64,1408]{2,1,0:T(8,128)(2,1)S(1)}, u32[]{:S(2)}, u32[]{:S(2)}) collective-permute-start(bf16[3,64,1408]{2,1,0:T(8,128)(2,1)S(1)} %pad_maximum_fusion.own_ref), channel_id=1, source_target_pairs={{0,32},{4,12},{8,40},{12,20},{16,48},{20,28},{24,56},{28,4},{32,64... | collective-permute-start | bytes 1622024 | tf_op jit(solution)/shard_map/ppermute | solution.py:443
  21.2 7.6 %collective-permute-start.5 = (f32[136,128]{1,0:T(8,128)S(1)}, f32[136,128]{1,0:T(8,128)S(1)}, u32[]{:S(2)}, u32[]{:S(2)}) collective-permute-start(f32[136,128]{1,0:T(8,128)S(1)} %get-tuple-element.30), channel_id=1, source_target_pairs={{0,64},{8,72},{16,80},{24,88},{32,96},{40,104},{48,112},{56,120},{... | collective-permute-start | bytes 208904 | tf_op jit(solution)/shard_map/ppermute | solution.py:469
  24.8 4.5 %collective-permute-start.6 = (f32[136,128]{1,0:T(8,128)S(1)}, f32[136,128]{1,0:T(8,128)S(1)}, u32[]{:S(2)}, u32[]{:S(2)}) collective-permute-start(f32[136,128]{1,0:T(8,128)S(1)} %get-tuple-element.30), channel_id=1, source_target_pairs={{0,96},{8,104},{16,112},{24,120},{1,97},{9,105},{17,113},{25,121},... | collective-permute-start | bytes 208904 | tf_op jit(solution)/shard_map/ppermute | solution.py:469
  29.3 2.8 %collective-permute-start.7 = (f32[128,128]{1,0:T(8,128)S(1)}, f32[128,128]{1,0:T(8,128)S(1)}, u32[]{:S(2)}, u32[]{:S(2)}) collective-permute-start(f32[128,128]{1,0:T(8,128)S(1)} %shard_map.149.mine_ref), channel_id=1, source_target_pairs={{0,4},{1,5},{2,6},{3,7},{8,12},{9,13},{10,14},{11,15},{16,20},{17,... | collective-permute-start | bytes 196616 | tf_op jit(solution)/shard_map/ppermute | solution.py:471
  32.1 40.1 %copy-start = (bf16[768,2048]{1,0:T(8,128)(2,1)S(1)}, bf16[768,2048]{1,0:T(8,128)(2,1)}, u32[]{:S(2)}) copy-start(bf16[768,2048]{1,0:T(8,128)(2,1)} %x_ref.1) | copy-start | bytes 9437188
  32.8 13.1 %collective-permute-start.8 = (bf16[768,256]{1,0:T(8,128)(2,1)S(1)}, bf16[768,256]{1,0:T(8,128)(2,1)S(1)}, u32[]{:S(2)}, u32[]{:S(2)}) collective-permute-start(bf16[768,256]{1,0:T(8,128)(2,1)S(1)} %shard_map.150.m0), channel_id=1, source_target_pairs={{0,1},{1,2},{2,3},{3,0},{4,5},{5,6},{6,7},{7,4},{8,9},{9,10},{10,1... | collective-permute-start | bytes 1179656 | tf_op jit(solution)/shard_map/ppermute | solution.py:484
  33.6 23.0 %collective-permute-start.20 = (bf16[3,64,1408]{2,1,0:T(8,128)(2,1)S(1)}, bf16[3,64,1408]{2,1,0:T(8,128)(2,1)S(1)}, u32[]{:S(2)}, u32[]{:S(2)}) collective-permute-start(bf16[3,64,1408]{2,1,0:T(8,128)(2,1)S(1)} %pad_maximum_fusion.own_ref), channel_id=1, source_target_pairs={{0,96},{4,28},{8,104},{12,4},{16,112},{20,12},{24,120},{28,20},{32... | collective-permute-start | bytes 1622024 | tf_op jit(solution)/shard_map/ppermute | solution.py:443
  37.2 23.7 %collective-permute-start.21 = (bf16[3,64,1408]{2,1,0:T(8,128)(2,1)S(1)}, bf16[3,64,1408]{2,1,0:T(8,128)(2,1)S(1)}, u32[]{:S(2)}, u32[]{:S(2)}) collective-permute-start(bf16[3,64,1408]{2,1,0:T(8,128)(2,1)S(1)} %pad_maximum_fusion.own_ref), channel_id=1, source_target_pairs={{0,64},{4,20},{8,72},{12,28},{16,80},{20,4},{24,88},{28,12},{32,96... | collective-permute-start | bytes 1622024 | tf_op jit(solution)/shard_map/ppermute | solution.py:443
  37.2 19.4 %collective-permute-start.9 = (bf16[768,256]{1,0:T(8,128)(2,1)S(1)}, bf16[768,256]{1,0:T(8,128)(2,1)S(1)}, u32[]{:S(2)}, u32[]{:S(2)}) collective-permute-start(bf16[768,256]{1,0:T(8,128)(2,1)S(1)} %shard_map.150.m0), channel_id=1, source_target_pairs={{0,3},{1,0},{2,1},{3,2},{4,7},{5,4},{6,5},{7,6},{8,11},{9,8},{10,9... | collective-permute-start | bytes 1179656 | tf_op jit(solution)/shard_map/ppermute | solution.py:484
  39.8 21.3 %collective-permute-start.16 = (bf16[128,2048]{1,0:T(8,128)(2,1)S(1)}, bf16[128,2048]{1,0:T(8,128)(2,1)S(1)}, u32[]{:S(2)}, u32[]{:S(2)}) collective-permute-start(bf16[128,2048]{1,0:T(8,128)(2,1)S(1)} %constant_dynamic-slice_fusion), channel_id=1, source_target_pairs={{0,2},{1,3},{2,0},{3,1},{4,6},{5,7},{6,4},{7,5},{8,10},{9,11},{10,... | collective-permute-start | bytes 1572872 | tf_op jit(solution)/shard_map/ppermute | solution.py:457
  45.9 22.6 %collective-permute-start.12 = (bf16[128,2048]{1,0:T(8,128)(2,1)S(1)}, bf16[128,2048]{1,0:T(8,128)(2,1)S(1)}, u32[]{:S(2)}, u32[]{:S(2)}) collective-permute-start(bf16[128,2048]{1,0:T(8,128)(2,1)S(1)} %collective-permute-done.10.got1), channel_id=1, source_target_pairs={{0,4},{4,0},{1,5},{5,1},{2,6},{6,2},{3,7},{7,3},{8,12},{12,8},{9,1... | collective-permute-start | bytes 1572872 | tf_op jit(solution)/shard_map/ppermute | solution.py:489
  56.6 8.5 %collective-permute-start.14 = (bf16[384,256]{1,0:T(8,128)(2,1)S(1)}, bf16[384,256]{1,0:T(8,128)(2,1)S(1)}, u32[]{:S(2)}, u32[]{:S(2)}) collective-permute-start(bf16[384,256]{1,0:T(8,128)(2,1)S(1)} %slice.8), channel_id=1, source_target_pairs={{0,1},{1,2},{2,3},{3,0},{4,5},{5,6},{6,7},{7,4},{8,9},{9,10},{10,1... | collective-permute-start | bytes 589832 | tf_op jit(solution)/shard_map/ppermute | solution.py:486
  56.6 9.9 %collective-permute-start.15 = (bf16[384,256]{1,0:T(8,128)(2,1)S(1)}, bf16[384,256]{1,0:T(8,128)(2,1)S(1)}, u32[]{:S(2)}, u32[]{:S(2)}) collective-permute-start(bf16[384,256]{1,0:T(8,128)(2,1)S(1)} %slice.9), channel_id=1, source_target_pairs={{0,3},{1,0},{2,1},{3,2},{4,7},{5,4},{6,5},{7,6},{8,11},{9,8},{10,9... | collective-permute-start | bytes 589832 | tf_op jit(solution)/shard_map/ppermute | solution.py:487
  60.9 7.7 %collective-permute-start.13 = (bf16[128,2048]{1,0:T(8,128)(2,1)S(1)}, bf16[128,2048]{1,0:T(8,128)(2,1)S(1)}, u32[]{:S(2)}, u32[]{:S(2)}) collective-permute-start(bf16[128,2048]{1,0:T(8,128)(2,1)S(1)} %collective-permute-done.11.got2), channel_id=1, source_target_pairs={{0,4},{4,0},{1,5},{5,1},{2,6},{6,2},{3,7},{7,3},{8,12},{12,8},{9,1... | collective-permute-start | bytes 1572872 | tf_op jit(solution)/shard_map/ppermute | solution.py:489
  61.1 25.4 %collective-permute-start.22 = (bf16[2,3,64,1408]{3,2,1,0:T(8,128)(2,1)S(1)}, bf16[2,3,64,1408]{3,2,1,0:T(8,128)(2,1)S(1)}, u32[]{:S(2)}, u32[]{:S(2)}) collective-permute-start(bf16[2,3,64,1408]{3,2,1,0:T(8,128)(2,1)S(1)} %get-tuple-element.35.refs_0_), channel_id=1, source_target_pairs={{0,8},{4,36},{8,16},{12,44},{16,24},{20,52},{24,0},{28,60},{32,40}... | collective-permute-start | bytes 3244040 | tf_op jit(solution)/shard_map/ppermute | solution.py:476
  65.1 21.9 %collective-permute-start.25 = (bf16[2,3,64,1408]{3,2,1,0:T(8,128)(2,1)S(1)}, bf16[2,3,64,1408]{3,2,1,0:T(8,128)(2,1)S(1)}, u32[]{:S(2)}, u32[]{:S(2)}) collective-permute-start(bf16[2,3,64,1408]{3,2,1,0:T(8,128)(2,1)S(1)} %get-tuple-element.36.refs_1_), channel_id=1, source_target_pairs={{0,24},{4,100},{8,0},{12,108},{16,8},{20,116},{24,16},{28,124},{32... | collective-permute-start | bytes 3244040 | tf_op jit(solution)/shard_map/ppermute | solution.py:477
  66.5 23.5 %collective-permute-start.23 = (bf16[2,3,64,1408]{3,2,1,0:T(8,128)(2,1)S(1)}, bf16[2,3,64,1408]{3,2,1,0:T(8,128)(2,1)S(1)}, u32[]{:S(2)}, u32[]{:S(2)}) collective-permute-start(bf16[2,3,64,1408]{3,2,1,0:T(8,128)(2,1)S(1)} %get-tuple-element.36.refs_1_), channel_id=1, source_target_pairs={{0,8},{4,36},{8,16},{12,44},{16,24},{20,52},{24,0},{28,60},{32,40}... | collective-permute-start | bytes 3244040 | tf_op jit(solution)/shard_map/ppermute | solution.py:478
  68.4 24.6 %collective-permute-start.24 = (bf16[2,3,64,1408]{3,2,1,0:T(8,128)(2,1)S(1)}, bf16[2,3,64,1408]{3,2,1,0:T(8,128)(2,1)S(1)}, u32[]{:S(2)}, u32[]{:S(2)}) collective-permute-start(bf16[2,3,64,1408]{3,2,1,0:T(8,128)(2,1)S(1)} %get-tuple-element.35.refs_0_), channel_id=1, source_target_pairs={{0,24},{4,100},{8,0},{12,108},{16,8},{20,116},{24,16},{28,124},{32... | collective-permute-start | bytes 3244040 | tf_op jit(solution)/shard_map/ppermute | solution.py:479
  68.6 7.2 %collective-permute-start.17 = (bf16[128,2048]{1,0:T(8,128)(2,1)S(1)}, bf16[128,2048]{1,0:T(8,128)(2,1)S(1)}, u32[]{:S(2)}, u32[]{:S(2)}) collective-permute-start(bf16[128,2048]{1,0:T(8,128)(2,1)S(1)} %collective-permute-done.16.got3), channel_id=1, source_target_pairs={{0,4},{4,0},{1,5},{5,1},{2,6},{6,2},{3,7},{7,3},{8,12},{12,8},{9,1... | collective-permute-start | bytes 1572872 | tf_op jit(solution)/shard_map/ppermute | solution.py:489
  75.8 35.3 %copy-start.9 = (bf16[3,1408]{1,0:T(4,128)(2,1)S(1)}, bf16[3,1408]{1,0:T(4,128)(2,1)}, u32[]{:S(2)}) copy-start(bf16[3,1408]{1,0:T(4,128)(2,1)} %tg_ref.5) | copy-start | bytes 25348
  75.8 35.3 %copy-start.10 = (bf16[3,1408]{1,0:T(4,128)(2,1)S(1)}, bf16[3,1408]{1,0:T(4,128)(2,1)}, u32[]{:S(2)}) copy-start(bf16[3,1408]{1,0:T(4,128)(2,1)} %tv_ref.5) | copy-start | bytes 25348
  80.2 6.3 %collective-permute-start.18 = (bf16[16,2048]{1,0:T(8,128)(2,1)S(1)}, bf16[16,2048]{1,0:T(8,128)(2,1)S(1)}, u32[]{:S(2)}, u32[]{:S(2)}) collective-permute-start(bf16[16,2048]{1,0:T(8,128)(2,1)S(1)} %get-tuple-element.34), channel_id=1, source_target_pairs={{0,4},{4,8},{8,12},{12,16},{16,20},{20,24},{24,28},{28,32},{32,36}... | collective-permute-start | bytes 196616 | tf_op jit(solution)/shard_map/ppermute | solution.py:503
  86.4 6.8 %collective-permute-start.28 = (bf16[2,3,64,1408]{3,2,1,0:T(8,128)(2,1)S(1)}, bf16[2,3,64,1408]{3,2,1,0:T(8,128)(2,1)S(1)}, u32[]{:S(2)}, u32[]{:S(2)}) collective-permute-start(bf16[2,3,64,1408]{3,2,1,0:T(8,128)(2,1)S(1)} %get-tuple-element.35.refs_0_), channel_id=1, source_target_pairs={{0,4},{4,0},{1,5},{5,1},{2,6},{6,2},{3,7},{7,3},{8,12},{12,8},{9,1... | collective-permute-start | bytes 3244040 | tf_op jit(solution)/shard_map/ppermute | solution.py:492
  86.5 7.1 %collective-permute-start.29 = (bf16[2,3,64,1408]{3,2,1,0:T(8,128)(2,1)S(1)}, bf16[2,3,64,1408]{3,2,1,0:T(8,128)(2,1)S(1)}, u32[]{:S(2)}, u32[]{:S(2)}) collective-permute-start(bf16[2,3,64,1408]{3,2,1,0:T(8,128)(2,1)S(1)} %get-tuple-element.36.refs_1_), channel_id=1, source_target_pairs={{0,4},{4,0},{1,5},{5,1},{2,6},{6,2},{3,7},{7,3},{8,12},{12,8},{9,1... | collective-permute-start | bytes 3244040 | tf_op jit(solution)/shard_map/ppermute | solution.py:492
  87.0 15.2 %collective-permute-start.26 = (bf16[2,3,64,1408]{3,2,1,0:T(8,128)(2,1)S(1)}, bf16[2,3,64,1408]{3,2,1,0:T(8,128)(2,1)S(1)}, u32[]{:S(2)}, u32[]{:S(2)}) collective-permute-start(bf16[2,3,64,1408]{3,2,1,0:T(8,128)(2,1)S(1)} %collective-permute-done.22.refs_2_), channel_id=1, source_target_pairs={{0,8},{4,36},{8,16},{12,44},{16,24},{20,52},{24,0},{28,60},{32,40}... | collective-permute-start | bytes 3244040 | tf_op jit(solution)/shard_map/ppermute | solution.py:490
  90.0 16.8 %collective-permute-start.27 = (bf16[2,3,64,1408]{3,2,1,0:T(8,128)(2,1)S(1)}, bf16[2,3,64,1408]{3,2,1,0:T(8,128)(2,1)S(1)}, u32[]{:S(2)}, u32[]{:S(2)}) collective-permute-start(bf16[2,3,64,1408]{3,2,1,0:T(8,128)(2,1)S(1)} %collective-permute-done.25.refs_5_), channel_id=1, source_target_pairs={{0,24},{4,100},{8,0},{12,108},{16,8},{20,116},{24,16},{28,124},{32... | collective-permute-start | bytes 3244040 | tf_op jit(solution)/shard_map/ppermute | solution.py:490
  93.1 13.8 %collective-permute-start.30 = (bf16[2,3,64,1408]{3,2,1,0:T(8,128)(2,1)S(1)}, bf16[2,3,64,1408]{3,2,1,0:T(8,128)(2,1)S(1)}, u32[]{:S(2)}, u32[]{:S(2)}) collective-permute-start(bf16[2,3,64,1408]{3,2,1,0:T(8,128)(2,1)S(1)} %collective-permute-done.22.refs_2_), channel_id=1, source_target_pairs={{0,4},{4,0},{1,5},{5,1},{2,6},{6,2},{3,7},{7,3},{8,12},{12,8},{9,1... | collective-permute-start | bytes 3244040 | tf_op jit(solution)/shard_map/ppermute | solution.py:492
  93.3 14.1 %collective-permute-start.33 = (bf16[2,3,64,1408]{3,2,1,0:T(8,128)(2,1)S(1)}, bf16[2,3,64,1408]{3,2,1,0:T(8,128)(2,1)S(1)}, u32[]{:S(2)}, u32[]{:S(2)}) collective-permute-start(bf16[2,3,64,1408]{3,2,1,0:T(8,128)(2,1)S(1)} %collective-permute-done.25.refs_5_), channel_id=1, source_target_pairs={{0,4},{4,0},{1,5},{5,1},{2,6},{6,2},{3,7},{7,3},{8,12},{12,8},{9,1... | collective-permute-start | bytes 3244040 | tf_op jit(solution)/shard_map/ppermute | solution.py:492
  93.6 13.8 %collective-permute-start.31 = (bf16[2,3,64,1408]{3,2,1,0:T(8,128)(2,1)S(1)}, bf16[2,3,64,1408]{3,2,1,0:T(8,128)(2,1)S(1)}, u32[]{:S(2)}, u32[]{:S(2)}) collective-permute-start(bf16[2,3,64,1408]{3,2,1,0:T(8,128)(2,1)S(1)} %collective-permute-done.23.refs_3_), channel_id=1, source_target_pairs={{0,4},{4,0},{1,5},{5,1},{2,6},{6,2},{3,7},{7,3},{8,12},{12,8},{9,1... | collective-permute-start | bytes 3244040 | tf_op jit(solution)/shard_map/ppermute | solution.py:492
  102.1 5.3 %collective-permute-start.32 = (bf16[2,3,64,1408]{3,2,1,0:T(8,128)(2,1)S(1)}, bf16[2,3,64,1408]{3,2,1,0:T(8,128)(2,1)S(1)}, u32[]{:S(2)}, u32[]{:S(2)}) collective-permute-start(bf16[2,3,64,1408]{3,2,1,0:T(8,128)(2,1)S(1)} %collective-permute-done.24.refs_4_), channel_id=1, source_target_pairs={{0,4},{4,0},{1,5},{5,1},{2,6},{6,2},{3,7},{7,3},{8,12},{12,8},{9,1... | collective-permute-start | bytes 3244040 | tf_op jit(solution)/shard_map/ppermute | solution.py:492
  106.8 2.7 %collective-permute-start.34 = (bf16[2,3,64,1408]{3,2,1,0:T(8,128)(2,1)S(1)}, bf16[2,3,64,1408]{3,2,1,0:T(8,128)(2,1)S(1)}, u32[]{:S(2)}, u32[]{:S(2)}) collective-permute-start(bf16[2,3,64,1408]{3,2,1,0:T(8,128)(2,1)S(1)} %collective-permute-done.26.refs_6_), channel_id=1, source_target_pairs={{0,4},{4,0},{1,5},{5,1},{2,6},{6,2},{3,7},{7,3},{8,12},{12,8},{9,1... | collective-permute-start | bytes 3244040 | tf_op jit(solution)/shard_map/ppermute | solution.py:492
  106.8 4.2 %collective-permute-start.35 = (bf16[2,3,64,1408]{3,2,1,0:T(8,128)(2,1)S(1)}, bf16[2,3,64,1408]{3,2,1,0:T(8,128)(2,1)S(1)}, u32[]{:S(2)}, u32[]{:S(2)}) collective-permute-start(bf16[2,3,64,1408]{3,2,1,0:T(8,128)(2,1)S(1)} %collective-permute-done.27.refs_7_), channel_id=1, source_target_pairs={{0,4},{4,0},{1,5},{5,1},{2,6},{6,2},{3,7},{7,3},{8,12},{12,8},{9,1... | collective-permute-start | bytes 3244040 | tf_op jit(solution)/shard_map/ppermute | solution.py:492
  116.2 13.7 %collective-permute-start.38 = (bf16[192,1024]{1,0:T(8,128)(2,1)S(1)}, bf16[192,1024]{1,0:T(8,128)(2,1)S(1)}, u32[]{:S(2)}, u32[]{:S(2)}) collective-permute-start(bf16[192,1024]{1,0:T(8,128)(2,1)S(1)} %get-tuple-element.42), channel_id=1, source_target_pairs={{0,1},{1,2},{2,3},{3,0},{4,5},{5,6},{6,7},{7,4},{8,9},{9,10},{10,1... | collective-permute-start | bytes 1179656 | tf_op jit(solution)/shard_map/ppermute | solution.py:507
  116.3 13.6 %collective-permute-start.39 = (bf16[192,1024]{1,0:T(8,128)(2,1)S(1)}, bf16[192,1024]{1,0:T(8,128)(2,1)S(1)}, u32[]{:S(2)}, u32[]{:S(2)}) collective-permute-start(bf16[192,1024]{1,0:T(8,128)(2,1)S(1)} %get-tuple-element.44), channel_id=1, source_target_pairs={{0,3},{1,0},{2,1},{3,2},{4,7},{5,4},{6,5},{7,6},{8,11},{9,8},{10,9... | collective-permute-start | bytes 1179656 | tf_op jit(solution)/shard_map/ppermute | solution.py:508
  127.8 12.1 %collective-permute-start.36 = (bf16[192,1024]{1,0:T(8,128)(2,1)S(1)}, bf16[192,1024]{1,0:T(8,128)(2,1)S(1)}, u32[]{:S(2)}, u32[]{:S(2)}) collective-permute-start(bf16[192,1024]{1,0:T(8,128)(2,1)S(1)} %get-tuple-element.39), channel_id=1, source_target_pairs={{0,3},{1,0},{2,1},{3,2},{4,7},{5,4},{6,5},{7,6},{8,11},{9,8},{10,9... | collective-permute-start | bytes 1179656 | tf_op jit(solution)/shard_map/ppermute | solution.py:513
  128.7 13.2 %collective-permute-start.37 = (bf16[192,1024]{1,0:T(8,128)(2,1)S(1)}, bf16[192,1024]{1,0:T(8,128)(2,1)S(1)}, u32[]{:S(2)}, u32[]{:S(2)}) collective-permute-start(bf16[192,1024]{1,0:T(8,128)(2,1)S(1)} %get-tuple-element.40), channel_id=1, source_target_pairs={{0,1},{1,2},{2,3},{3,0},{4,5},{5,6},{6,7},{7,4},{8,9},{9,10},{10,1... | collective-permute-start | bytes 1179656 | tf_op jit(solution)/shard_map/ppermute | solution.py:512
  130.1 18.6 %collective-permute-start.40 = (bf16[192,1024]{1,0:T(8,128)(2,1)S(1)}, bf16[192,1024]{1,0:T(8,128)(2,1)S(1)}, u32[]{:S(2)}, u32[]{:S(2)}) collective-permute-start(bf16[192,1024]{1,0:T(8,128)(2,1)S(1)} %get-tuple-element.45), channel_id=1, source_target_pairs={{0,1},{1,2},{2,3},{3,0},{4,5},{5,6},{6,7},{7,4},{8,9},{9,10},{10,1... | collective-permute-start | bytes 1179656 | tf_op jit(solution)/shard_map/ppermute | solution.py:517
  130.1 18.5 %collective-permute-start.41 = (bf16[192,1024]{1,0:T(8,128)(2,1)S(1)}, bf16[192,1024]{1,0:T(8,128)(2,1)S(1)}, u32[]{:S(2)}, u32[]{:S(2)}) collective-permute-start(bf16[192,1024]{1,0:T(8,128)(2,1)S(1)} %get-tuple-element.46), channel_id=1, source_target_pairs={{0,3},{1,0},{2,1},{3,2},{4,7},{5,4},{6,5},{7,6},{8,11},{9,8},{10,9... | collective-permute-start | bytes 1179656 | tf_op jit(solution)/shard_map/ppermute | solution.py:518
  (11 other events, 102.6 us)
